TPU v7x, 512 devices: a whole 4x4x16 slice. The times are simulated.
512 devices in a mesh: ep: 32 (over z, core), tp: 16 (over y, x).
Axes of the slice: x: 4, y: 4, z: 16, core: 2. Of those that a mesh axis runs over, the one named last changes fastest.
Arguments:
- tokens: bfloat16 [4096, 2048], P('ep'), may hold values from -6 to 6
- cotangent: bfloat16 [4096, 2048], P('ep'), may hold values from -6 to 6
- expert_ids: int32 [4096, 2], P('ep'), may hold values from 0 to 31, all different within a row; in each aligned block of 128 rows (0 to 127, 128 to 255, ...) at most 16 rows name the same one
- route_weight: bfloat16 [4096, 2], P('ep'), may hold values from 0.19921875 to 1
- gate_weight: bfloat16 [32, 1024, 2048], P('ep', 'tp'), may hold values from -0.125 to 0.125
- up_weight: bfloat16 [32, 1024, 2048], P('ep', 'tp'), may hold values from -0.125 to 0.125
- down_weight: bfloat16 [32, 1024, 2048], P('ep', 'tp'), may hold values from -0.1875 to 0.1875
Outputs:
- tokens_grad: bfloat16 [4096, 2048], P('ep', 'tp')
- route_weight_grad: float32 [4096, 2], P('ep')
- gate_weight_grad: float32 [32, 1024, 2048], P('ep', 'tp')
- up_weight_grad: float32 [32, 1024, 2048], P('ep', 'tp')
- down_weight_grad: float32 [32, 1024, 2048], P('ep', 'tp')
Inputs may be any that keep to these rules, and one draw needn't show every extreme that they name: `expert_ids`: within each aligned block of 128 rows every expert is named at most 16 times; the two experts of a row differ.
All inputs are finite; a program needn't handle non-finite values.
Results may differ from a plain program's by a relative error of at most 0.0058.
Values may be sent and summed in bfloat16 or wider, within the bound.
No kernel may reach another device: no remote copies, remote signals or barrier semaphores. Data moves between devices by JAX's collectives and lax.ppermute only.
A program may use at most 64 MiB of HBM per device.

v0:
```python
import math

import jax
import jax.numpy as jnp
from jax import lax
from jax.sharding import PartitionSpec as P


def sent_together(arrays, axis, split_dim, concat_dim, along):
    widths = [math.prod(a.shape[along:]) for a in arrays]
    both = jnp.concatenate(
        [a.reshape(*a.shape[:along], w) for a, w in zip(arrays, widths)], axis=along
    )
    out = lax.all_to_all(both, axis, split_axis=split_dim, concat_axis=concat_dim, tiled=True)
    pieces = jnp.split(out, [sum(widths[:k]) for k in range(1, len(widths))], axis=along)
    return tuple((b.reshape(*out.shape[:along], *a.shape[along:]) for a, b in zip(arrays, pieces)))


def sent_together_2(arrays, axis, dim, along):
    widths = [a.shape[along] for a in arrays]
    both = jnp.concatenate(arrays, axis=along)
    out = lax.all_gather(both, axis, axis=dim, tiled=True)
    return tuple(jnp.split(out, [sum(widths[:k]) for k in range(1, len(widths))], axis=along))


def copy_for_each(shard, axis):
    copies = jnp.broadcast_to(shard, (lax.axis_size(axis), *shard.shape))
    return lax.all_to_all(copies, axis, split_axis=0, concat_axis=0, tiled=True)


def of_everyone(shard, axis):
    everything = copy_for_each(shard, axis)
    return jnp.sum(everything, axis=0)


def gather_turned(arrays, axis, dims):
    turned = [jnp.moveaxis(a, dim, 0) for a, dim in zip(arrays, dims)]
    both = jnp.concatenate([t.reshape(len(t), -1) for t in turned], axis=1)
    out, at, gathered = (lax.all_gather(both, axis, axis=0, tiled=True), 0, [])
    for t, dim in zip(turned, dims):
        section = out[:, at : at + t[0].size].reshape(-1, *t.shape[1:])
        gathered.append(jnp.moveaxis(section, 0, dim))
        at += t[0].size
    return tuple(gathered)


def sent_together_3(arrays, axis, split_dim, concat_dim, along):
    both = jnp.concatenate(arrays, axis=along)
    out, at, gathered = (
        lax.all_to_all(both, axis, split_axis=split_dim, concat_axis=concat_dim, tiled=True),
        0,
        [],
    )
    for a in arrays:
        gathered.append(lax.slice_in_dim(out, at, at + a.shape[along], axis=along))
        at += a.shape[along]
    return tuple(gathered)


def per_device(tokens, cotangent, expert_ids, route_weight, gate_weight, up_weight, down_weight):
    tok_rows, model_width = tokens.shape
    top_count = expert_ids.shape[1]
    local_experts = gate_weight.shape[0]
    ep_size = lax.axis_size("ep")
    tp_size = lax.axis_size("tp")
    expert_count = local_experts * ep_size
    capacity = 2 * tok_rows * top_count // expert_count
    column_span = model_width // tp_size
    flat_ids = expert_ids.reshape(-1)
    routed = flat_ids.shape[0]
    member = (flat_ids[:, None] == jnp.arange(expert_count, dtype=jnp.int32)[None, :]).astype(
        jnp.int32
    )
    rank_slot = jnp.sum((jnp.cumsum(member, axis=0) - 1) * member, axis=1)
    slot_index = flat_ids * capacity + rank_slot
    buffer_rows = expert_count * capacity
    source_pair = (
        jnp.full((buffer_rows,), routed, jnp.int32)
        .at[slot_index]
        .set(jnp.arange(routed, dtype=jnp.int32))
    )
    filled = source_pair < routed
    safe_pair = jnp.minimum(source_pair, routed - 1)
    token_of = safe_pair // top_count
    zero_value = jnp.zeros((), tokens.dtype)
    send_weight = jnp.where(filled, route_weight.reshape(-1)[safe_pair], zero_value)
    offset = lax.axis_index("tp") * column_span
    token_cols = lax.dynamic_slice_in_dim(tokens, offset, column_span, 1)
    cotangent_cols = lax.dynamic_slice_in_dim(cotangent, offset, column_span, 1)
    part_tokens, part_cotangent, got_weight = sent_together(
        (token_cols[token_of], cotangent_cols[token_of], send_weight), "ep", 0, 0, 1
    )
    got_tokens, got_cotangent = sent_together_2((part_tokens, part_cotangent), "tp", 1, 0)
    block_shape = (ep_size, local_experts, capacity, model_width)
    routed_rows = got_tokens.reshape(block_shape)
    routed_cotangent = got_cotangent.reshape(block_shape)
    pair_weight = got_weight.reshape(ep_size, local_experts, capacity, 1).astype(jnp.float32)
    pre_gate = jnp.einsum(
        "secd,efd->secf", routed_rows, gate_weight, preferred_element_type=jnp.float32
    )
    pre_up = jnp.einsum(
        "secd,efd->secf", routed_rows, up_weight, preferred_element_type=jnp.float32
    )
    sigma = jax.nn.sigmoid(pre_gate)
    silu_gate = pre_gate * sigma
    hidden = silu_gate * pre_up
    back_hidden = jnp.einsum(
        "secd,efd->secf", routed_cotangent, down_weight, preferred_element_type=jnp.float32
    )
    pair_products = of_everyone(jnp.sum(hidden * back_hidden, axis=3), "tp")
    scaled = pair_weight * back_hidden
    grad_gate = (scaled * pre_up * sigma * (1.0 + pre_gate * (1.0 - sigma))).astype(jnp.bfloat16)
    grad_up = (scaled * silu_gate).astype(jnp.bfloat16)
    weighted = (pair_weight * hidden).astype(jnp.bfloat16)
    down_grad = jnp.einsum(
        "secf,secd->efd", weighted, routed_cotangent, preferred_element_type=jnp.float32
    )
    gate_grad = jnp.einsum(
        "secf,secd->efd", grad_gate, routed_rows, preferred_element_type=jnp.float32
    )
    up_grad = jnp.einsum("secf,secd->efd", grad_up, routed_rows, preferred_element_type=jnp.float32)
    full_gate, full_up = gather_turned((grad_gate, grad_up), "tp", (3, 3))
    gate_cols, up_cols = sent_together_3((gate_weight, up_weight), "tp", 2, 1, 0)
    pair_grad = (
        jnp.einsum("secf,efd->secd", full_gate, gate_cols, preferred_element_type=jnp.float32)
        + jnp.einsum("secf,efd->secd", full_up, up_cols, preferred_element_type=jnp.float32)
    ).astype(jnp.bfloat16)
    returned = lax.all_to_all(
        pair_grad.reshape(buffer_rows, column_span), "ep", split_axis=0, concat_axis=0, tiled=True
    )
    returned_products = lax.all_to_all(
        pair_products.reshape(buffer_rows), "ep", split_axis=0, concat_axis=0, tiled=True
    )
    per_pair = returned[slot_index].astype(jnp.float32).reshape(tok_rows, top_count, column_span)
    tokens_grad = jnp.sum(per_pair, axis=1).astype(jnp.bfloat16)
    route_grad = returned_products[slot_index].reshape(tok_rows, top_count)
    return (tokens_grad, route_grad, gate_grad, up_grad, down_grad)


def solution(mesh):
    in_specs = (
        P("ep", None),
        P("ep", None),
        P("ep", None),
        P("ep", None),
        P("ep", "tp", None),
        P("ep", "tp", None),
        P("ep", "tp", None),
    )
    out_specs = (
        P("ep", "tp"),
        P("ep", None),
        P("ep", "tp", None),
        P("ep", "tp", None),
        P("ep", "tp", None),
    )
    return jax.shard_map(
        per_device, mesh=mesh, in_specs=in_specs, out_specs=out_specs, check_vma=False
    )
```

profile of v0, /device:TPU:1, one launch (start us, length us, event | category | flops | bytes accessed | tf_op | source)
XLA Modules:
  0.0 244.9 jit_solution(12894059135491128948)
XLA Ops:
  7.2 0.7 broadcast_multiply_fusion
  7.9 0.8 copy.70
  9.0 0.8 copy.73
  11.2 1.4 scatter_custom_fusion
  12.6 3.4 %gather_fusion.2 = bf16[512]{0:T(512)(128)(2,1)S(1)} fusion(bf16[256]{0:T(256)(128)(2,1)S(1)} %reshape.200, s32[1024]{0:T(1024)S(1)} %get-tuple-element.38), kind=kCustom, calls=%fused_computation.2 | custom fusion | bytes 4096 | tf_op jit(solution)/shard_map/gather | solution.py:86
  16.0 0.8 constant_dynamic-slice_fusion
  16.8 1.3 gather_fusion.1
  18.1 1.3 gather_fusion
  19.8 44.3 %all_to_all.53 = bf16[32,16,257]{2,1,0:T(8,128)(2,1)S(1)} all-to-all(bf16[32,16,257]{2,1,0:T(8,128)(2,1)S(1)} %pad_maximum_fusion.1), channel_id=1, replica_groups=mesh['ep'=32,'tp'=16] {'ep'}, dimensions={0} | all-to-all | bytes 526336 | tf_op jit(solution)/shard_map/all_to_all | solution.py:14
  64.1 0.7 pad_maximum_fusion.2
  65.1 62.1 %all-gather.3.cloned.1.call-done = bf16[1024,2048]{1,0:T(8,128)(2,1)} async-done(((bf16[1024,128]{1,0:T(8,128)(2,1)}), bf16[1024,2048]{1,0:T(8,128)(2,1)}) %all-gather.3.cloned.1.call-update) | async-done | bytes 4194320 | tf_op jit(solution)/shard_map/all_gather | solution.py:22
  127.2 2.6 %fusion.49 = (bf16[512,2048]{1,0:T(8,128)(2,1)S(1)}, bf16[512,2048]{1,0:T(8,128)(2,1)S(1)}) fusion(bf16[1024,2048]{1,0:T(8,128)(2,1)} %all-gather.3.cloned.1.call-done), kind=kLoop, calls=%fused_computation.95 | loop fusion | bytes 8388608 | tf_op jit(solution)/shard_map/split | solution.py:23
  129.9 0.7 fusion.28
  131.0 0.7 fusion.26
  131.7 1.4 fusion.20
  133.3 0.6 pad_maximum_fusion.3
  134.0 0.8 pad_maximum_fusion
  134.8 2.3 copy.67
  137.2 1.5 reshape.290
  138.7 4.7 %all-to-all-start = ((bf16[16,2,8192]{2,1,0:T(2,128)(2,1)}), bf16[16,2,8192]{2,1,0:T(2,128)(2,1)}, u32[]{:S(2)}, u32[]{:S(2)}) async-start(bf16[16,2,8192]{2,1,0:T(2,128)(2,1)} %reshape.290), calls=%async_computation | async-start | bytes 1048576 | tf_op jit(solution)/shard_map/all_to_all | solution.py:50
  143.4 9.4 %all-to-all-done = bf16[16,2,8192]{2,1,0:T(2,128)(2,1)} async-done(((bf16[16,2,8192]{2,1,0:T(2,128)(2,1)}), bf16[16,2,8192]{2,1,0:T(2,128)(2,1)}, u32[]{:S(2)}, u32[]{:S(2)}) %all-to-all-start) | async-done | bytes 524320 | tf_op jit(solution)/shard_map/all_to_all | solution.py:50
  152.9 3.0 %reshape.291 = bf16[2048,2,64]{2,1,0:T(2,128)(2,1)S(1)} reshape(bf16[16,2,8192]{2,1,0:T(2,128)(2,1)} %all-to-all-done) | data formatting | bytes 1048576
  155.9 1.8 copy.68
  157.7 1.8 fusion.51
  159.6 1.3 fusion.10
  160.9 0.7 reshape.292
  161.7 3.5 %all-to-all-start.3 = ((f32[16,1,512]{2,1,0:T(1,128)}), f32[16,1,512]{2,1,0:T(1,128)S(1)}, u32[]{:S(2)}, u32[]{:S(2)}) async-start(f32[16,1,512]{2,1,0:T(1,128)} %reshape.292), calls=%async_computation.3 | async-start | bytes 65536 | tf_op jit(solution)/shard_map/all_to_all | solution.py:28
  165.2 3.0 %convolution_bitcast_fusion = f32[1,64,2048]{2,1,0:T(8,128)} fusion(bf16[32,16,2048]{2,1,0:T(8,128)(2,1)} %bitcast.214, f32[32,16]{1,0:T(8,128)S(1)} %reshape.217, f32[32,16,64]{2,1,0:T(8,128)S(1)} %copy-done.5, f32[32,16,64]{2,1,0:T(8,128)S(1)} %copy-done.6), kind=kOutput, calls=%fused_computation.6 | convolution fusion | flops 134447104 | bytes 2885632 | tf_op jit(solution)/shard_map/secf,secd->efd/dot_general | solution.py:115
  168.2 3.4 %all-to-all-done.3 = f32[16,1,512]{2,1,0:T(1,128)S(1)} async-done(((f32[16,1,512]{2,1,0:T(1,128)}), f32[16,1,512]{2,1,0:T(1,128)S(1)}, u32[]{:S(2)}, u32[]{:S(2)}) %all-to-all-start.3) | async-done | bytes 32800 | tf_op jit(solution)/shard_map/all_to_all | solution.py:28
  172.1 0.7 reduce.11
  172.9 0.7 copy.83
  173.6 16.6 %all-to-all-start.4 = ((f32[32,16,1]{1,2,0:T(1,128)}), f32[32,16,1]{1,2,0:T(1,128)S(1)}, u32[]{:S(2)}, u32[]{:S(2)}) async-start(f32[32,16,1]{1,2,0:T(1,128)} %copy.83), calls=%async_computation.4 | async-start | bytes 32768 | tf_op jit(solution)/shard_map/all_to_all | solution.py:131
  190.3 3.4 %all-gather.5.cloned.1.call-done = bf16[1024,1024]{1,0:T(8,128)(2,1)} async-done(((bf16[64,1024]{1,0:T(8,128)(2,1)}), bf16[1024,1024]{1,0:T(8,128)(2,1)}) %all-gather.5.cloned.1.call-update) | async-done | bytes 2097168 | tf_op jit(solution)/shard_map/all_gather | solution.py:39
  193.6 3.0 %fusion.50 = (bf16[1024,512]{1,0:T(8,128)(2,1)}, bf16[1024,512]{1,0:T(8,128)(2,1)}) fusion(bf16[1024,1024]{1,0:T(8,128)(2,1)} %all-gather.5.cloned.1.call-done), kind=kLoop, calls=%fused_computation.96 | loop fusion | bytes 4194304 | tf_op jit(solution)/shard_map/slice | solution.py:41
  196.6 2.3 copy.86
  198.9 2.3 copy.85
  201.2 2.1 fusion.3
  203.3 2.0 fusion.1
  205.3 0.7 copy.81
  206.0 14.6 %all-to-all-start.2 = ((bf16[32,16,128]{2,1,0:T(8,128)(2,1)}), bf16[32,16,128]{2,1,0:T(8,128)(2,1)S(1)}, u32[]{:S(2)}, u32[]{:S(2)}) async-start(bf16[32,16,128]{2,1,0:T(8,128)(2,1)} %copy.81), calls=%async_computation.2 | async-start | bytes 262144 | tf_op jit(solution)/shard_map/all_to_all | solution.py:128
  220.6 1.4 convolution_bitcast_fusion.1
  222.0 1.4 convolution_bitcast_fusion.2
  223.9 0.7 reduce.10
  224.7 1.9 gather_fusion.4
  226.8 0.6 copy.84
  227.4 9.0 %all-to-all-done.2 = bf16[32,16,128]{2,1,0:T(8,128)(2,1)S(1)} async-done(((bf16[32,16,128]{2,1,0:T(8,128)(2,1)}), bf16[32,16,128]{2,1,0:T(8,128)(2,1)S(1)}, u32[]{:S(2)}, u32[]{:S(2)}) %all-to-all-start.2) | async-done | bytes 131104 | tf_op jit(solution)/shard_map/all_to_all | solution.py:128
  236.4 0.9 gather_fusion.3
  237.3 0.8 reduce_sum.43
  (55 shorter events, 4.3 us)
Async XLA Ops:
  7.2 122.7 %copy-start = (bf16[1,64,2048]{2,1,0:T(8,128)(2,1)S(1)}, bf16[1,64,2048]{2,1,0:T(8,128)(2,1)}, u32[]{:S(2)}) copy-start(bf16[1,64,2048]{2,1,0:T(8,128)(2,1)} %param.13) | copy-start | bytes 786436
  7.2 120.0 %all-gather.3.cloned.1.call-start = ((), (), s32[]{:S(2)}) async-start(), calls=%async_computation.5 | async-start | bytes 4456448 | tf_op jit(solution)/shard_map/all_gather | solution.py:22
  64.9 128.8 %all-gather.5.cloned.1.call-start = ((), (), s32[]{:S(2)}) async-start(), calls=%async_computation.6 | async-start | bytes 2228224 | tf_op jit(solution)/shard_map/all_gather | solution.py:39
  129.8 1.9 copy-start.1
  129.8 1.1 copy-start.7
  129.9 1.8 copy-start.8
  130.6 2.5 %copy-start.2 = (f32[32,16,64]{2,1,0:T(8,128)}, f32[32,16,64]{2,1,0:T(8,128)S(1)}, u32[]{:S(2)}) copy-start(f32[32,16,64]{2,1,0:T(8,128)S(1)} %fusion.28) | copy-start | bytes 393220
  131.7 1.4 copy-start.4
  138.7 14.2 %all-to-all-start = ((bf16[16,2,8192]{2,1,0:T(2,128)(2,1)}), bf16[16,2,8192]{2,1,0:T(2,128)(2,1)}, u32[]{:S(2)}, u32[]{:S(2)}) async-start(bf16[16,2,8192]{2,1,0:T(2,128)(2,1)} %reshape.290), calls=%async_computation | async-start | bytes 1048576 | tf_op jit(solution)/shard_map/all_to_all | solution.py:50
  157.7 7.4 %copy-start.5 = (f32[32,16,64]{2,1,0:T(8,128)S(1)}, f32[32,16,64]{2,1,0:T(8,128)}, u32[]{:S(2)}) copy-start(f32[32,16,64]{2,1,0:T(8,128)} %copy-done.4) | copy-start | bytes 393220
  157.7 7.4 %copy-start.6 = (f32[32,16,64]{2,1,0:T(8,128)S(1)}, f32[32,16,64]{2,1,0:T(8,128)}, u32[]{:S(2)}) copy-start(f32[32,16,64]{2,1,0:T(8,128)} %get-tuple-element.37) | copy-start | bytes 393220
  161.7 9.9 %all-to-all-start.3 = ((f32[16,1,512]{2,1,0:T(1,128)}), f32[16,1,512]{2,1,0:T(1,128)S(1)}, u32[]{:S(2)}, u32[]{:S(2)}) async-start(f32[16,1,512]{2,1,0:T(1,128)} %reshape.292), calls=%async_computation.3 | async-start | bytes 65536 | tf_op jit(solution)/shard_map/all_to_all | solution.py:28
  173.6 32.4 %all-to-all-start.4 = ((f32[32,16,1]{1,2,0:T(1,128)}), f32[32,16,1]{1,2,0:T(1,128)S(1)}, u32[]{:S(2)}, u32[]{:S(2)}) async-start(f32[32,16,1]{1,2,0:T(1,128)} %copy.83), calls=%async_computation.4 | async-start | bytes 32768 | tf_op jit(solution)/shard_map/all_to_all | solution.py:131
  201.2 19.4 %copy-start.3 = (f32[32,16,64]{2,1,0:T(8,128)S(1)}, f32[32,16,64]{2,1,0:T(8,128)}, u32[]{:S(2)}) copy-start(f32[32,16,64]{2,1,0:T(8,128)} %copy-done.2) | copy-start | bytes 393220
  206.0 30.4 %all-to-all-start.2 = ((bf16[32,16,128]{2,1,0:T(8,128)(2,1)}), bf16[32,16,128]{2,1,0:T(8,128)(2,1)S(1)}, u32[]{:S(2)}, u32[]{:S(2)}) async-start(bf16[32,16,128]{2,1,0:T(8,128)(2,1)} %copy.81), calls=%async_computation.2 | async-start | bytes 262144 | tf_op jit(solution)/shard_map/all_to_all | solution.py:128
Sparse Core Ops, SparseCore 0:
  65.0 62.1 all-gather.2
  134.1 59.4 all-gather.4
where the time goes:
time: 246 us; the launch traced here: 245 us
  waiting for transfers between devices  87.4 us (36%)
  blocking collectives  44.3 us (18%)
  starting transfers between devices  39.5 us (16%)
  local copies, waits for them, and re-layouts  39.3 us (16%)
  between operations  14.4 us (6%)
  matrix products  12.7 us (5%)
  other arithmetic  7.35 us (3%)
    all_gather x1, waiting for transfers between devices, sent_together_2(): out = lax.all_gather(both, axis, axis=dim, tiled=True)  62.1 us
    all_to_all x1, blocking collectives, sent_together(): lax.all_to_all(both, axis, split_axis=split_dim, concat_axis=concat_dim,...  44.3 us
    all_to_all x1, starting transfers between devices, per_device(): lax.all_to_all(pair_products.reshape(buffer_rows), 'ep', split_axis=0, co...  16.6 us
    all_to_all x1, starting transfers between devices, per_device(): lax.all_to_all(pair_grad.reshape(buffer_rows, column_span), 'ep', split_a...  14.6 us
    unnamed x28, local copies, waits for them, and re-layouts  12.6 us
    all_to_all x1, waiting for transfers between devices, sent_together_3(): lax.all_to_all(both, axis, split_axis=split_dim, concat_axis=concat_dim,...  9.44 us
    all_to_all x1, waiting for transfers between devices, per_device(): lax.all_to_all(pair_grad.reshape(buffer_rows, column_span), 'ep', split_a...  9.01 us
  transfers between devices with their start and end apart: 6, of which 5 were waited for; matrix products, arithmetic and copies ran while one was open for 15% of the time, Pallas kernels for 0%

commit v1 on v0

v1 whole, which is shorter than its diff:
```python
import functools

import jax
import jax.numpy as jnp
from jax import lax
from jax.experimental import pallas as pl
from jax.experimental.pallas import tpu as pltpu
from jax.sharding import Mesh
from jax.sharding import PartitionSpec as P

BF = jnp.bfloat16
F32 = jnp.float32
I32 = jnp.int32
NZ = 16
TP = 16
TOK = 128
CAP = 16
COL = 128
HID = 64
ROWS = 512
BLK = 4
RB = ROWS // BLK
EXT = 8


def iota(shape, dim):
    return lax.broadcasted_iota(I32, shape, dim)


def dot(a, b, ca, cb, precision=None):
    return lax.dot_general(
        a, b, (((ca,), (cb,)), ((), ())), precision=precision, preferred_element_type=F32
    )


def routing(ids_ref, core):
    experts = 2 * NZ
    row = iota((experts, TOK), 0)
    first = (ids_ref[0:1, :] == row).astype(F32)
    second = (ids_ref[1:2, :] == row).astype(F32)
    member = first + second
    earlier = (iota((TOK, TOK), 0) < iota((TOK, TOK), 1)).astype(BF)
    rank = dot(member.astype(BF), earlier, 1, 0)
    slots = 2 * NZ * CAP
    slot = iota((slots, experts), 0)
    half = slot >> 8
    expert = 2 * ((slot & 255) >> 4) + jnp.where(half == 0, core, 1 - core)
    expand = (expert == iota((slots, experts), 1)).astype(BF)
    hit = dot(expand, member.astype(BF), 1, 0)
    at = dot(expand, rank.astype(BF), 1, 0)
    place = (iota((slots, TOK), 0) & 15).astype(F32)
    chosen = (hit > 0.5) & (at == place)
    return first, second, rank, expand, chosen


def dispatch_kernel(s_ref, ids_ref, w_ref, tok_ref, cot_ref, own_ref, other_ref):
    first, second, _, expand, chosen = routing(ids_ref, s_ref[1])
    w = w_ref[...].astype(F32)
    weighted = first * w[0:1, :] + second * w[1:2, :]
    scale = dot(expand, weighted.astype(BF), 1, 0)
    pick = jnp.where(chosen, 1.0, 0.0).astype(BF)
    pick_scaled = jnp.where(chosen, scale, 0.0).astype(BF)
    rows = dot(pick, tok_ref[...], 1, 0).astype(BF)
    cots = dot(pick_scaled, cot_ref[...], 1, 0).astype(BF)
    half = NZ * CAP
    own_ref[:, 0] = rows[:half].reshape(NZ, CAP, COL)
    own_ref[:, 1] = cots[:half].reshape(NZ, CAP, COL)
    other_ref[:, 0] = rows[half:].reshape(NZ, CAP, COL)
    other_ref[:, 1] = cots[half:].reshape(NZ, CAP, COL)


def dispatch(where, ids, w, tokens, cotangent):
    full = lambda *shape: pl.BlockSpec(shape, lambda i, s: (0,) * len(shape))
    out = jax.ShapeDtypeStruct((NZ, 2, CAP, COL), BF)
    return pl.pallas_call(
        dispatch_kernel,
        grid_spec=pltpu.PrefetchScalarGridSpec(
            num_scalar_prefetch=1,
            grid=(1,),
            in_specs=[
                full(2, TOK),
                full(2, TOK),
                pl.BlockSpec((TOK, COL), lambda i, s: (0, s[0])),
                pl.BlockSpec((TOK, COL), lambda i, s: (0, s[0])),
            ],
            out_specs=[full(NZ, 2, CAP, COL)] * 2,
        ),
        out_shape=[out, out],
        name="dispatch",
        cost_estimate=pl.CostEstimate(flops=10**8, bytes_accessed=10**6, transcendentals=0),
    )(where, ids, w, tokens, cotangent)


def forward_kernel(x_ref, wg_ref, wu_ref, wd_ref, part_ref, gg_ref, gu_ref, wt_ref, xt, xc):
    for j in range(TP):
        xt[:, j * COL : (j + 1) * COL] = x_ref[j, :, 0].reshape(RB, COL)
        xc[:, j * COL : (j + 1) * COL] = x_ref[j, :, 1].reshape(RB, COL)
    wg, wu = wg_ref[0], wu_ref[0]
    gate = dot(xt[...], wg, 1, 1)
    up = dot(xt[...], wu, 1, 1)
    back = dot(xc[...], wd_ref[0], 1, 1)
    sigma = 1.0 / (1.0 + jnp.exp(-gate))
    silu = gate * sigma
    hidden = silu * up
    grad_gate = (back * up * sigma * (1.0 + gate * (1.0 - sigma))).astype(BF)
    grad_up = (back * silu).astype(BF)
    gg_ref[...] = grad_gate
    gu_ref[...] = grad_up
    wt_ref[...] = hidden.astype(BF)
    total = jnp.sum(hidden * back, axis=1, keepdims=True)
    lane = iota((RB, COL), 1)
    spread = jnp.where((lane & 31) == (iota((RB, COL), 0) & 31), total, 0.0)
    group = (iota((EXT, RB), 0) == (iota((EXT, RB), 1) >> 5)).astype(F32)
    sums = dot(group, spread, 1, 0, lax.Precision.HIGHEST)
    high = sums.astype(BF)
    low = (sums - high.astype(F32)).astype(BF)
    extra = jnp.where(iota((EXT, COL), 1) < 32, high.astype(F32), low.astype(F32)).astype(BF)
    for j in range(TP):
        cols = slice(j * COL, (j + 1) * COL)
        piece = dot(grad_gate, wg[:, cols], 1, 0) + dot(grad_up, wu[:, cols], 1, 0)
        part_ref[j, 0, :RB] = piece.astype(BF)
        part_ref[j, 0, RB:] = extra


def forward(x, wg, wu, wd):
    d = TP * COL
    weight = pl.BlockSpec((1, HID, d), lambda i: (0, 0, 0))
    grads = pl.BlockSpec((RB, HID), lambda i: (i, 0))
    gs = jax.ShapeDtypeStruct((ROWS, HID), BF)
    return pl.pallas_call(
        forward_kernel,
        grid=(BLK,),
        in_specs=[
            pl.BlockSpec((TP, NZ // BLK, 2, 2 * CAP, COL), lambda i: (0, i, 0, 0, 0)),
            weight,
            weight,
            weight,
        ],
        out_specs=[
            pl.BlockSpec((TP, 1, RB + EXT, COL), lambda i: (0, i, 0, 0)),
            grads,
            grads,
            grads,
        ],
        out_shape=[jax.ShapeDtypeStruct((TP, BLK, RB + EXT, COL), BF), gs, gs, gs],
        scratch_shapes=[pltpu.VMEM((RB, d), BF), pltpu.VMEM((RB, d), BF)],
        name="forward",
        cost_estimate=pl.CostEstimate(flops=7 * 10**8, bytes_accessed=7 * 10**6, transcendentals=10**5),
    )(x, wg, wu, wd)


def weights_kernel(x_ref, gg_ref, gu_ref, wt_ref, dg_ref, du_ref, dd_ref):
    gg, gu, wt = gg_ref[...], gu_ref[...], wt_ref[...]
    for j in range(x_ref.shape[0]):
        cols = slice(j * COL, (j + 1) * COL)
        rows = x_ref[j, :, 0].reshape(ROWS, COL)
        cots = x_ref[j, :, 1].reshape(ROWS, COL)
        dg_ref[0, :, cols] = dot(gg, rows, 0, 0)
        du_ref[0, :, cols] = dot(gu, rows, 0, 0)
        dd_ref[0, :, cols] = dot(wt, cots, 0, 0)


def weights(x, gg, gu, wt):
    d, pieces = TP * COL, 4
    out = jax.ShapeDtypeStruct((1, HID, d), F32)
    grads = pl.BlockSpec((ROWS, HID), lambda i: (0, 0))
    return pl.pallas_call(
        weights_kernel,
        grid=(TP // pieces,),
        in_specs=[
            pl.BlockSpec((pieces, NZ, 2, 2 * CAP, COL), lambda i: (i, 0, 0, 0, 0)),
            grads,
            grads,
            grads,
        ],
        out_specs=[pl.BlockSpec((1, HID, pieces * COL), lambda i: (0, 0, i))] * 3,
        out_shape=[out, out, out],
        name="weights",
        cost_estimate=pl.CostEstimate(flops=4 * 10**9, bytes_accessed=6 * 10**6, transcendentals=0),
    )(x, gg, gu, wt)


def total_kernel(p_ref, out_ref):
    rows = p_ref[0, 0].astype(F32)
    for j in range(1, TP):
        rows = rows + p_ref[j, 0].astype(F32)
    out_ref[:, : 2 * CAP] = rows[:RB].astype(BF).reshape(NZ // BLK, 2 * CAP, COL)
    sums = rows[RB:]
    sums = sums + pltpu.roll(sums, COL - 32, 1)
    high = sums.astype(BF).astype(F32)
    low = pltpu.roll(sums - high, 32, 1)
    extra = jnp.where(iota((EXT, COL), 1) < 32, high, low)
    for k in range(NZ // BLK):
        out_ref[k, 2 * CAP :] = jnp.broadcast_to(extra[k : k + 1], (EXT, COL)).astype(BF)


def total(part):
    return pl.pallas_call(
        total_kernel,
        grid=(BLK,),
        in_specs=[pl.BlockSpec((TP, 1, RB + EXT, COL), lambda i: (0, i, 0, 0))],
        out_specs=pl.BlockSpec((NZ // BLK, 2 * CAP + EXT, COL), lambda i: (i, 0, 0)),
        out_shape=jax.ShapeDtypeStruct((NZ, 2 * CAP + EXT, COL), BF),
        name="total",
        cost_estimate=pl.CostEstimate(flops=10**7, bytes_accessed=2 * 10**6, transcendentals=0),
    )(part)


def combine_kernel(s_ref, ids_ref, w_ref, own_ref, other_ref, tok_ref, route_ref):
    core = s_ref[1]
    first, second, rank, _, chosen = routing(ids_ref, core)
    pick = jnp.where(chosen, 1.0, 0.0).astype(BF)
    half = NZ * CAP
    own = own_ref[:, :CAP].reshape(half, COL)
    other = other_ref[:, :CAP].reshape(half, COL)
    tok_ref[...] = (dot(pick[:half], own, 0, 0) + dot(pick[half:], other, 0, 0)).astype(BF)
    own_sums = own_ref[:, 2 * CAP :].reshape(NZ * EXT, COL)
    other_sums = other_ref[:, CAP:].reshape(NZ * EXT, COL)
    row = iota((NZ * EXT, TOK), 0)
    leads = (row & 7) == 0
    chip = row >> 3
    lane = iota((COL, TOK), 0)
    w = w_ref[...].astype(F32)
    for k, member in enumerate((first, second)):
        ids = ids_ref[k : k + 1, :]
        at = jnp.sum(member * rank, axis=0, keepdims=True).astype(I32)
        mine = (leads & (ids == 2 * chip + core)).astype(BF)
        theirs = (leads & (ids == 2 * chip + 1 - core)).astype(BF)
        near = dot(own_sums, mine, 0, 0)
        far = dot(other_sums, theirs, 0, 0)
        near = jnp.where((lane == at) | (lane == at + 32), near, 0.0)
        far = jnp.where((lane == at + 16) | (lane == at + 48), far, 0.0)
        route_ref[k : k + 1, :] = jnp.sum(near + far, axis=0, keepdims=True) / w[k : k + 1, :]


def combine(where, ids, w, own, other):
    full = lambda *shape: pl.BlockSpec(shape, lambda i, s: (0,) * len(shape))
    return pl.pallas_call(
        combine_kernel,
        grid_spec=pltpu.PrefetchScalarGridSpec(
            num_scalar_prefetch=1,
            grid=(1,),
            in_specs=[
                full(2, TOK),
                full(2, TOK),
                full(NZ, 2 * CAP + EXT, COL),
                full(NZ, CAP + EXT, COL),
            ],
            out_specs=[full(TOK, COL), full(2, TOK)],
        ),
        out_shape=[jax.ShapeDtypeStruct((TOK, COL), BF), jax.ShapeDtypeStruct((2, TOK), F32)],
        name="combine",
        cost_estimate=pl.CostEstimate(flops=10**8, bytes_accessed=10**6, transcendentals=0),
    )(where, ids, w, own, other)


def exchange(x, axis):
    return lax.all_to_all(x, axis, split_axis=0, concat_axis=0, tiled=True)


def per_device(tokens, cotangent, expert_ids, route_weight, gate_weight, up_weight, down_weight):
    swap = [(0, 1), (1, 0)]
    tp = lax.axis_index("y") * lax.axis_size("x") + lax.axis_index("x")
    where = jnp.stack([tp, lax.axis_index("c")]).astype(I32)
    ids, w = expert_ids.T, route_weight.T
    own, other = dispatch(where, ids, w, tokens, cotangent)
    got = lax.ppermute(other, "c", swap)
    mine = jnp.stack([own, got], axis=2).reshape(NZ, 2, 2 * CAP, COL)
    mine = exchange(mine, "z")
    gathered = exchange(jnp.broadcast_to(mine[None], (TP, *mine.shape)), ("y", "x"))
    part, gg, gu, wt = forward(gathered, gate_weight, up_weight, down_weight)
    parts = exchange(part, ("y", "x"))
    gate_grad, up_grad, down_grad = weights(gathered, gg, gu, wt)
    back = exchange(total(parts), "z")
    far = lax.ppermute(back[:, CAP:], "c", swap)
    tokens_grad, route_grad = combine(where, ids, w, back, far)
    return tokens_grad, route_grad.T, gate_grad, up_grad, down_grad


def solution(mesh):
    grid = Mesh(mesh.devices.reshape(NZ, 2, 4, 4), ("z", "c", "y", "x"))
    ep, tp = ("z", "c"), ("y", "x")
    weight = P(ep, tp, None)
    return jax.shard_map(
        per_device,
        mesh=grid,
        in_specs=(P(ep, None), P(ep, None), P(ep, None), P(ep, None), weight, weight, weight),
        out_specs=(P(ep, tp), P(ep, None), weight, weight, weight),
        check_vma=False,
    )
```

time: 246 us -> 178 us (0.72)
  blocking collectives: 44.3 us -> 135 us
  waiting for transfers between devices: 87.4 us -> 1.18 us
  local copies, waits for them, and re-layouts: 39.3 us -> 1.71 us
  starting transfers between devices: 39.5 us -> 15.4 us
  Pallas kernels: 0 us -> 22 us
  between operations: 14.4 us -> 0.69 us
  matrix products: 12.7 us -> 0 us
  other arithmetic: 7.35 us -> 1.52 us
    all_to_all x1 -> x4, blocking collectives: 44.3 us -> 135 us  [exchange(): return lax.all_to_all(x, axis, split_axis=0, concat_axis=0, tiled=True)]
    all_gather x2 -> x0, waiting for transfers between devices: 65.5 us -> none  [the longest x1 62.1 us: sent_together_2(): out = lax.all_gather(both, axis, axis=dim, tiled=True)]
    all_to_all x4 -> x0, starting transfers between devices: 39.4 us -> none  [the longest x1 16.6 us: per_device(): lax.all_to_all(pair_products.reshape(buffer_rows), 'ep', split_axis=0, co...]
    pallas_call x0 -> x5, Pallas kernels: none -> 22 us  [the longest x1 7.88 us: forward(): pl.pallas_call(forward_kernel, grid=(BLK,), in_specs=[pl.BlockSpec((TP, N...]
    all_to_all x4 -> x0, waiting for transfers between devices: 21.8 us -> none  [the longest x1 9.44 us: sent_together_3(): lax.all_to_all(both, axis, split_axis=split_dim, concat_axis=concat_dim,...]
    ppermute x0 -> x2, starting transfers between devices: none -> 15.4 us  [the longest x1 8.73 us: per_device(): got = lax.ppermute(other, 'c', swap)]
    dot_general x8 -> x0, matrix products: 12.7 us -> none  [the longest x1 2.98 us: per_device(): jnp.einsum('secf,secd->efd', weighted, routed_cotangent, preferred_elemen...]
    unnamed x28 -> x4, local copies, waits for them, and re-layouts: 12.6 us -> 0.63 us
  transfers between devices with their start and end apart: 6 -> 2, of which waited for: 5 -> 1; matrix products, arithmetic and copies ran while one was open for 15% -> 0% of each run, Pallas kernels for 0% -> 3%
where the time goes in v1:
time: 178 us; the launch traced here: 177 us
  blocking collectives  135 us (76%)
  Pallas kernels  22 us (12%)
  starting transfers between devices  15.4 us (9%)
    all_to_all x4, blocking collectives, exchange(): return lax.all_to_all(x, axis, split_axis=0, concat_axis=0, tiled=True)  135 us
    ppermute x1, starting transfers between devices, per_device(): got = lax.ppermute(other, 'c', swap)  8.73 us
    pallas_call x1, Pallas kernels, forward(): pl.pallas_call(forward_kernel, grid=(BLK,), in_specs=[pl.BlockSpec((TP, N...  7.88 us
    ppermute x1, starting transfers between devices, per_device(): far = lax.ppermute(back[:, CAP:], 'c', swap)  6.63 us
    pallas_call x1, Pallas kernels, weights(): pl.pallas_call(weights_kernel, grid=(TP // pieces,), in_specs=[pl.BlockSp...  4.96 us
    pallas_call x1, Pallas kernels, total(): pl.pallas_call(total_kernel, grid=(BLK,), in_specs=[pl.BlockSpec((TP, 1,...  3.7 us
  transfers between devices with their start and end apart: 2, of which 1 were waited for; matrix products, arithmetic and copies ran while one was open for 0% of the time, Pallas kernels for 3%

profile of v1, /device:TPU:1, one launch (start us, length us, event | category | flops | bytes accessed | tf_op | source)
XLA Modules:
  0.0 177.2 jit_solution(13899602582063943003)
XLA Ops:
  0.6 0.6 pad_add_fusion.s_ref
  1.2 2.6 %dispatch.1 = (bf16[16,2,16,128]{3,2,1,0:T(8,128)(2,1)}, bf16[16,2,16,128]{3,2,1,0:T(8,128)(2,1)}) custom-call(s32[2]{0:T(128)} %pad_add_fusion.s_ref, s32[2,128]{1,0:T(2,128)} %bitcast.11, bf16[2,128]{1,0:T(2,128)(2,1)} %bitcast.13, bf16[128,2048]{1,0:T(8,128)(2,1)} %tok_ref.1, bf16[128,2048]{1,0:T(8,128)(2,1)} %cot_ref.1), custom_call_target="tpu_custom_call" | custom-call | flops 100000000 | bytes 1000000 | tf_op jit(solution)/shard_map/dispatch/pallas_call | solution.py:75
  3.8 8.7 %collective-permute-start = (bf16[16,2,16,128]{3,2,1,0:T(8,128)(2,1)}, bf16[16,2,16,128]{3,2,1,0:T(8,128)(2,1)S(1)}, u32[]{:S(2)}, u32[]{:S(2)}) collective-permute-start(bf16[16,2,16,128]{3,2,1,0:T(8,128)(2,1)} %get-tuple-element.17), channel_id=1, source_target_pairs={{0,16},{16,0},{1,17},{17,1},{2,18},{18,2},{3,19},{19,3},{4,20},{20... | collective-permute-start | bytes 393224 | tf_op jit(solution)/shard_map/ppermute | solution.py:267
  12.6 1.2 collective-permute-done
  13.7 0.9 pad_maximum_fusion
  14.7 23.4 %all_to_all.20 = bf16[16,2,32,128]{3,2,1,0:T(8,128)(2,1)S(1)} all-to-all(bf16[16,2,32,128]{3,2,1,0:T(8,128)(2,1)S(1)} %bitcast.8), channel_id=1, replica_groups=mesh['z'=16,'c'=2,'y'=4,'x'=4] {'z'}, dimensions={0} | all-to-all | bytes 524288 | tf_op jit(solution)/shard_map/all_to_all | solution.py:258
  38.1 1.1 broadcast_in_dim.2
  39.2 53.3 %all_to_all.21.x_ref = bf16[16,16,2,32,128]{4,3,2,1,0:T(8,128)(2,1)} all-to-all(bf16[16,16,2,32,128]{4,3,2,1,0:T(8,128)(2,1)S(1)} %broadcast_in_dim.2), channel_id=1, replica_groups=mesh['z'=16,'c'=2,'y'=4,'x'=4] {'y','x'}, dimensions={0} | all-to-all | bytes 8388608 | tf_op jit(solution)/shard_map/all_to_all | solution.py:258
  92.5 7.9 %forward.1 = (bf16[16,4,136,128]{3,2,1,0:T(8,128)(2,1)}, bf16[512,64]{1,0:T(8,128)(2,1)}, bf16[512,64]{1,0:T(8,128)(2,1)}, bf16[512,64]{1,0:T(8,128)(2,1)}) custom-call(bf16[16,16,2,32,128]{4,3,2,1,0:T(8,128)(2,1)} %all_to_all.21.x_ref, bf16[1,64,2048]{2,1,0:T(8,128)(2,1)} %wg_ref.1, bf16[1,64,2048]{2,1,0:T(8,128)(2,1)} %wu_ref.1, bf16[1,64,2048]{2,1,0:T(8,128)(2,1)} %wd_ref.1), custom_call_target="tpu_custom_call" | custom-call | flops 700000000 | bytes 7000000 | tf_op jit(solution)/shard_map/forward/pallas_call | solution.py:130
  100.3 28.4 %all_to_all.22.p_ref = bf16[16,4,136,128]{3,2,1,0:T(8,128)(2,1)} all-to-all(bf16[16,4,136,128]{3,2,1,0:T(8,128)(2,1)} %get-tuple-element.18), channel_id=1, replica_groups=mesh['z'=16,'c'=2,'y'=4,'x'=4] {'y','x'}, dimensions={0} | all-to-all | bytes 4456448 | tf_op jit(solution)/shard_map/all_to_all | solution.py:258
  128.7 3.7 %total.1 = bf16[16,40,128]{2,1,0:T(8,128)(2,1)} custom-call(bf16[16,4,136,128]{3,2,1,0:T(8,128)(2,1)} %all_to_all.22.p_ref), custom_call_target="tpu_custom_call" | custom-call | flops 10000000 | bytes 2000000 | tf_op jit(solution)/shard_map/total/pallas_call | solution.py:198
  132.4 29.7 %all_to_all.23.own_ref = bf16[16,40,128]{2,1,0:T(8,128)(2,1)S(1)} all-to-all(bf16[16,40,128]{2,1,0:T(8,128)(2,1)} %total.1), channel_id=1, replica_groups=mesh['z'=16,'c'=2,'y'=4,'x'=4] {'z'}, dimensions={0} | all-to-all | bytes 327680 | tf_op jit(solution)/shard_map/all_to_all | solution.py:258
  162.1 0.0 copy-start
  162.1 6.6 %collective-permute-start.1 = (bf16[16,24,128]{2,1,0:T(8,128)(2,1)S(1)}, bf16[16,24,128]{2,1,0:T(8,128)(2,1)S(1)}, u32[]{:S(2)}, u32[]{:S(2)}) collective-permute-start(bf16[16,24,128]{2,1,0:T(8,128)(2,1)S(1)} %slice.4), channel_id=1, source_target_pairs={{0,16},{16,0},{1,17},{17,1},{2,18},{18,2},{3,19},{19,3},{4,20},{20... | collective-permute-start | bytes 294920 | tf_op jit(solution)/shard_map/ppermute | solution.py:275
  168.7 5.0 %weights.1 = (f32[1,64,2048]{2,1,0:T(8,128)}, f32[1,64,2048]{2,1,0:T(8,128)}, f32[1,64,2048]{2,1,0:T(8,128)}) custom-call(bf16[16,16,2,32,128]{4,3,2,1,0:T(8,128)(2,1)} %all_to_all.21.x_ref, bf16[512,64]{1,0:T(8,128)(2,1)} %get-tuple-element.21.gg_ref, bf16[512,64]{1,0:T(8,128)(2,1)} %get-tuple-element.22.gu_ref, bf16[512,64]{1,0:T(8,128)(2,1)} %get-tuple-element.23.wt_ref), custom_call_target="tpu_custom_call" | custom-call | flops 4000000000 | bytes 6000000 | tf_op jit(solution)/shard_map/weights/pallas_call | solution.py:167
  173.7 0.0 copy-done
  173.7 0.0 collective-permute-done.1.other_ref
  173.7 0.0 copy-start.1
  173.7 0.6 copy-done.1
  174.3 2.8 %combine.1 = (bf16[128,128]{1,0:T(8,128)(2,1)}, f32[2,128]{1,0:T(2,128)}) custom-call(s32[2]{0:T(128)} %pad_add_fusion.s_ref, s32[2,128]{1,0:T(2,128)} %bitcast.12, bf16[2,128]{1,0:T(2,128)(2,1)} %bitcast.14, bf16[16,40,128]{2,1,0:T(8,128)(2,1)} %copy-done, bf16[16,24,128]{2,1,0:T(8,128)(2,1)} %copy-done.1), custom_call_target="tpu_custom_call" | custom-call | flops 100000000 | bytes 1000000 | tf_op jit(solution)/shard_map/combine/pallas_call | solution.py:238
  (2 shorter events, 0.0 us)
Async XLA Ops:
  3.8 9.9 %collective-permute-start = (bf16[16,2,16,128]{3,2,1,0:T(8,128)(2,1)}, bf16[16,2,16,128]{3,2,1,0:T(8,128)(2,1)S(1)}, u32[]{:S(2)}, u32[]{:S(2)}) collective-permute-start(bf16[16,2,16,128]{3,2,1,0:T(8,128)(2,1)} %get-tuple-element.17), channel_id=1, source_target_pairs={{0,16},{16,0},{1,17},{17,1},{2,18},{18,2},{3,19},{19,3},{4,20},{20... | collective-permute-start | bytes 393224 | tf_op jit(solution)/shard_map/ppermute | solution.py:267
  162.1 11.6 %copy-start = (bf16[16,40,128]{2,1,0:T(8,128)(2,1)}, bf16[16,40,128]{2,1,0:T(8,128)(2,1)S(1)}, u32[]{:S(2)}) copy-start(bf16[16,40,128]{2,1,0:T(8,128)(2,1)S(1)} %all_to_all.23.own_ref) | copy-start | bytes 491524
  162.1 11.6 %collective-permute-start.1 = (bf16[16,24,128]{2,1,0:T(8,128)(2,1)S(1)}, bf16[16,24,128]{2,1,0:T(8,128)(2,1)S(1)}, u32[]{:S(2)}, u32[]{:S(2)}) collective-permute-start(bf16[16,24,128]{2,1,0:T(8,128)(2,1)S(1)} %slice.4), channel_id=1, source_target_pairs={{0,16},{16,0},{1,17},{17,1},{2,18},{18,2},{3,19},{19,3},{4,20},{20... | collective-permute-start | bytes 294920 | tf_op jit(solution)/shard_map/ppermute | solution.py:275
  173.7 0.6 copy-start.1

commit v2 on v1

--- a/solution.py
+++ b/solution.py
@@ -1,5 +1,3 @@
-import functools
-
 import jax
 import jax.numpy as jnp
 from jax import lax
@@ -7,6 +5,7 @@
 from jax.experimental.pallas import tpu as pltpu
 from jax.sharding import Mesh
 from jax.sharding import PartitionSpec as P
+
 
 BF = jnp.bfloat16
 F32 = jnp.float32
@@ -91,105 +90,174 @@
     )(where, ids, w, tokens, cotangent)
 
 
-def forward_kernel(x_ref, wg_ref, wu_ref, wd_ref, part_ref, gg_ref, gu_ref, wt_ref, xt, xc):
+def forward_kernel(
+    s_ref, t_ref, c0_ref, c1_ref, c2_ref, c3_ref, wg_ref, wu_ref, wd_ref, g_ref, wt_ref, xt, xc, wgu, wdd
+):
+    @pl.when(pl.program_id(0) == 0)
+    def _():
+        wgu[:HID] = wg_ref[0]
+        wgu[HID:] = wu_ref[0]
+        wdd[:HID] = wd_ref[0]
+        wdd[HID:] = wd_ref[0]
+
     for j in range(TP):
-        xt[:, j * COL : (j + 1) * COL] = x_ref[j, :, 0].reshape(RB, COL)
-        xc[:, j * COL : (j + 1) * COL] = x_ref[j, :, 1].reshape(RB, COL)
-    wg, wu = wg_ref[0], wu_ref[0]
-    gate = dot(xt[...], wg, 1, 1)
-    up = dot(xt[...], wu, 1, 1)
-    back = dot(xc[...], wd_ref[0], 1, 1)
+        xt[:, j * COL : (j + 1) * COL] = t_ref[j].reshape(RB, COL)
+    for kx, c_ref in enumerate((c0_ref, c1_ref, c2_ref, c3_ref)):
+        for ky in range(4):
+            xc[:, piece_cols(s_ref, kx, ky)] = c_ref[ky].reshape(RB, COL)
+    pre = dot(xt[...], wgu[...], 1, 1)
+    back = dot(xc[...], wdd[...], 1, 1)
+    lane = iota((RB, COL), 1)
+    low_half = lane < HID
+    turned = pltpu.roll(pre, HID, 1)
+    gate = jnp.where(low_half, pre, turned)
+    up = jnp.where(low_half, turned, pre)
     sigma = 1.0 / (1.0 + jnp.exp(-gate))
     silu = gate * sigma
     hidden = silu * up
-    grad_gate = (back * up * sigma * (1.0 + gate * (1.0 - sigma))).astype(BF)
-    grad_up = (back * silu).astype(BF)
-    gg_ref[...] = grad_gate
-    gu_ref[...] = grad_up
-    wt_ref[...] = hidden.astype(BF)
-    total = jnp.sum(hidden * back, axis=1, keepdims=True)
-    lane = iota((RB, COL), 1)
+    grads = jnp.where(low_half, back * up * sigma * (1.0 + gate * (1.0 - sigma)), back * silu).astype(BF)
+    wt_ref[...] = hidden[:, :HID].astype(BF)
+    total = jnp.sum(jnp.where(low_half, hidden * back, 0.0), axis=1, keepdims=True)
     spread = jnp.where((lane & 31) == (iota((RB, COL), 0) & 31), total, 0.0)
     group = (iota((EXT, RB), 0) == (iota((EXT, RB), 1) >> 5)).astype(F32)
-    sums = dot(group, spread, 1, 0, lax.Precision.HIGHEST)
-    high = sums.astype(BF)
-    low = (sums - high.astype(F32)).astype(BF)
-    extra = jnp.where(iota((EXT, COL), 1) < 32, high.astype(F32), low.astype(F32)).astype(BF)
+    extra = two_parts(dot(group, spread, 1, 0, lax.Precision.HIGHEST))
+    for x in range(4):
+        g_ref[x, 0, :RB] = grads
+        g_ref[x, 0, RB:] = extra
+
+
+def two_parts(sums):
+    high = sums.astype(BF).astype(F32)
+    return jnp.where(iota((EXT, COL), 1) < 32, high, sums - high).astype(BF)
+
+
+def one_sum(parts):
+    both = parts + pltpu.roll(parts, COL - 32, 1)
+    low = iota((EXT, COL), 1) < 32
+    both = jnp.where(low, both, 0.0)
+    return both + pltpu.roll(both, 32, 1)
+
+
+def piece_cols(s_ref, kx, ky):
+    j = ((s_ref[2] - ky) & 3) * 4 + ((s_ref[3] - kx) & 3)
+    return pl.ds(pl.multiple_of(j * COL, COL), COL)
+
+
+def forward(where, t, cs, wg, wu, wd):
+    d = TP * COL
+    weight = pl.BlockSpec((1, HID, d), lambda i, s: (0, 0, 0))
+    return pl.pallas_call(
+        forward_kernel,
+        grid_spec=pltpu.PrefetchScalarGridSpec(
+            num_scalar_prefetch=1,
+            grid=(BLK,),
+            in_specs=[
+                pl.BlockSpec((TP, NZ // BLK, 2 * CAP, COL), lambda i, s: (0, i, 0, 0)),
+                *[pl.BlockSpec((4, NZ // BLK, 2 * CAP, COL), lambda i, s: (0, i, 0, 0))] * 4,
+                weight,
+                weight,
+                weight,
+            ],
+            out_specs=[
+                pl.BlockSpec((4, 1, RB + EXT, COL), lambda i, s: (0, i, 0, 0)),
+                pl.BlockSpec((RB, HID), lambda i, s: (i, 0)),
+            ],
+            scratch_shapes=[
+                pltpu.VMEM((RB, d), BF),
+                pltpu.VMEM((RB, d), BF),
+                pltpu.VMEM((2 * HID, d), BF),
+                pltpu.VMEM((2 * HID, d), BF),
+            ],
+        ),
+        out_shape=[
+            jax.ShapeDtypeStruct((4, BLK, RB + EXT, COL), BF),
+            jax.ShapeDtypeStruct((ROWS, HID), BF),
+        ],
+        name="forward",
+        cost_estimate=pl.CostEstimate(flops=10**9, bytes_accessed=5 * 10**6, transcendentals=10**5),
+    )(where, t, *cs, wg, wu, wd)
+
+
+def back_kernel(s_ref, g_ref, w_ref, out_ref, w):
+    @pl.when(pl.program_id(0) == 0)
+    def _():
+        for k in range(4):
+            rows = pl.ds(pl.multiple_of(((s_ref[3] - k) & 3) * COL, COL), COL)
+            for y in range(4):
+                w[rows, y * COL : (y + 1) * COL] = w_ref[k, y]
+
+    grads = jnp.concatenate([g_ref[x, 0, :RB] for x in range(4)], axis=1)
+    pieces = dot(grads, w[...], 1, 0).astype(BF)
+    parts = g_ref[0, 0, RB:].astype(F32)
+    for x in range(1, 4):
+        parts = parts + g_ref[x, 0, RB:].astype(F32)
+    extra = two_parts(one_sum(parts))
+    for y in range(4):
+        out_ref[y, 0, :RB] = pieces[:, y * COL : (y + 1) * COL]
+        out_ref[y, 0, RB:] = extra
+
+
+def back(where, g, w):
+    block = pl.BlockSpec((4, 1, RB + EXT, COL), lambda i, s: (0, i, 0, 0))
+    return pl.pallas_call(
+        back_kernel,
+        grid_spec=pltpu.PrefetchScalarGridSpec(
+            num_scalar_prefetch=1,
+            grid=(BLK,),
+            in_specs=[block, pl.BlockSpec((4, 4, 2 * HID, COL), lambda i, s: (0, 0, 0, 0))],
+            out_specs=block,
+            scratch_shapes=[pltpu.VMEM((4 * COL, 4 * COL), BF)],
+        ),
+        out_shape=jax.ShapeDtypeStruct((4, BLK, RB + EXT, COL), BF),
+        compiler_params=pltpu.CompilerParams(vmem_limit_bytes=8 * 2**20),
+        name="back",
+        cost_estimate=pl.CostEstimate(flops=3 * 10**8, bytes_accessed=10**6, transcendentals=0),
+    )(where, g, w)
+
+
+def weights_kernel(s_ref, t_ref, c0_ref, c1_ref, c2_ref, c3_ref, g_ref, wt_ref, dg_ref, du_ref, dd_ref):
+    grads = jnp.concatenate([g_ref[0, b, :RB] for b in range(BLK)], axis=0)
     for j in range(TP):
         cols = slice(j * COL, (j + 1) * COL)
-        piece = dot(grad_gate, wg[:, cols], 1, 0) + dot(grad_up, wu[:, cols], 1, 0)
-        part_ref[j, 0, :RB] = piece.astype(BF)
-        part_ref[j, 0, RB:] = extra
-
-
-def forward(x, wg, wu, wd):
+        both = dot(grads, t_ref[j].reshape(ROWS, COL), 0, 0)
+        dg_ref[0, :, cols] = both[:HID]
+        du_ref[0, :, cols] = both[HID:]
+    for kx, c_ref in enumerate((c0_ref, c1_ref, c2_ref, c3_ref)):
+        for ky in range(4):
+            dd_ref[0, :, piece_cols(s_ref, kx, ky)] = dot(
+                wt_ref[...], c_ref[ky].reshape(ROWS, COL), 0, 0
+            )
+
+
+def weights(where, t, cs, g, wt):
+    full = lambda *shape: pl.BlockSpec(shape, lambda i, s: (0,) * len(shape))
     d = TP * COL
-    weight = pl.BlockSpec((1, HID, d), lambda i: (0, 0, 0))
-    grads = pl.BlockSpec((RB, HID), lambda i: (i, 0))
-    gs = jax.ShapeDtypeStruct((ROWS, HID), BF)
-    return pl.pallas_call(
-        forward_kernel,
-        grid=(BLK,),
-        in_specs=[
-            pl.BlockSpec((TP, NZ // BLK, 2, 2 * CAP, COL), lambda i: (0, i, 0, 0, 0)),
-            weight,
-            weight,
-            weight,
-        ],
-        out_specs=[
-            pl.BlockSpec((TP, 1, RB + EXT, COL), lambda i: (0, i, 0, 0)),
-            grads,
-            grads,
-            grads,
-        ],
-        out_shape=[jax.ShapeDtypeStruct((TP, BLK, RB + EXT, COL), BF), gs, gs, gs],
-        scratch_shapes=[pltpu.VMEM((RB, d), BF), pltpu.VMEM((RB, d), BF)],
-        name="forward",
-        cost_estimate=pl.CostEstimate(flops=7 * 10**8, bytes_accessed=7 * 10**6, transcendentals=10**5),
-    )(x, wg, wu, wd)
-
-
-def weights_kernel(x_ref, gg_ref, gu_ref, wt_ref, dg_ref, du_ref, dd_ref):
-    gg, gu, wt = gg_ref[...], gu_ref[...], wt_ref[...]
-    for j in range(x_ref.shape[0]):
-        cols = slice(j * COL, (j + 1) * COL)
-        rows = x_ref[j, :, 0].reshape(ROWS, COL)
-        cots = x_ref[j, :, 1].reshape(ROWS, COL)
-        dg_ref[0, :, cols] = dot(gg, rows, 0, 0)
-        du_ref[0, :, cols] = dot(gu, rows, 0, 0)
-        dd_ref[0, :, cols] = dot(wt, cots, 0, 0)
-
-
-def weights(x, gg, gu, wt):
-    d, pieces = TP * COL, 4
     out = jax.ShapeDtypeStruct((1, HID, d), F32)
-    grads = pl.BlockSpec((ROWS, HID), lambda i: (0, 0))
     return pl.pallas_call(
         weights_kernel,
-        grid=(TP // pieces,),
-        in_specs=[
-            pl.BlockSpec((pieces, NZ, 2, 2 * CAP, COL), lambda i: (i, 0, 0, 0, 0)),
-            grads,
-            grads,
-            grads,
-        ],
-        out_specs=[pl.BlockSpec((1, HID, pieces * COL), lambda i: (0, 0, i))] * 3,
+        grid_spec=pltpu.PrefetchScalarGridSpec(
+            num_scalar_prefetch=1,
+            grid=(1,),
+            in_specs=[
+                full(TP, NZ, 2 * CAP, COL),
+                *[full(4, NZ, 2 * CAP, COL)] * 4,
+                full(1, BLK, RB + EXT, COL),
+                full(ROWS, HID),
+            ],
+            out_specs=[full(1, HID, d)] * 3,
+        ),
         out_shape=[out, out, out],
         name="weights",
         cost_estimate=pl.CostEstimate(flops=4 * 10**9, bytes_accessed=6 * 10**6, transcendentals=0),
-    )(x, gg, gu, wt)
+    )(where, t, *cs, g, wt)
 
 
 def total_kernel(p_ref, out_ref):
     rows = p_ref[0, 0].astype(F32)
-    for j in range(1, TP):
-        rows = rows + p_ref[j, 0].astype(F32)
+    for y in range(1, 4):
+        rows = rows + p_ref[y, 0].astype(F32)
     out_ref[:, : 2 * CAP] = rows[:RB].astype(BF).reshape(NZ // BLK, 2 * CAP, COL)
-    sums = rows[RB:]
-    sums = sums + pltpu.roll(sums, COL - 32, 1)
-    high = sums.astype(BF).astype(F32)
-    low = pltpu.roll(sums - high, 32, 1)
-    extra = jnp.where(iota((EXT, COL), 1) < 32, high, low)
+    extra = two_parts(one_sum(rows[RB:])).astype(F32)
     for k in range(NZ // BLK):
         out_ref[k, 2 * CAP :] = jnp.broadcast_to(extra[k : k + 1], (EXT, COL)).astype(BF)
 
@@ -198,9 +266,10 @@
     return pl.pallas_call(
         total_kernel,
         grid=(BLK,),
-        in_specs=[pl.BlockSpec((TP, 1, RB + EXT, COL), lambda i: (0, i, 0, 0))],
+        in_specs=[pl.BlockSpec((4, 1, RB + EXT, COL), lambda i: (0, i, 0, 0))],
         out_specs=pl.BlockSpec((NZ // BLK, 2 * CAP + EXT, COL), lambda i: (i, 0, 0)),
         out_shape=jax.ShapeDtypeStruct((NZ, 2 * CAP + EXT, COL), BF),
+        compiler_params=pltpu.CompilerParams(vmem_limit_bytes=4 * 2**20),
         name="total",
         cost_estimate=pl.CostEstimate(flops=10**7, bytes_accessed=2 * 10**6, transcendentals=0),
     )(part)
@@ -249,6 +318,7 @@
             out_specs=[full(TOK, COL), full(2, TOK)],
         ),
         out_shape=[jax.ShapeDtypeStruct((TOK, COL), BF), jax.ShapeDtypeStruct((2, TOK), F32)],
+        compiler_params=pltpu.CompilerParams(vmem_limit_bytes=4 * 2**20),
         name="combine",
         cost_estimate=pl.CostEstimate(flops=10**8, bytes_accessed=10**6, transcendentals=0),
     )(where, ids, w, own, other)
@@ -258,22 +328,46 @@
     return lax.all_to_all(x, axis, split_axis=0, concat_axis=0, tiled=True)
 
 
+def copies(x, n):
+    return jnp.broadcast_to(x[None], (n, *x.shape))
+
+
+def shifted(x, axis, by):
+    n = lax.axis_size(axis)
+    return lax.ppermute(x, axis, [(i, (i + by) % n) for i in range(n)])
+
+
+def row_weights(gate_weight, up_weight, x):
+    both = jnp.concatenate([gate_weight[0], up_weight[0]], axis=0)
+    blocks = both.reshape(2 * HID, 4, 4, COL).transpose(2, 1, 0, 3)
+    own = [lax.dynamic_index_in_dim(blocks, (x + k) & 3, 0, keepdims=False) for k in range(4)]
+    moved = [shifted(own[k], "x", k) for k in range(1, 4)]
+    return jnp.stack([own[0]] + moved)
+
+
 def per_device(tokens, cotangent, expert_ids, route_weight, gate_weight, up_weight, down_weight):
-    swap = [(0, 1), (1, 0)]
-    tp = lax.axis_index("y") * lax.axis_size("x") + lax.axis_index("x")
-    where = jnp.stack([tp, lax.axis_index("c")]).astype(I32)
+    y, x, core = lax.axis_index("y"), lax.axis_index("x"), lax.axis_index("c")
+    where = jnp.stack([y * 4 + x, core, y, x]).astype(I32)
     ids, w = expert_ids.T, route_weight.T
     own, other = dispatch(where, ids, w, tokens, cotangent)
-    got = lax.ppermute(other, "c", swap)
+    got = shifted(other, "c", 1)
     mine = jnp.stack([own, got], axis=2).reshape(NZ, 2, 2 * CAP, COL)
     mine = exchange(mine, "z")
-    gathered = exchange(jnp.broadcast_to(mine[None], (TP, *mine.shape)), ("y", "x"))
-    part, gg, gu, wt = forward(gathered, gate_weight, up_weight, down_weight)
-    parts = exchange(part, ("y", "x"))
-    gate_grad, up_grad, down_grad = weights(gathered, gg, gu, wt)
-    back = exchange(total(parts), "z")
-    far = lax.ppermute(back[:, CAP:], "c", swap)
-    tokens_grad, route_grad = combine(where, ids, w, back, far)
+    row_w = row_weights(gate_weight, up_weight, x)
+    tok, cot = mine[:, 0], mine[:, 1]
+    tok_row = exchange(copies(tok, 4), "x")
+    cot_moved = [shifted(cot, "y", k) for k in range(1, 4)]
+    cot_col = jnp.stack([cot] + cot_moved)
+    tok_all = exchange(copies(tok_row, 4), "y").reshape(TP, NZ, 2 * CAP, COL)
+    cot_all = [cot_col] + [shifted(cot_col, "x", k) for k in range(1, 4)]
+    g, wt = forward(where, tok_all, cot_all, gate_weight, up_weight, down_weight)
+    g_all = exchange(g, "x")
+    part = back(where, g_all, row_w)
+    sums = exchange(part, "y")
+    gate_grad, up_grad, down_grad = weights(where, tok_all, cot_all, g, wt)
+    home = exchange(total(sums), "z")
+    far = shifted(home[:, CAP:], "c", 1)
+    tokens_grad, route_grad = combine(where, ids, w, home, far)
     return tokens_grad, route_grad.T, gate_grad, up_grad, down_grad
 
 

time: 178 us -> 194 us (1.090)
  blocking collectives: 135 us -> 76.9 us
  starting transfers between devices: 15.4 us -> 54.6 us
  waiting for transfers between devices: 1.18 us -> 34.5 us
  local copies, waits for them, and re-layouts: 1.71 us -> 5.48 us
  Pallas kernels: 22 us -> 18.7 us
    all_to_all x4, blocking collectives: 135 us -> 76.9 us  [exchange(): return lax.all_to_all(x, axis, split_axis=0, concat_axis=0, tiled=True)]
    ppermute x2 -> x11, waiting for transfers between devices: 1.18 us -> 34.5 us  [shifted(): return lax.ppermute(x, axis, [(i, (i + by) % n) for i in range(n)])]
    ppermute x2 -> x11, starting transfers between devices: 15.4 us -> 45.5 us  [shifted(): return lax.ppermute(x, axis, [(i, (i + by) % n) for i in range(n)])]
    all_to_all x0 -> x2, starting transfers between devices: none -> 9.11 us  [exchange(): return lax.all_to_all(x, axis, split_axis=0, concat_axis=0, tiled=True)]
    pallas_call x3 -> x4, Pallas kernels: 16.5 us -> 14.4 us  [the longest x1 6.91 us: forward(): pl.pallas_call(forward_kernel, grid_spec=pltpu.PrefetchScalarGridSpec(num...]
  transfers between devices with their start and end apart: 2 -> 13, of which waited for: 1 -> 8; matrix products, arithmetic and copies ran while one was open for 0% -> 1% of each run, Pallas kernels for 3% -> 3%
where the time goes in v2:
time: 194 us; the launch traced here: 193 us
  blocking collectives  76.9 us (40%)
  starting transfers between devices  54.6 us (28%)
  waiting for transfers between devices  34.5 us (18%)
  Pallas kernels  18.7 us (10%)
  local copies, waits for them, and re-layouts  5.48 us (3%)
    all_to_all x4, blocking collectives, exchange(): return lax.all_to_all(x, axis, split_axis=0, concat_axis=0, tiled=True)  76.9 us
    ppermute x11, starting transfers between devices, shifted(): return lax.ppermute(x, axis, [(i, (i + by) % n) for i in range(n)])  45.5 us
    ppermute x11, waiting for transfers between devices, shifted(): return lax.ppermute(x, axis, [(i, (i + by) % n) for i in range(n)])  34.5 us
    all_to_all x2, starting transfers between devices, exchange(): return lax.all_to_all(x, axis, split_axis=0, concat_axis=0, tiled=True)  9.11 us
    pallas_call x1, Pallas kernels, forward(): pl.pallas_call(forward_kernel, grid_spec=pltpu.PrefetchScalarGridSpec(num...  6.91 us
    pallas_call x1, Pallas kernels, weights(): pl.pallas_call(weights_kernel, grid_spec=pltpu.PrefetchScalarGridSpec(num...  5.02 us
  transfers between devices with their start and end apart: 13, of which 8 were waited for; matrix products, arithmetic and copies ran while one was open for 1% of the time, Pallas kernels for 3%

profile of v2, /device:TPU:1, one launch (start us, length us, event | category | flops | bytes accessed | tf_op | source)
XLA Modules:
  0.0 192.8 jit_solution(14823511388322058974)
XLA Ops:
  0.6 0.7 pad_add_fusion.s_ref
  1.3 2.6 %dispatch.1 = (bf16[16,2,16,128]{3,2,1,0:T(8,128)(2,1)}, bf16[16,2,16,128]{3,2,1,0:T(8,128)(2,1)}) custom-call(s32[4]{0:T(128)} %pad_add_fusion.s_ref, s32[2,128]{1,0:T(2,128)} %bitcast.40, bf16[2,128]{1,0:T(2,128)(2,1)} %bitcast.42, bf16[128,2048]{1,0:T(8,128)(2,1)} %tok_ref.1, bf16[128,2048]{1,0:T(8,128)(2,1)} %cot_ref.1), custom_call_target="tpu_custom_call" | custom-call | flops 100000000 | bytes 1000000 | tf_op jit(solution)/shard_map/dispatch/pallas_call | solution.py:74
  3.9 8.7 %collective-permute-start = (bf16[16,2,16,128]{3,2,1,0:T(8,128)(2,1)}, bf16[16,2,16,128]{3,2,1,0:T(8,128)(2,1)S(1)}, u32[]{:S(2)}, u32[]{:S(2)}) collective-permute-start(bf16[16,2,16,128]{3,2,1,0:T(8,128)(2,1)} %get-tuple-element.15), channel_id=1, source_target_pairs={{0,16},{16,0},{1,17},{17,1},{2,18},{18,2},{3,19},{19,3},{4,20},{20... | collective-permute-start | bytes 393224 | tf_op jit(solution)/shard_map/ppermute | solution.py:337
  12.6 1.2 collective-permute-done
  13.8 0.9 pad_maximum_fusion.2
  14.8 23.4 %all_to_all.30 = bf16[16,2,32,128]{3,2,1,0:T(8,128)(2,1)S(1)} all-to-all(bf16[16,2,32,128]{3,2,1,0:T(8,128)(2,1)S(1)} %bitcast.46), channel_id=1, replica_groups=mesh['z'=16,'c'=2,'y'=4,'x'=4] {'z'}, dimensions={0} | all-to-all | bytes 524288 | tf_op jit(solution)/shard_map/all_to_all | solution.py:328
  38.2 0.1 broadcast_in_dim.14
  38.3 10.7 %all_to_all.31 = bf16[4,16,32,128]{3,2,1,0:T(8,128)(2,1)S(1)} all-to-all(bf16[4,16,32,128]{3,2,1,0:T(8,128)(2,1)S(1)} %broadcast_in_dim.14), channel_id=1, replica_groups=mesh['z'=16,'c'=2,'y'=4,'x'=4] {'x'}, dimensions={0} | all-to-all | bytes 1048576 | tf_op jit(solution)/shard_map/all_to_all | solution.py:328
  49.1 1.8 broadcast_in_dim.15
  50.8 4.3 %all-to-all-start.2 = ((bf16[4,4,16,32,128]{4,3,2,1,0:T(8,128)(2,1)}), bf16[4,4,16,32,128]{4,3,2,1,0:T(8,128)(2,1)S(1)}, u32[]{:S(2)}, u32[]{:S(2)}) async-start(bf16[4,4,16,32,128]{4,3,2,1,0:T(8,128)(2,1)} %broadcast_in_dim.15), calls=%async_computation.2 | async-start | bytes 4194304 | tf_op jit(solution)/shard_map/all_to_all | solution.py:328
  55.1 3.4 %collective-permute-start.1 = (bf16[16,32,128]{2,1,0:T(8,128)(2,1)S(1)}, bf16[16,32,128]{2,1,0:T(8,128)(2,1)S(1)}, u32[]{:S(2)}, u32[]{:S(2)}) collective-permute-start(bf16[16,32,128]{2,1,0:T(8,128)(2,1)S(1)} %get-tuple-element.28), channel_id=1, source_target_pairs={{0,4},{4,8},{8,12},{12,0},{1,5},{5,9},{9,13},{13,1},{2,6},{6,10},{... | collective-permute-start | bytes 393224 | tf_op jit(solution)/shard_map/ppermute | solution.py:337
  58.5 4.3 %collective-permute-start.2 = (bf16[16,32,128]{2,1,0:T(8,128)(2,1)S(1)}, bf16[16,32,128]{2,1,0:T(8,128)(2,1)S(1)}, u32[]{:S(2)}, u32[]{:S(2)}) collective-permute-start(bf16[16,32,128]{2,1,0:T(8,128)(2,1)S(1)} %get-tuple-element.28), channel_id=1, source_target_pairs={{0,8},{4,12},{8,0},{12,4},{1,9},{5,13},{9,1},{13,5},{2,10},{6,14},... | collective-permute-start | bytes 393224 | tf_op jit(solution)/shard_map/ppermute | solution.py:337
  62.8 3.1 %collective-permute-start.3 = (bf16[16,32,128]{2,1,0:T(8,128)(2,1)S(1)}, bf16[16,32,128]{2,1,0:T(8,128)(2,1)S(1)}, u32[]{:S(2)}, u32[]{:S(2)}) collective-permute-start(bf16[16,32,128]{2,1,0:T(8,128)(2,1)S(1)} %get-tuple-element.28), channel_id=1, source_target_pairs={{0,12},{4,0},{8,4},{12,8},{1,13},{5,1},{9,5},{13,9},{2,14},{6,2},{... | collective-permute-start | bytes 393224 | tf_op jit(solution)/shard_map/ppermute | solution.py:337
  65.9 8.3 %collective-permute-done.1 = bf16[16,32,128]{2,1,0:T(8,128)(2,1)S(1)} collective-permute-done((bf16[16,32,128]{2,1,0:T(8,128)(2,1)S(1)}, bf16[16,32,128]{2,1,0:T(8,128)(2,1)S(1)}, u32[]{:S(2)}, u32[]{:S(2)}) %collective-permute-start.1) | collective-permute-done | bytes 131104 | tf_op jit(solution)/shard_map/ppermute | solution.py:337
  74.2 6.3 %collective-permute-done.2 = bf16[16,32,128]{2,1,0:T(8,128)(2,1)S(1)} collective-permute-done((bf16[16,32,128]{2,1,0:T(8,128)(2,1)S(1)}, bf16[16,32,128]{2,1,0:T(8,128)(2,1)S(1)}, u32[]{:S(2)}, u32[]{:S(2)}) %collective-permute-start.2) | collective-permute-done | bytes 131104 | tf_op jit(solution)/shard_map/ppermute | solution.py:337
  80.5 0.0 collective-permute-done.3
  80.5 0.1 pad_maximum_fusion.c0_ref
  80.6 2.2 %collective-permute-start.4 = (bf16[4,16,32,128]{3,2,1,0:T(8,128)(2,1)S(1)}, bf16[4,16,32,128]{3,2,1,0:T(8,128)(2,1)}, u32[]{:S(2)}, u32[]{:S(2)}) collective-permute-start(bf16[4,16,32,128]{3,2,1,0:T(8,128)(2,1)S(1)} %pad_maximum_fusion.c0_ref), channel_id=1, source_target_pairs={{0,1},{1,2},{2,3},{3,0},{4,5},{5,6},{6,7},{7,4},{8,9},{9,10},{10,1... | collective-permute-start | bytes 1572872 | tf_op jit(solution)/shard_map/ppermute | solution.py:337
  82.8 3.7 %collective-permute-start.5 = (bf16[4,16,32,128]{3,2,1,0:T(8,128)(2,1)S(1)}, bf16[4,16,32,128]{3,2,1,0:T(8,128)(2,1)}, u32[]{:S(2)}, u32[]{:S(2)}) collective-permute-start(bf16[4,16,32,128]{3,2,1,0:T(8,128)(2,1)S(1)} %pad_maximum_fusion.c0_ref), channel_id=1, source_target_pairs={{0,2},{1,3},{2,0},{3,1},{4,6},{5,7},{6,4},{7,5},{8,10},{9,11},{10,... | collective-permute-start | bytes 1572872 | tf_op jit(solution)/shard_map/ppermute | solution.py:337
  86.5 2.5 %collective-permute-start.6 = (bf16[4,16,32,128]{3,2,1,0:T(8,128)(2,1)S(1)}, bf16[4,16,32,128]{3,2,1,0:T(8,128)(2,1)}, u32[]{:S(2)}, u32[]{:S(2)}) collective-permute-start(bf16[4,16,32,128]{3,2,1,0:T(8,128)(2,1)S(1)} %pad_maximum_fusion.c0_ref), channel_id=1, source_target_pairs={{0,3},{1,0},{2,1},{3,2},{4,7},{5,4},{6,5},{7,6},{8,11},{9,8},{10,9... | collective-permute-start | bytes 1572872 | tf_op jit(solution)/shard_map/ppermute | solution.py:337
  89.0 0.9 concatenate.8
  89.9 0.2 concatenate.9
  90.1 1.0 copy_dynamic-update-slice_fusion.1
  91.1 4.5 %collective-permute-done.4.c1_ref = bf16[4,16,32,128]{3,2,1,0:T(8,128)(2,1)} collective-permute-done((bf16[4,16,32,128]{3,2,1,0:T(8,128)(2,1)S(1)}, bf16[4,16,32,128]{3,2,1,0:T(8,128)(2,1)}, u32[]{:S(2)}, u32[]{:S(2)}) %collective-permute-start.4) | collective-permute-done | bytes 524320 | tf_op jit(solution)/shard_map/ppermute | solution.py:337
  95.6 4.4 %collective-permute-done.5.c2_ref = bf16[4,16,32,128]{3,2,1,0:T(8,128)(2,1)} collective-permute-done((bf16[4,16,32,128]{3,2,1,0:T(8,128)(2,1)S(1)}, bf16[4,16,32,128]{3,2,1,0:T(8,128)(2,1)}, u32[]{:S(2)}, u32[]{:S(2)}) %collective-permute-start.5) | collective-permute-done | bytes 524320 | tf_op jit(solution)/shard_map/ppermute | solution.py:337
  100.0 6.6 %collective-permute-done.6.c3_ref = bf16[4,16,32,128]{3,2,1,0:T(8,128)(2,1)} collective-permute-done((bf16[4,16,32,128]{3,2,1,0:T(8,128)(2,1)S(1)}, bf16[4,16,32,128]{3,2,1,0:T(8,128)(2,1)}, u32[]{:S(2)}, u32[]{:S(2)}) %collective-permute-start.6) | collective-permute-done | bytes 524320 | tf_op jit(solution)/shard_map/ppermute | solution.py:337
  106.6 0.0 all-to-all-done.2
  106.6 1.3 copy-done.4
  108.0 6.9 %forward.1 = (bf16[4,4,136,128]{3,2,1,0:T(8,128)(2,1)}, bf16[512,64]{1,0:T(8,128)(2,1)}) custom-call(s32[4]{0:T(128)} %pad_add_fusion.s_ref, bf16[16,16,32,128]{3,2,1,0:T(8,128)(2,1)} %bitcast.44, bf16[4,16,32,128]{3,2,1,0:T(8,128)(2,1)} %copy-done.5, bf16[4,16,32,128]{3,2,1,0:T(8,128)(2,1)} %collective-permute-done.4.c1_ref, ...), custom_call_target="tpu_custom_call" | custom-call | flops 1000000000 | bytes 5000000 | tf_op jit(solution)/shard_map/forward/pallas_call | solution.py:149
  114.9 4.8 %all-to-all-start.3 = ((bf16[4,4,136,128]{3,2,1,0:T(8,128)(2,1)}), bf16[4,4,136,128]{3,2,1,0:T(8,128)(2,1)S(1)}, u32[]{:S(2)}, u32[]{:S(2)}) async-start(bf16[4,4,136,128]{3,2,1,0:T(8,128)(2,1)} %get-tuple-element.16.g_ref), calls=%async_computation.3 | async-start | bytes 1114112 | tf_op jit(solution)/shard_map/all_to_all | solution.py:328
  119.7 0.1 copy_dynamic-update-slice_fusion
  119.8 3.4 %collective-permute-start.7 = (bf16[4,128,128]{2,1,0:T(8,128)(2,1)S(1)}, bf16[4,128,128]{2,1,0:T(8,128)(2,1)S(1)}, u32[]{:S(2)}, u32[]{:S(2)}) collective-permute-start(bf16[4,128,128]{2,1,0:T(8,128)(2,1)S(1)} %get-tuple-element.26), channel_id=1, source_target_pairs={{0,1},{1,2},{2,3},{3,0},{4,5},{5,6},{6,7},{7,4},{8,9},{9,10},{10,1... | collective-permute-start | bytes 393224 | tf_op jit(solution)/shard_map/ppermute | solution.py:337
  123.2 4.3 %collective-permute-start.8 = (bf16[4,128,128]{2,1,0:T(8,128)(2,1)S(1)}, bf16[4,128,128]{2,1,0:T(8,128)(2,1)S(1)}, u32[]{:S(2)}, u32[]{:S(2)}) collective-permute-start(bf16[4,128,128]{2,1,0:T(8,128)(2,1)S(1)} %get-tuple-element.25), channel_id=1, source_target_pairs={{0,2},{1,3},{2,0},{3,1},{4,6},{5,7},{6,4},{7,5},{8,10},{9,11},{10,... | collective-permute-start | bytes 393224 | tf_op jit(solution)/shard_map/ppermute | solution.py:337
  127.5 3.1 %collective-permute-start.9 = (bf16[4,128,128]{2,1,0:T(8,128)(2,1)S(1)}, bf16[4,128,128]{2,1,0:T(8,128)(2,1)S(1)}, u32[]{:S(2)}, u32[]{:S(2)}) collective-permute-start(bf16[4,128,128]{2,1,0:T(8,128)(2,1)S(1)} %get-tuple-element.24), channel_id=1, source_target_pairs={{0,3},{1,0},{2,1},{3,2},{4,7},{5,4},{6,5},{7,6},{8,11},{9,8},{10,9... | collective-permute-start | bytes 393224 | tf_op jit(solution)/shard_map/ppermute | solution.py:337
  130.6 0.0 collective-permute-done.7
  130.6 1.5 collective-permute-done.8
  132.1 1.7 collective-permute-done.9
  133.8 0.1 pad_maximum_fusion.1.w_ref
  133.9 0.0 all-to-all-done.3.g_ref
  133.9 1.8 back.1
  135.7 9.5 %all_to_all.32.p_ref = bf16[4,4,136,128]{3,2,1,0:T(8,128)(2,1)S(1)} all-to-all(bf16[4,4,136,128]{3,2,1,0:T(8,128)(2,1)S(1)} %back.1), channel_id=1, replica_groups=mesh['z'=16,'c'=2,'y'=4,'x'=4] {'y'}, dimensions={0} | all-to-all | bytes 1114112 | tf_op jit(solution)/shard_map/all_to_all | solution.py:328
  145.2 0.7 total.1
  145.8 33.2 %all_to_all.33.own_ref = bf16[16,40,128]{2,1,0:T(8,128)(2,1)S(1)} all-to-all(bf16[16,40,128]{2,1,0:T(8,128)(2,1)S(1)} %total.1), channel_id=1, replica_groups=mesh['z'=16,'c'=2,'y'=4,'x'=4] {'z'}, dimensions={0} | all-to-all | bytes 327680 | tf_op jit(solution)/shard_map/all_to_all | solution.py:328
  179.1 6.9 %collective-permute-start.10 = (bf16[16,24,128]{2,1,0:T(8,128)(2,1)S(1)}, bf16[16,24,128]{2,1,0:T(8,128)(2,1)S(1)}, u32[]{:S(2)}, u32[]{:S(2)}) collective-permute-start(bf16[16,24,128]{2,1,0:T(8,128)(2,1)S(1)} %slice.14), channel_id=1, source_target_pairs={{0,16},{16,0},{1,17},{17,1},{2,18},{18,2},{3,19},{19,3},{4,20},{20... | collective-permute-start | bytes 294920 | tf_op jit(solution)/shard_map/ppermute | solution.py:337
  186.0 0.0 copy-start.2
  186.0 0.0 copy-start.3
  186.0 5.0 %weights.1 = (f32[1,64,2048]{2,1,0:T(8,128)}, f32[1,64,2048]{2,1,0:T(8,128)}, f32[1,64,2048]{2,1,0:T(8,128)}) custom-call(s32[4]{0:T(128)} %pad_add_fusion.s_ref, bf16[16,16,32,128]{3,2,1,0:T(8,128)(2,1)} %bitcast.45, bf16[4,16,32,128]{3,2,1,0:T(8,128)(2,1)} %copy-done.5, bf16[4,16,32,128]{3,2,1,0:T(8,128)(2,1)} %collective-permute-done.4.c1_ref, ...), custom_call_target="tpu_custom_call" | custom-call | flops 4000000000 | bytes 6000000 | tf_op jit(solution)/shard_map/weights/pallas_call | solution.py:236
  191.0 1.7 combine.1
  (18 shorter events, 0.1 us)
Async XLA Ops:
  3.9 9.9 %collective-permute-start = (bf16[16,2,16,128]{3,2,1,0:T(8,128)(2,1)}, bf16[16,2,16,128]{3,2,1,0:T(8,128)(2,1)S(1)}, u32[]{:S(2)}, u32[]{:S(2)}) collective-permute-start(bf16[16,2,16,128]{3,2,1,0:T(8,128)(2,1)} %get-tuple-element.15), channel_id=1, source_target_pairs={{0,16},{16,0},{1,17},{17,1},{2,18},{18,2},{3,19},{19,3},{4,20},{20... | collective-permute-start | bytes 393224 | tf_op jit(solution)/shard_map/ppermute | solution.py:337
  50.8 38.2 %copy-start.6 = (bf16[1,64,2048]{2,1,0:T(8,128)(2,1)S(1)}, bf16[1,64,2048]{2,1,0:T(8,128)(2,1)}, u32[]{:S(2)}) copy-start(bf16[1,64,2048]{2,1,0:T(8,128)(2,1)} %wg_ref.1) | copy-start | bytes 786436
  50.8 39.1 %copy-start.7 = (bf16[1,64,2048]{2,1,0:T(8,128)(2,1)S(1)}, bf16[1,64,2048]{2,1,0:T(8,128)(2,1)}, u32[]{:S(2)}) copy-start(bf16[1,64,2048]{2,1,0:T(8,128)(2,1)} %wu_ref.1) | copy-start | bytes 786436
  50.8 55.8 %all-to-all-start.2 = ((bf16[4,4,16,32,128]{4,3,2,1,0:T(8,128)(2,1)}), bf16[4,4,16,32,128]{4,3,2,1,0:T(8,128)(2,1)S(1)}, u32[]{:S(2)}, u32[]{:S(2)}) async-start(bf16[4,4,16,32,128]{4,3,2,1,0:T(8,128)(2,1)} %broadcast_in_dim.15), calls=%async_computation.2 | async-start | bytes 4194304 | tf_op jit(solution)/shard_map/all_to_all | solution.py:328
  55.1 19.1 %collective-permute-start.1 = (bf16[16,32,128]{2,1,0:T(8,128)(2,1)S(1)}, bf16[16,32,128]{2,1,0:T(8,128)(2,1)S(1)}, u32[]{:S(2)}, u32[]{:S(2)}) collective-permute-start(bf16[16,32,128]{2,1,0:T(8,128)(2,1)S(1)} %get-tuple-element.28), channel_id=1, source_target_pairs={{0,4},{4,8},{8,12},{12,0},{1,5},{5,9},{9,13},{13,1},{2,6},{6,10},{... | collective-permute-start | bytes 393224 | tf_op jit(solution)/shard_map/ppermute | solution.py:337
  58.5 22.0 %collective-permute-start.2 = (bf16[16,32,128]{2,1,0:T(8,128)(2,1)S(1)}, bf16[16,32,128]{2,1,0:T(8,128)(2,1)S(1)}, u32[]{:S(2)}, u32[]{:S(2)}) collective-permute-start(bf16[16,32,128]{2,1,0:T(8,128)(2,1)S(1)} %get-tuple-element.28), channel_id=1, source_target_pairs={{0,8},{4,12},{8,0},{12,4},{1,9},{5,13},{9,1},{13,5},{2,10},{6,14},... | collective-permute-start | bytes 393224 | tf_op jit(solution)/shard_map/ppermute | solution.py:337
  62.8 17.7 %collective-permute-start.3 = (bf16[16,32,128]{2,1,0:T(8,128)(2,1)S(1)}, bf16[16,32,128]{2,1,0:T(8,128)(2,1)S(1)}, u32[]{:S(2)}, u32[]{:S(2)}) collective-permute-start(bf16[16,32,128]{2,1,0:T(8,128)(2,1)S(1)} %get-tuple-element.28), channel_id=1, source_target_pairs={{0,12},{4,0},{8,4},{12,8},{1,13},{5,1},{9,5},{13,9},{2,14},{6,2},{... | collective-permute-start | bytes 393224 | tf_op jit(solution)/shard_map/ppermute | solution.py:337
  80.6 26.1 %copy-start.5 = (bf16[4,16,32,128]{3,2,1,0:T(8,128)(2,1)}, bf16[4,16,32,128]{3,2,1,0:T(8,128)(2,1)S(1)}, u32[]{:S(2)}) copy-start(bf16[4,16,32,128]{3,2,1,0:T(8,128)(2,1)S(1)} %pad_maximum_fusion.c0_ref) | copy-start | bytes 1572868
  80.6 15.1 %collective-permute-start.4 = (bf16[4,16,32,128]{3,2,1,0:T(8,128)(2,1)S(1)}, bf16[4,16,32,128]{3,2,1,0:T(8,128)(2,1)}, u32[]{:S(2)}, u32[]{:S(2)}) collective-permute-start(bf16[4,16,32,128]{3,2,1,0:T(8,128)(2,1)S(1)} %pad_maximum_fusion.c0_ref), channel_id=1, source_target_pairs={{0,1},{1,2},{2,3},{3,0},{4,5},{5,6},{6,7},{7,4},{8,9},{9,10},{10,1... | collective-permute-start | bytes 1572872 | tf_op jit(solution)/shard_map/ppermute | solution.py:337
  82.8 17.3 %collective-permute-start.5 = (bf16[4,16,32,128]{3,2,1,0:T(8,128)(2,1)S(1)}, bf16[4,16,32,128]{3,2,1,0:T(8,128)(2,1)}, u32[]{:S(2)}, u32[]{:S(2)}) collective-permute-start(bf16[4,16,32,128]{3,2,1,0:T(8,128)(2,1)S(1)} %pad_maximum_fusion.c0_ref), channel_id=1, source_target_pairs={{0,2},{1,3},{2,0},{3,1},{4,6},{5,7},{6,4},{7,5},{8,10},{9,11},{10,... | collective-permute-start | bytes 1572872 | tf_op jit(solution)/shard_map/ppermute | solution.py:337
  86.5 20.2 %collective-permute-start.6 = (bf16[4,16,32,128]{3,2,1,0:T(8,128)(2,1)S(1)}, bf16[4,16,32,128]{3,2,1,0:T(8,128)(2,1)}, u32[]{:S(2)}, u32[]{:S(2)}) collective-permute-start(bf16[4,16,32,128]{3,2,1,0:T(8,128)(2,1)S(1)} %pad_maximum_fusion.c0_ref), channel_id=1, source_target_pairs={{0,3},{1,0},{2,1},{3,2},{4,7},{5,4},{6,5},{7,6},{8,11},{9,8},{10,9... | collective-permute-start | bytes 1572872 | tf_op jit(solution)/shard_map/ppermute | solution.py:337
  106.6 1.3 copy-start.4
  114.9 19.0 %copy-start = (s32[4]{0:T(128)S(1)}, s32[4]{0:T(128)}, u32[]{:S(2)}) copy-start(s32[4]{0:T(128)} %pad_add_fusion.s_ref) | copy-start | bytes 52
  114.9 19.0 %all-to-all-start.3 = ((bf16[4,4,136,128]{3,2,1,0:T(8,128)(2,1)}), bf16[4,4,136,128]{3,2,1,0:T(8,128)(2,1)S(1)}, u32[]{:S(2)}, u32[]{:S(2)}) async-start(bf16[4,4,136,128]{3,2,1,0:T(8,128)(2,1)} %get-tuple-element.16.g_ref), calls=%async_computation.3 | async-start | bytes 1114112 | tf_op jit(solution)/shard_map/all_to_all | solution.py:328
  119.8 10.8 %collective-permute-start.7 = (bf16[4,128,128]{2,1,0:T(8,128)(2,1)S(1)}, bf16[4,128,128]{2,1,0:T(8,128)(2,1)S(1)}, u32[]{:S(2)}, u32[]{:S(2)}) collective-permute-start(bf16[4,128,128]{2,1,0:T(8,128)(2,1)S(1)} %get-tuple-element.26), channel_id=1, source_target_pairs={{0,1},{1,2},{2,3},{3,0},{4,5},{5,6},{6,7},{7,4},{8,9},{9,10},{10,1... | collective-permute-start | bytes 393224 | tf_op jit(solution)/shard_map/ppermute | solution.py:337
  123.2 8.9 %collective-permute-start.8 = (bf16[4,128,128]{2,1,0:T(8,128)(2,1)S(1)}, bf16[4,128,128]{2,1,0:T(8,128)(2,1)S(1)}, u32[]{:S(2)}, u32[]{:S(2)}) collective-permute-start(bf16[4,128,128]{2,1,0:T(8,128)(2,1)S(1)} %get-tuple-element.25), channel_id=1, source_target_pairs={{0,2},{1,3},{2,0},{3,1},{4,6},{5,7},{6,4},{7,5},{8,10},{9,11},{10,... | collective-permute-start | bytes 393224 | tf_op jit(solution)/shard_map/ppermute | solution.py:337
  127.5 6.3 %collective-permute-start.9 = (bf16[4,128,128]{2,1,0:T(8,128)(2,1)S(1)}, bf16[4,128,128]{2,1,0:T(8,128)(2,1)S(1)}, u32[]{:S(2)}, u32[]{:S(2)}) collective-permute-start(bf16[4,128,128]{2,1,0:T(8,128)(2,1)S(1)} %get-tuple-element.24), channel_id=1, source_target_pairs={{0,3},{1,0},{2,1},{3,2},{4,7},{5,4},{6,5},{7,6},{8,11},{9,8},{10,9... | collective-permute-start | bytes 393224 | tf_op jit(solution)/shard_map/ppermute | solution.py:337
  179.1 11.9 %collective-permute-start.10 = (bf16[16,24,128]{2,1,0:T(8,128)(2,1)S(1)}, bf16[16,24,128]{2,1,0:T(8,128)(2,1)S(1)}, u32[]{:S(2)}, u32[]{:S(2)}) collective-permute-start(bf16[16,24,128]{2,1,0:T(8,128)(2,1)S(1)} %slice.14), channel_id=1, source_target_pairs={{0,16},{16,0},{1,17},{17,1},{2,18},{18,2},{3,19},{19,3},{4,20},{20... | collective-permute-start | bytes 294920 | tf_op jit(solution)/shard_map/ppermute | solution.py:337
  186.0 5.1 %copy-start.1 = (s32[4]{0:T(128)S(1)}, s32[4]{0:T(128)}, u32[]{:S(2)}) copy-start(s32[4]{0:T(128)} %pad_add_fusion.s_ref) | copy-start | bytes 52
  186.0 5.1 %copy-start.2 = (s32[128,2]{0,1:T(2,128)S(1)}, s32[128,2]{0,1:T(2,128)}, u32[]{:S(2)}) copy-start(s32[128,2]{0,1:T(2,128)} %param.9) | copy-start | bytes 3076
  186.0 5.1 %copy-start.3 = (bf16[128,2]{0,1:T(2,128)(2,1)S(1)}, bf16[128,2]{0,1:T(2,128)(2,1)}, u32[]{:S(2)}) copy-start(bf16[128,2]{0,1:T(2,128)(2,1)} %param.10) | copy-start | bytes 1540

commit v3 on v2

--- a/solution.py
+++ b/solution.py
@@ -19,6 +19,7 @@
 ROWS = 512
 BLK = 4
 RB = ROWS // BLK
+SMALL = 12 * 2**20
 EXT = 8
 
 
@@ -90,23 +91,108 @@
     )(where, ids, w, tokens, cotangent)
 
 
-def forward_kernel(
-    s_ref, t_ref, c0_ref, c1_ref, c2_ref, c3_ref, wg_ref, wu_ref, wd_ref, g_ref, wt_ref, xt, xc, wgu, wdd
-):
+def x_of(s_ref, k):
+    return (s_ref[3] + k) & 3
+
+
+def pack_kernel(s_ref, wg_ref, wu_ref, wd_ref, *out_refs):
+    for k, out_ref in enumerate(out_refs):
+        for y in range(4):
+            cols = pl.ds(pl.multiple_of((y * 4 + x_of(s_ref, k)) * COL, COL), COL)
+            out_ref[y, :HID] = wg_ref[0, :, cols]
+            out_ref[y, HID : 2 * HID] = wu_ref[0, :, cols]
+            out_ref[y, 2 * HID :] = wd_ref[0, :, cols]
+
+
+def full(*shape):
+    return pl.BlockSpec(shape, lambda i, s: (0,) * len(shape))
+
+
+def call(kernel, where, args, in_specs, out_specs, out_shape, scratch=(), grid=1, flops=10**8, vmem=None):
+    return pl.pallas_call(
+        kernel,
+        grid_spec=pltpu.PrefetchScalarGridSpec(
+            num_scalar_prefetch=1,
+            grid=(grid,),
+            in_specs=in_specs,
+            out_specs=out_specs,
+            scratch_shapes=list(scratch),
+        ),
+        out_shape=out_shape,
+        compiler_params=pltpu.CompilerParams(vmem_limit_bytes=vmem),
+        cost_estimate=pl.CostEstimate(flops=flops, bytes_accessed=2 * 10**6, transcendentals=0),
+    )(where, *args)
+
+
+def pack(where, wg, wu, wd):
+    shape = (4, 3 * HID, COL)
+    return call(
+        pack_kernel,
+        where,
+        (wg, wu, wd),
+        [full(1, HID, TP * COL)] * 3,
+        [full(*shape)] * 4,
+        [jax.ShapeDtypeStruct(shape, BF)] * 4,
+    )
+
+
+def low_lanes(rows):
+    return iota((rows, COL), 1) < HID
+
+
+def features(x_ref, which, rows):
+    return jnp.concatenate([x_ref[y, :, which].reshape(rows, COL) for y in range(4)], axis=1)
+
+
+def pre_kernel(s_ref, x_ref, w_ref, out_ref, wgu, wdd):
     @pl.when(pl.program_id(0) == 0)
     def _():
-        wgu[:HID] = wg_ref[0]
-        wgu[HID:] = wu_ref[0]
-        wdd[:HID] = wd_ref[0]
-        wdd[HID:] = wd_ref[0]
-
-    for j in range(TP):
-        xt[:, j * COL : (j + 1) * COL] = t_ref[j].reshape(RB, COL)
-    for kx, c_ref in enumerate((c0_ref, c1_ref, c2_ref, c3_ref)):
-        for ky in range(4):
-            xc[:, piece_cols(s_ref, kx, ky)] = c_ref[ky].reshape(RB, COL)
-    pre = dot(xt[...], wgu[...], 1, 1)
-    back = dot(xc[...], wdd[...], 1, 1)
+        for k in range(4):
+            for y in range(4):
+                cols = slice(y * COL, (y + 1) * COL)
+                wgu[k * COL : (k + 1) * COL, cols] = w_ref[k, y, : 2 * HID]
+                wdd[k * COL : k * COL + HID, cols] = w_ref[k, y, 2 * HID :]
+                wdd[k * COL + HID : (k + 1) * COL, cols] = w_ref[k, y, 2 * HID :]
+
+    pre = dot(features(x_ref, 0, RB), wgu[...], 1, 1).astype(BF)
+    back = dot(features(x_ref, 1, RB), wdd[...], 1, 1)
+    for k in range(4):
+        cols = slice(k * COL, (k + 1) * COL)
+        to = x_of(s_ref, -k)
+        half = back[:, cols]
+        out_ref[to, 0, :RB] = pre[:, cols]
+        out_ref[to, 0, RB:] = jnp.where(low_lanes(RB // 2), half[: RB // 2], half[RB // 2 :]).astype(BF)
+
+
+PRE = RB + RB // 2
+ACT = PRE + EXT
+
+
+def pre_activations(where, x, w):
+    return call(
+        pre_kernel,
+        where,
+        (x, w),
+        [
+            pl.BlockSpec((4, NZ // BLK, 2, 2 * CAP, COL), lambda i, s: (0, i, 0, 0, 0)),
+            full(4, 4, 3 * HID, COL),
+        ],
+        pl.BlockSpec((4, 1, PRE, COL), lambda i, s: (0, i, 0, 0)),
+        jax.ShapeDtypeStruct((4, BLK, PRE, COL), BF),
+        [pltpu.VMEM((4 * COL, 4 * COL), BF), pltpu.VMEM((4 * COL, 4 * COL), BF)],
+        grid=BLK,
+        vmem=SMALL,
+    )
+
+
+def act_kernel(s_ref, p_ref, g_ref):
+    sums = p_ref[0, 0].astype(F32)
+    for x in range(1, 4):
+        sums = sums + p_ref[x, 0].astype(F32)
+    pre, packed = sums[:RB], sums[RB:]
+    low = low_lanes(RB // 2)
+    other = pltpu.roll(packed, HID, 1)
+    back = jnp.concatenate([jnp.where(low, packed, other), jnp.where(low, other, packed)], axis=0)
     lane = iota((RB, COL), 1)
     low_half = lane < HID
     turned = pltpu.roll(pre, HID, 1)
@@ -116,14 +202,28 @@
     silu = gate * sigma
     hidden = silu * up
     grads = jnp.where(low_half, back * up * sigma * (1.0 + gate * (1.0 - sigma)), back * silu).astype(BF)
-    wt_ref[...] = hidden[:, :HID].astype(BF)
+    weighted = jnp.where(low, hidden[: RB // 2], hidden[RB // 2 :]).astype(BF)
     total = jnp.sum(jnp.where(low_half, hidden * back, 0.0), axis=1, keepdims=True)
     spread = jnp.where((lane & 31) == (iota((RB, COL), 0) & 31), total, 0.0)
     group = (iota((EXT, RB), 0) == (iota((EXT, RB), 1) >> 5)).astype(F32)
     extra = two_parts(dot(group, spread, 1, 0, lax.Precision.HIGHEST))
     for x in range(4):
         g_ref[x, 0, :RB] = grads
-        g_ref[x, 0, RB:] = extra
+        g_ref[x, 0, RB:PRE] = weighted
+        g_ref[x, 0, PRE:] = extra
+
+
+def activations(where, p):
+    return call(
+        act_kernel,
+        where,
+        (p,),
+        [pl.BlockSpec((4, 1, PRE, COL), lambda i, s: (0, i, 0, 0))],
+        pl.BlockSpec((4, 1, ACT, COL), lambda i, s: (0, i, 0, 0)),
+        jax.ShapeDtypeStruct((4, BLK, ACT, COL), BF),
+        grid=BLK,
+        vmem=SMALL,
+    )
 
 
 def two_parts(sums):
@@ -138,59 +238,19 @@
     return both + pltpu.roll(both, 32, 1)
 
 
-def piece_cols(s_ref, kx, ky):
-    j = ((s_ref[2] - ky) & 3) * 4 + ((s_ref[3] - kx) & 3)
-    return pl.ds(pl.multiple_of(j * COL, COL), COL)
-
-
-def forward(where, t, cs, wg, wu, wd):
-    d = TP * COL
-    weight = pl.BlockSpec((1, HID, d), lambda i, s: (0, 0, 0))
-    return pl.pallas_call(
-        forward_kernel,
-        grid_spec=pltpu.PrefetchScalarGridSpec(
-            num_scalar_prefetch=1,
-            grid=(BLK,),
-            in_specs=[
-                pl.BlockSpec((TP, NZ // BLK, 2 * CAP, COL), lambda i, s: (0, i, 0, 0)),
-                *[pl.BlockSpec((4, NZ // BLK, 2 * CAP, COL), lambda i, s: (0, i, 0, 0))] * 4,
-                weight,
-                weight,
-                weight,
-            ],
-            out_specs=[
-                pl.BlockSpec((4, 1, RB + EXT, COL), lambda i, s: (0, i, 0, 0)),
-                pl.BlockSpec((RB, HID), lambda i, s: (i, 0)),
-            ],
-            scratch_shapes=[
-                pltpu.VMEM((RB, d), BF),
-                pltpu.VMEM((RB, d), BF),
-                pltpu.VMEM((2 * HID, d), BF),
-                pltpu.VMEM((2 * HID, d), BF),
-            ],
-        ),
-        out_shape=[
-            jax.ShapeDtypeStruct((4, BLK, RB + EXT, COL), BF),
-            jax.ShapeDtypeStruct((ROWS, HID), BF),
-        ],
-        name="forward",
-        cost_estimate=pl.CostEstimate(flops=10**9, bytes_accessed=5 * 10**6, transcendentals=10**5),
-    )(where, t, *cs, wg, wu, wd)
-
-
 def back_kernel(s_ref, g_ref, w_ref, out_ref, w):
     @pl.when(pl.program_id(0) == 0)
     def _():
         for k in range(4):
-            rows = pl.ds(pl.multiple_of(((s_ref[3] - k) & 3) * COL, COL), COL)
+            rows = pl.ds(pl.multiple_of(x_of(s_ref, -k) * COL, COL), COL)
             for y in range(4):
-                w[rows, y * COL : (y + 1) * COL] = w_ref[k, y]
+                w[rows, y * COL : (y + 1) * COL] = w_ref[k, y, : 2 * HID]
 
     grads = jnp.concatenate([g_ref[x, 0, :RB] for x in range(4)], axis=1)
     pieces = dot(grads, w[...], 1, 0).astype(BF)
-    parts = g_ref[0, 0, RB:].astype(F32)
+    parts = g_ref[0, 0, PRE:].astype(F32)
     for x in range(1, 4):
-        parts = parts + g_ref[x, 0, RB:].astype(F32)
+        parts = parts + g_ref[x, 0, PRE:].astype(F32)
     extra = two_parts(one_sum(parts))
     for y in range(4):
         out_ref[y, 0, :RB] = pieces[:, y * COL : (y + 1) * COL]
@@ -198,58 +258,69 @@
 
 
 def back(where, g, w):
-    block = pl.BlockSpec((4, 1, RB + EXT, COL), lambda i, s: (0, i, 0, 0))
-    return pl.pallas_call(
+    return call(
         back_kernel,
-        grid_spec=pltpu.PrefetchScalarGridSpec(
-            num_scalar_prefetch=1,
-            grid=(BLK,),
-            in_specs=[block, pl.BlockSpec((4, 4, 2 * HID, COL), lambda i, s: (0, 0, 0, 0))],
-            out_specs=block,
-            scratch_shapes=[pltpu.VMEM((4 * COL, 4 * COL), BF)],
-        ),
-        out_shape=jax.ShapeDtypeStruct((4, BLK, RB + EXT, COL), BF),
-        compiler_params=pltpu.CompilerParams(vmem_limit_bytes=8 * 2**20),
-        name="back",
-        cost_estimate=pl.CostEstimate(flops=3 * 10**8, bytes_accessed=10**6, transcendentals=0),
-    )(where, g, w)
-
-
-def weights_kernel(s_ref, t_ref, c0_ref, c1_ref, c2_ref, c3_ref, g_ref, wt_ref, dg_ref, du_ref, dd_ref):
-    grads = jnp.concatenate([g_ref[0, b, :RB] for b in range(BLK)], axis=0)
-    for j in range(TP):
-        cols = slice(j * COL, (j + 1) * COL)
-        both = dot(grads, t_ref[j].reshape(ROWS, COL), 0, 0)
-        dg_ref[0, :, cols] = both[:HID]
-        du_ref[0, :, cols] = both[HID:]
-    for kx, c_ref in enumerate((c0_ref, c1_ref, c2_ref, c3_ref)):
-        for ky in range(4):
-            dd_ref[0, :, piece_cols(s_ref, kx, ky)] = dot(
-                wt_ref[...], c_ref[ky].reshape(ROWS, COL), 0, 0
-            )
-
-
-def weights(where, t, cs, g, wt):
-    full = lambda *shape: pl.BlockSpec(shape, lambda i, s: (0,) * len(shape))
-    d = TP * COL
-    out = jax.ShapeDtypeStruct((1, HID, d), F32)
-    return pl.pallas_call(
+        where,
+        (g, w),
+        [pl.BlockSpec((4, 1, ACT, COL), lambda i, s: (0, i, 0, 0)), full(4, 4, 3 * HID, COL)],
+        pl.BlockSpec((4, 1, RB + EXT, COL), lambda i, s: (0, i, 0, 0)),
+        jax.ShapeDtypeStruct((4, BLK, RB + EXT, COL), BF),
+        [pltpu.VMEM((4 * COL, 4 * COL), BF)],
+        grid=BLK,
+        vmem=SMALL,
+    )
+
+
+def weights_kernel(s_ref, x_ref, g_ref, own_ref, *out_refs):
+    tok, cot = features(x_ref, 0, ROWS), features(x_ref, 1, ROWS)
+    for k, out_ref in enumerate((own_ref, *out_refs)):
+        owner = x_of(s_ref, k)
+        grads = jnp.concatenate([g_ref[owner, b, :RB] for b in range(BLK)], axis=0)
+        halves = []
+        for b in range(BLK):
+            packed = g_ref[owner, b, RB:PRE]
+            halves += [packed, pltpu.roll(packed.astype(F32), HID, 1).astype(BF)]
+        both = dot(grads, tok, 0, 0)
+        down = dot(jnp.concatenate(halves, axis=0), cot, 0, 0)
+        out_ref[: 2 * HID] = both.astype(out_ref.dtype)
+        out_ref[2 * HID :] = down[:HID].astype(out_ref.dtype)
+
+
+def weights(where, x, g):
+    shape = (3 * HID, 4 * COL)
+    return call(
         weights_kernel,
-        grid_spec=pltpu.PrefetchScalarGridSpec(
-            num_scalar_prefetch=1,
-            grid=(1,),
-            in_specs=[
-                full(TP, NZ, 2 * CAP, COL),
-                *[full(4, NZ, 2 * CAP, COL)] * 4,
-                full(1, BLK, RB + EXT, COL),
-                full(ROWS, HID),
-            ],
-            out_specs=[full(1, HID, d)] * 3,
-        ),
-        out_shape=[out, out, out],
-        name="weights",
-        cost_estimate=pl.CostEstimate(flops=4 * 10**9, bytes_accessed=6 * 10**6, transcendentals=0),
-    )(where, t, *cs, g, wt)
+        where,
+        (x, g),
+        [full(4, NZ, 2, 2 * CAP, COL), full(4, BLK, ACT, COL)],
+        [full(*shape)] * 4,
+        [jax.ShapeDtypeStruct(shape, F32)] + [jax.ShapeDtypeStruct(shape, BF)] * 3,
+        flops=4 * 10**9,
+    )
+
+
+def assemble_kernel(s_ref, *refs):
+    *parts, dg_ref, du_ref, dd_ref = refs
+    for k, p_ref in enumerate(parts):
+        for y in range(4):
+            cols = pl.ds(pl.multiple_of((y * 4 + x_of(s_ref, -k)) * COL, COL), COL)
+            here = slice(y * COL, (y + 1) * COL)
+            dg_ref[0, :, cols] = p_ref[:HID, here].astype(F32)
+            du_ref[0, :, cols] = p_ref[HID : 2 * HID, here].astype(F32)
+            dd_ref[0, :, cols] = p_ref[2 * HID :, here].astype(F32)
+
+
+def assemble(where, parts):
+    shape = (1, HID, TP * COL)
+    return call(
+        assemble_kernel,
+        where,
+        parts,
+        [full(3 * HID, 4 * COL)] * 4,
+        [full(*shape)] * 3,
+        [jax.ShapeDtypeStruct(shape, F32)] * 3,
+        flops=10**9,
+    )
 
 
 def total_kernel(p_ref, out_ref):
@@ -337,12 +408,10 @@
     return lax.ppermute(x, axis, [(i, (i + by) % n) for i in range(n)])
 
 
-def row_weights(gate_weight, up_weight, x):
-    both = jnp.concatenate([gate_weight[0], up_weight[0]], axis=0)
-    blocks = both.reshape(2 * HID, 4, 4, COL).transpose(2, 1, 0, 3)
-    own = [lax.dynamic_index_in_dim(blocks, (x + k) & 3, 0, keepdims=False) for k in range(4)]
-    moved = [shifted(own[k], "x", k) for k in range(1, 4)]
-    return jnp.stack([own[0]] + moved)
+def row_weights(where, wg, wu, wd):
+    own, *others = pack(where, wg, wu, wd)
+    moved = [shifted(other, "x", k + 1) for k, other in enumerate(others)]
+    return jnp.stack([own, *moved])
 
 
 def per_device(tokens, cotangent, expert_ids, route_weight, gate_weight, up_weight, down_weight):
@@ -353,19 +422,18 @@
     got = shifted(other, "c", 1)
     mine = jnp.stack([own, got], axis=2).reshape(NZ, 2, 2 * CAP, COL)
     mine = exchange(mine, "z")
-    row_w = row_weights(gate_weight, up_weight, x)
-    tok, cot = mine[:, 0], mine[:, 1]
-    tok_row = exchange(copies(tok, 4), "x")
-    cot_moved = [shifted(cot, "y", k) for k in range(1, 4)]
-    cot_col = jnp.stack([cot] + cot_moved)
-    tok_all = exchange(copies(tok_row, 4), "y").reshape(TP, NZ, 2 * CAP, COL)
-    cot_all = [cot_col] + [shifted(cot_col, "x", k) for k in range(1, 4)]
-    g, wt = forward(where, tok_all, cot_all, gate_weight, up_weight, down_weight)
-    g_all = exchange(g, "x")
-    part = back(where, g_all, row_w)
+    row_w = row_weights(where, gate_weight, up_weight, down_weight)
+    rows = exchange(copies(mine, 4), "y")
+    pre = pre_activations(where, rows, row_w)
+    pre = exchange(pre, "x")
+    g = activations(where, pre)
+    g = exchange(g, "x")
+    part = back(where, g, row_w)
     sums = exchange(part, "y")
-    gate_grad, up_grad, down_grad = weights(where, tok_all, cot_all, g, wt)
+    kept, *sent = weights(where, rows, g)
     home = exchange(total(sums), "z")
+    moved = [shifted(part, "x", k + 1) for k, part in enumerate(sent)]
+    gate_grad, up_grad, down_grad = assemble(where, (kept, *moved))
     far = shifted(home[:, CAP:], "c", 1)
     tokens_grad, route_grad = combine(where, ids, w, home, far)
     return tokens_grad, route_grad.T, gate_grad, up_grad, down_grad

time: 194 us -> 148 us (0.76)
  waiting for transfers between devices: 34.5 us -> 4.74 us
  blocking collectives: 76.9 us -> 57.2 us
  Pallas kernels: 18.7 us -> 22.5 us
  local copies, waits for them, and re-layouts: 5.48 us -> 2.11 us
    ppermute x11 -> x8, waiting for transfers between devices: 34.5 us -> 4.73 us  [shifted(): return lax.ppermute(x, axis, [(i, (i + by) % n) for i in range(n)])]
    all_to_all x4, blocking collectives: 76.9 us -> 57.2 us  [exchange(): return lax.all_to_all(x, axis, split_axis=0, concat_axis=0, tiled=True)]
    all_to_all x2, starting transfers between devices: 9.11 us -> 20.1 us  [exchange(): return lax.all_to_all(x, axis, split_axis=0, concat_axis=0, tiled=True)]
    ppermute x11 -> x8, starting transfers between devices: 45.5 us -> 36.1 us  [shifted(): return lax.ppermute(x, axis, [(i, (i + by) % n) for i in range(n)])]
    pallas_call x3 -> x6, Pallas kernels: 13.7 us -> 16.5 us  [call(): pl.pallas_call(kernel, grid_spec=pltpu.PrefetchScalarGridSpec(num_scalar_...]
  transfers between devices with their start and end apart: 13 -> 10, of which waited for: 8 -> 3; matrix products, arithmetic and copies ran while one was open for 1% -> 1% of each run, Pallas kernels for 3% -> 7%
where the time goes in v3:
time: 148 us; the launch traced here: 146 us
  blocking collectives  57.2 us (39%)
  starting transfers between devices  56.2 us (38%)
  Pallas kernels  22.5 us (15%)
  waiting for transfers between devices  4.74 us (3%)
  other arithmetic  2.51 us (2%)
  local copies, waits for them, and re-layouts  2.11 us (1%)
    all_to_all x4, blocking collectives, exchange(): return lax.all_to_all(x, axis, split_axis=0, concat_axis=0, tiled=True)  57.2 us
    ppermute x8, starting transfers between devices, shifted(): return lax.ppermute(x, axis, [(i, (i + by) % n) for i in range(n)])  36.1 us
    all_to_all x2, starting transfers between devices, exchange(): return lax.all_to_all(x, axis, split_axis=0, concat_axis=0, tiled=True)  20.1 us
    pallas_call x6, Pallas kernels, call(): pl.pallas_call(kernel, grid_spec=pltpu.PrefetchScalarGridSpec(num_scalar_...  16.5 us
    ppermute x8, waiting for transfers between devices, shifted(): return lax.ppermute(x, axis, [(i, (i + by) % n) for i in range(n)])  4.73 us
  transfers between devices with their start and end apart: 10, of which 3 were waited for; matrix products, arithmetic and copies ran while one was open for 1% of the time, Pallas kernels for 7%

profile of v3, /device:TPU:1, one launch (start us, length us, event | category | flops | bytes accessed | tf_op | source)
XLA Modules:
  0.0 146.2 jit_solution(4989080220548067863)
XLA Ops:
  0.6 0.6 pad_add_fusion.s_ref
  1.2 2.6 %dispatch.1 = (bf16[16,2,16,128]{3,2,1,0:T(8,128)(2,1)}, bf16[16,2,16,128]{3,2,1,0:T(8,128)(2,1)}) custom-call(s32[4]{0:T(128)} %pad_add_fusion.s_ref, s32[2,128]{1,0:T(2,128)} %bitcast.14, bf16[2,128]{1,0:T(2,128)(2,1)} %bitcast.16, bf16[128,2048]{1,0:T(8,128)(2,1)} %tok_ref.1, bf16[128,2048]{1,0:T(8,128)(2,1)} %cot_ref.1), custom_call_target="tpu_custom_call" | custom-call | flops 100000000 | bytes 1000000 | tf_op jit(solution)/shard_map/dispatch/pallas_call | solution.py:75
  3.8 8.7 %collective-permute-start = (bf16[16,2,16,128]{3,2,1,0:T(8,128)(2,1)}, bf16[16,2,16,128]{3,2,1,0:T(8,128)(2,1)S(1)}, u32[]{:S(2)}, u32[]{:S(2)}) collective-permute-start(bf16[16,2,16,128]{3,2,1,0:T(8,128)(2,1)} %get-tuple-element.21), channel_id=1, source_target_pairs={{0,16},{16,0},{1,17},{17,1},{2,18},{18,2},{3,19},{19,3},{4,20},{20... | collective-permute-start | bytes 393224 | tf_op jit(solution)/shard_map/ppermute | solution.py:408
  12.5 1.2 collective-permute-done
  13.7 0.9 pad_maximum_fusion.1
  14.7 23.4 %all_to_all.30 = bf16[16,2,32,128]{3,2,1,0:T(8,128)(2,1)S(1)} all-to-all(bf16[16,2,32,128]{3,2,1,0:T(8,128)(2,1)S(1)} %bitcast.18), channel_id=1, replica_groups=mesh['z'=16,'c'=2,'y'=4,'x'=4] {'z'}, dimensions={0} | all-to-all | bytes 524288 | tf_op jit(solution)/shard_map/all_to_all | solution.py:399
  38.1 1.3 broadcast_in_dim.2
  39.3 4.2 %all-to-all-start.1 = ((bf16[4,16,2,32,128]{4,3,2,1,0:T(8,128)(2,1)}), bf16[4,16,2,32,128]{4,3,2,1,0:T(8,128)(2,1)S(1)}, u32[]{:S(2)}, u32[]{:S(2)}) async-start(bf16[4,16,2,32,128]{4,3,2,1,0:T(8,128)(2,1)} %broadcast_in_dim.2), calls=%async_computation.1 | async-start | bytes 2097152 | tf_op jit(solution)/shard_map/all_to_all | solution.py:399
  43.5 2.8 %shard_map.110 = (bf16[4,192,128]{2,1,0:T(8,128)(2,1)}, bf16[4,192,128]{2,1,0:T(8,128)(2,1)}, bf16[4,192,128]{2,1,0:T(8,128)(2,1)}, bf16[4,192,128]{2,1,0:T(8,128)(2,1)}) custom-call(s32[4]{0:T(128)} %pad_add_fusion.s_ref, bf16[1,64,2048]{2,1,0:T(8,128)(2,1)} %wg_ref.1, bf16[1,64,2048]{2,1,0:T(8,128)(2,1)} %wu_ref.1, bf16[1,64,2048]{2,1,0:T(8,128)(2,1)} %wd_ref.1), custom_call_target="tpu_custom_call" | custom-call | flops 100000000 | bytes 2000000 | tf_op jit(solution)/shard_map/pallas_call | solution.py:112
  46.3 3.1 %collective-permute-start.1 = (bf16[4,192,128]{2,1,0:T(8,128)(2,1)}, bf16[4,192,128]{2,1,0:T(8,128)(2,1)S(1)}, u32[]{:S(2)}, u32[]{:S(2)}) collective-permute-start(bf16[4,192,128]{2,1,0:T(8,128)(2,1)} %get-tuple-element.23), channel_id=1, source_target_pairs={{0,1},{1,2},{2,3},{3,0},{4,5},{5,6},{6,7},{7,4},{8,9},{9,10},{10,1... | collective-permute-start | bytes 589832 | tf_op jit(solution)/shard_map/ppermute | solution.py:408
  49.5 4.4 %collective-permute-start.2 = (bf16[4,192,128]{2,1,0:T(8,128)(2,1)}, bf16[4,192,128]{2,1,0:T(8,128)(2,1)S(1)}, u32[]{:S(2)}, u32[]{:S(2)}) collective-permute-start(bf16[4,192,128]{2,1,0:T(8,128)(2,1)} %get-tuple-element.24), channel_id=1, source_target_pairs={{0,2},{1,3},{2,0},{3,1},{4,6},{5,7},{6,4},{7,5},{8,10},{9,11},{10,... | collective-permute-start | bytes 589832 | tf_op jit(solution)/shard_map/ppermute | solution.py:408
  53.8 3.1 %collective-permute-start.3 = (bf16[4,192,128]{2,1,0:T(8,128)(2,1)}, bf16[4,192,128]{2,1,0:T(8,128)(2,1)S(1)}, u32[]{:S(2)}, u32[]{:S(2)}) collective-permute-start(bf16[4,192,128]{2,1,0:T(8,128)(2,1)} %get-tuple-element.25), channel_id=1, source_target_pairs={{0,3},{1,0},{2,1},{3,2},{4,7},{5,4},{6,5},{7,6},{8,11},{9,8},{10,9... | collective-permute-start | bytes 589832 | tf_op jit(solution)/shard_map/ppermute | solution.py:408
  56.9 0.0 collective-permute-done.1
  56.9 1.0 collective-permute-done.2
  57.9 2.6 %collective-permute-done.3 = bf16[4,192,128]{2,1,0:T(8,128)(2,1)S(1)} collective-permute-done((bf16[4,192,128]{2,1,0:T(8,128)(2,1)}, bf16[4,192,128]{2,1,0:T(8,128)(2,1)S(1)}, u32[]{:S(2)}, u32[]{:S(2)}) %collective-permute-start.3) | collective-permute-done | bytes 196640 | tf_op jit(solution)/shard_map/ppermute | solution.py:408
  60.4 1.0 pad_maximum_fusion.w_ref
  61.5 0.0 all-to-all-done.1.x_ref
  61.5 0.0 copy-done.2
  61.5 0.0 copy-start
  61.5 2.8 %shard_map.111 = bf16[4,4,192,128]{3,2,1,0:T(8,128)(2,1)S(1)} custom-call(s32[4]{0:T(128)S(1)} %copy-done.2, bf16[4,16,2,32,128]{4,3,2,1,0:T(8,128)(2,1)S(1)} %all-to-all-done.1.x_ref, bf16[4,4,192,128]{3,2,1,0:T(8,128)(2,1)S(1)} %pad_maximum_fusion.w_ref), custom_call_target="tpu_custom_call" | custom-call | flops 100000000 | bytes 2000000 | tf_op jit(solution)/shard_map/pallas_call | solution.py:112
  64.4 0.0 copy-done
  64.4 11.8 %all_to_all.31.p_ref = bf16[4,4,192,128]{3,2,1,0:T(8,128)(2,1)S(1)} all-to-all(bf16[4,4,192,128]{3,2,1,0:T(8,128)(2,1)S(1)} %shard_map.111), channel_id=1, replica_groups=mesh['z'=16,'c'=2,'y'=4,'x'=4] {'x'}, dimensions={0} | all-to-all | bytes 1572864 | tf_op jit(solution)/shard_map/all_to_all | solution.py:399
  76.2 2.1 %shard_map.112 = bf16[4,4,200,128]{3,2,1,0:T(8,128)(2,1)S(1)} custom-call(s32[4]{0:T(128)S(1)} %copy-done.2, bf16[4,4,192,128]{3,2,1,0:T(8,128)(2,1)S(1)} %all_to_all.31.p_ref), custom_call_target="tpu_custom_call" | custom-call | flops 100000000 | bytes 2000000 | tf_op jit(solution)/shard_map/pallas_call | solution.py:112
  78.3 10.9 %all_to_all.32.g_ref = bf16[4,4,200,128]{3,2,1,0:T(8,128)(2,1)S(1)} all-to-all(bf16[4,4,200,128]{3,2,1,0:T(8,128)(2,1)S(1)} %shard_map.112), channel_id=1, replica_groups=mesh['z'=16,'c'=2,'y'=4,'x'=4] {'x'}, dimensions={0} | all-to-all | bytes 1638400 | tf_op jit(solution)/shard_map/all_to_all | solution.py:399
  89.2 1.8 %shard_map.113 = bf16[4,4,136,128]{3,2,1,0:T(8,128)(2,1)S(1)} custom-call(s32[4]{0:T(128)S(1)} %copy-done.2, bf16[4,4,200,128]{3,2,1,0:T(8,128)(2,1)S(1)} %all_to_all.32.g_ref, bf16[4,4,192,128]{3,2,1,0:T(8,128)(2,1)S(1)} %pad_maximum_fusion.w_ref), custom_call_target="tpu_custom_call" | custom-call | flops 100000000 | bytes 2000000 | tf_op jit(solution)/shard_map/pallas_call | solution.py:112
  90.9 0.0 copy-done.1
  91.0 11.1 %all_to_all.33.p_ref = bf16[4,4,136,128]{3,2,1,0:T(8,128)(2,1)S(1)} all-to-all(bf16[4,4,136,128]{3,2,1,0:T(8,128)(2,1)S(1)} %shard_map.113), channel_id=1, replica_groups=mesh['z'=16,'c'=2,'y'=4,'x'=4] {'y'}, dimensions={0} | all-to-all | bytes 1114112 | tf_op jit(solution)/shard_map/all_to_all | solution.py:399
  102.1 1.7 %total.1 = bf16[16,40,128]{2,1,0:T(8,128)(2,1)} custom-call(bf16[4,4,136,128]{3,2,1,0:T(8,128)(2,1)S(1)} %all_to_all.33.p_ref), custom_call_target="tpu_custom_call" | custom-call | flops 10000000 | bytes 2000000 | tf_op jit(solution)/shard_map/total/pallas_call | solution.py:337
  103.8 15.9 %all-to-all-start.5 = ((bf16[16,40,128]{2,1,0:T(8,128)(2,1)}), bf16[16,40,128]{2,1,0:T(8,128)(2,1)S(1)}, u32[]{:S(2)}, u32[]{:S(2)}) async-start(bf16[16,40,128]{2,1,0:T(8,128)(2,1)} %total.1), calls=%async_computation.5 | async-start | bytes 327680 | tf_op jit(solution)/shard_map/all_to_all | solution.py:399
  119.8 3.6 %shard_map.114 = (f32[192,512]{1,0:T(8,128)}, bf16[192,512]{1,0:T(8,128)(2,1)}, bf16[192,512]{1,0:T(8,128)(2,1)}, bf16[192,512]{1,0:T(8,128)(2,1)}) custom-call(s32[4]{0:T(128)} %pad_add_fusion.s_ref, bf16[4,16,2,32,128]{4,3,2,1,0:T(8,128)(2,1)} %copy-done, bf16[4,4,200,128]{3,2,1,0:T(8,128)(2,1)} %copy-done.1), custom_call_target="tpu_custom_call" | custom-call | flops 4000000000 | bytes 2000000 | tf_op jit(solution)/shard_map/pallas_call | solution.py:112
  123.4 2.2 %collective-permute-start.5 = (bf16[192,512]{1,0:T(8,128)(2,1)}, bf16[192,512]{1,0:T(8,128)(2,1)S(1)}, u32[]{:S(2)}, u32[]{:S(2)}) collective-permute-start(bf16[192,512]{1,0:T(8,128)(2,1)} %get-tuple-element.29), channel_id=1, source_target_pairs={{0,1},{1,2},{2,3},{3,0},{4,5},{5,6},{6,7},{7,4},{8,9},{9,10},{10,1... | collective-permute-start | bytes 589832 | tf_op jit(solution)/shard_map/ppermute | solution.py:408
  125.6 3.7 %collective-permute-start.6 = (bf16[192,512]{1,0:T(8,128)(2,1)}, bf16[192,512]{1,0:T(8,128)(2,1)S(1)}, u32[]{:S(2)}, u32[]{:S(2)}) collective-permute-start(bf16[192,512]{1,0:T(8,128)(2,1)} %get-tuple-element.30), channel_id=1, source_target_pairs={{0,2},{1,3},{2,0},{3,1},{4,6},{5,7},{6,4},{7,5},{8,10},{9,11},{10,... | collective-permute-start | bytes 589832 | tf_op jit(solution)/shard_map/ppermute | solution.py:408
  129.3 2.6 %collective-permute-start.7 = (bf16[192,512]{1,0:T(8,128)(2,1)}, bf16[192,512]{1,0:T(8,128)(2,1)S(1)}, u32[]{:S(2)}, u32[]{:S(2)}) collective-permute-start(bf16[192,512]{1,0:T(8,128)(2,1)} %get-tuple-element.31), channel_id=1, source_target_pairs={{0,3},{1,0},{2,1},{3,2},{4,7},{5,4},{6,5},{7,6},{8,11},{9,8},{10,9... | collective-permute-start | bytes 589832 | tf_op jit(solution)/shard_map/ppermute | solution.py:408
  131.9 0.0 all-to-all-done.5.own_ref
  131.9 8.3 %collective-permute-start.4 = (bf16[16,24,128]{2,1,0:T(8,128)(2,1)S(1)}, bf16[16,24,128]{2,1,0:T(8,128)(2,1)S(1)}, u32[]{:S(2)}, u32[]{:S(2)}) collective-permute-start(bf16[16,24,128]{2,1,0:T(8,128)(2,1)S(1)} %slice.4), channel_id=1, source_target_pairs={{0,16},{16,0},{1,17},{17,1},{2,18},{18,2},{3,19},{19,3},{4,20},{20... | collective-permute-start | bytes 294920 | tf_op jit(solution)/shard_map/ppermute | solution.py:408
  140.2 0.0 collective-permute-done.5.refs_1_
  140.2 0.0 copy-start.6
  140.3 0.0 collective-permute-done.6.refs_2_
  140.3 0.0 copy-start.7
  140.3 0.0 collective-permute-done.7.refs_3_
  140.3 0.0 copy-start.8
  140.3 0.6 copy-done.6
  140.9 0.1 copy-done.7
  141.0 0.1 copy-done.8
  141.1 3.3 %shard_map.115 = (f32[1,64,2048]{2,1,0:T(8,128)}, f32[1,64,2048]{2,1,0:T(8,128)}, f32[1,64,2048]{2,1,0:T(8,128)}) custom-call(s32[4]{0:T(128)} %pad_add_fusion.s_ref, f32[192,512]{1,0:T(8,128)} %get-tuple-element.28.refs_0_, bf16[192,512]{1,0:T(8,128)(2,1)} %copy-done.6, bf16[192,512]{1,0:T(8,128)(2,1)} %copy-done.7, bf16[192,512]{1,0:T(8,128)(2,1)} %copy-done.8), custom_call_target="tpu_custom_call" | custom-call | flops 1000000000 | bytes 2000000 | tf_op jit(solution)/shard_map/pallas_call | solution.py:112
  144.4 0.0 collective-permute-done.4.other_ref
  144.4 0.0 copy-done.3
  144.4 1.7 %combine.1 = (bf16[128,128]{1,0:T(8,128)(2,1)}, f32[2,128]{1,0:T(2,128)}) custom-call(s32[4]{0:T(128)S(1)} %copy-done.3, s32[2,128]{1,0:T(2,128)S(1)} %bitcast.15, bf16[2,128]{1,0:T(2,128)(2,1)S(1)} %bitcast.17, bf16[16,40,128]{2,1,0:T(8,128)(2,1)S(1)} %all-to-all-done.5.own_ref, bf16[16,24,128]{2,1,0:T(8,128)(2,1)S(1)} %collective-permute-done.4.other_ref), custom_call_target="tpu_custom_call" | custom-call | flops 100000000 | bytes 1000000 | tf_op jit(solution)/shard_map/combine/pallas_call | solution.py:378
  (9 shorter events, 0.0 us)
Async XLA Ops:
  3.8 9.9 %collective-permute-start = (bf16[16,2,16,128]{3,2,1,0:T(8,128)(2,1)}, bf16[16,2,16,128]{3,2,1,0:T(8,128)(2,1)S(1)}, u32[]{:S(2)}, u32[]{:S(2)}) collective-permute-start(bf16[16,2,16,128]{3,2,1,0:T(8,128)(2,1)} %get-tuple-element.21), channel_id=1, source_target_pairs={{0,16},{16,0},{1,17},{17,1},{2,18},{18,2},{3,19},{19,3},{4,20},{20... | collective-permute-start | bytes 393224 | tf_op jit(solution)/shard_map/ppermute | solution.py:408
  39.3 22.2 %all-to-all-start.1 = ((bf16[4,16,2,32,128]{4,3,2,1,0:T(8,128)(2,1)}), bf16[4,16,2,32,128]{4,3,2,1,0:T(8,128)(2,1)S(1)}, u32[]{:S(2)}, u32[]{:S(2)}) async-start(bf16[4,16,2,32,128]{4,3,2,1,0:T(8,128)(2,1)} %broadcast_in_dim.2), calls=%async_computation.1 | async-start | bytes 2097152 | tf_op jit(solution)/shard_map/all_to_all | solution.py:399
  46.3 10.6 %collective-permute-start.1 = (bf16[4,192,128]{2,1,0:T(8,128)(2,1)}, bf16[4,192,128]{2,1,0:T(8,128)(2,1)S(1)}, u32[]{:S(2)}, u32[]{:S(2)}) collective-permute-start(bf16[4,192,128]{2,1,0:T(8,128)(2,1)} %get-tuple-element.23), channel_id=1, source_target_pairs={{0,1},{1,2},{2,3},{3,0},{4,5},{5,6},{6,7},{7,4},{8,9},{9,10},{10,1... | collective-permute-start | bytes 589832 | tf_op jit(solution)/shard_map/ppermute | solution.py:408
  49.5 8.4 %collective-permute-start.2 = (bf16[4,192,128]{2,1,0:T(8,128)(2,1)}, bf16[4,192,128]{2,1,0:T(8,128)(2,1)S(1)}, u32[]{:S(2)}, u32[]{:S(2)}) collective-permute-start(bf16[4,192,128]{2,1,0:T(8,128)(2,1)} %get-tuple-element.24), channel_id=1, source_target_pairs={{0,2},{1,3},{2,0},{3,1},{4,6},{5,7},{6,4},{7,5},{8,10},{9,11},{10,... | collective-permute-start | bytes 589832 | tf_op jit(solution)/shard_map/ppermute | solution.py:408
  53.8 6.6 %collective-permute-start.3 = (bf16[4,192,128]{2,1,0:T(8,128)(2,1)}, bf16[4,192,128]{2,1,0:T(8,128)(2,1)S(1)}, u32[]{:S(2)}, u32[]{:S(2)}) collective-permute-start(bf16[4,192,128]{2,1,0:T(8,128)(2,1)} %get-tuple-element.25), channel_id=1, source_target_pairs={{0,3},{1,0},{2,1},{3,2},{4,7},{5,4},{6,5},{7,6},{8,11},{9,8},{10,9... | collective-permute-start | bytes 589832 | tf_op jit(solution)/shard_map/ppermute | solution.py:408
  60.4 1.0 copy-start.2
  61.5 2.9 %copy-start = (bf16[4,16,2,32,128]{4,3,2,1,0:T(8,128)(2,1)}, bf16[4,16,2,32,128]{4,3,2,1,0:T(8,128)(2,1)S(1)}, u32[]{:S(2)}) copy-start(bf16[4,16,2,32,128]{4,3,2,1,0:T(8,128)(2,1)S(1)} %all-to-all-done.1.x_ref) | copy-start | bytes 3145732
  89.2 1.8 %copy-start.1 = (bf16[4,4,200,128]{3,2,1,0:T(8,128)(2,1)}, bf16[4,4,200,128]{3,2,1,0:T(8,128)(2,1)S(1)}, u32[]{:S(2)}) copy-start(bf16[4,4,200,128]{3,2,1,0:T(8,128)(2,1)S(1)} %all_to_all.32.g_ref) | copy-start | bytes 2457604
  103.8 28.1 %all-to-all-start.5 = ((bf16[16,40,128]{2,1,0:T(8,128)(2,1)}), bf16[16,40,128]{2,1,0:T(8,128)(2,1)S(1)}, u32[]{:S(2)}, u32[]{:S(2)}) async-start(bf16[16,40,128]{2,1,0:T(8,128)(2,1)} %total.1), calls=%async_computation.5 | async-start | bytes 327680 | tf_op jit(solution)/shard_map/all_to_all | solution.py:399
  123.4 16.9 %collective-permute-start.5 = (bf16[192,512]{1,0:T(8,128)(2,1)}, bf16[192,512]{1,0:T(8,128)(2,1)S(1)}, u32[]{:S(2)}, u32[]{:S(2)}) collective-permute-start(bf16[192,512]{1,0:T(8,128)(2,1)} %get-tuple-element.29), channel_id=1, source_target_pairs={{0,1},{1,2},{2,3},{3,0},{4,5},{5,6},{6,7},{7,4},{8,9},{9,10},{10,1... | collective-permute-start | bytes 589832 | tf_op jit(solution)/shard_map/ppermute | solution.py:408
  125.6 14.7 %collective-permute-start.6 = (bf16[192,512]{1,0:T(8,128)(2,1)}, bf16[192,512]{1,0:T(8,128)(2,1)S(1)}, u32[]{:S(2)}, u32[]{:S(2)}) collective-permute-start(bf16[192,512]{1,0:T(8,128)(2,1)} %get-tuple-element.30), channel_id=1, source_target_pairs={{0,2},{1,3},{2,0},{3,1},{4,6},{5,7},{6,4},{7,5},{8,10},{9,11},{10,... | collective-permute-start | bytes 589832 | tf_op jit(solution)/shard_map/ppermute | solution.py:408
  129.3 11.0 %collective-permute-start.7 = (bf16[192,512]{1,0:T(8,128)(2,1)}, bf16[192,512]{1,0:T(8,128)(2,1)S(1)}, u32[]{:S(2)}, u32[]{:S(2)}) collective-permute-start(bf16[192,512]{1,0:T(8,128)(2,1)} %get-tuple-element.31), channel_id=1, source_target_pairs={{0,3},{1,0},{2,1},{3,2},{4,7},{5,4},{6,5},{7,6},{8,11},{9,8},{10,9... | collective-permute-start | bytes 589832 | tf_op jit(solution)/shard_map/ppermute | solution.py:408
  131.9 12.5 %collective-permute-start.4 = (bf16[16,24,128]{2,1,0:T(8,128)(2,1)S(1)}, bf16[16,24,128]{2,1,0:T(8,128)(2,1)S(1)}, u32[]{:S(2)}, u32[]{:S(2)}) collective-permute-start(bf16[16,24,128]{2,1,0:T(8,128)(2,1)S(1)} %slice.4), channel_id=1, source_target_pairs={{0,16},{16,0},{1,17},{17,1},{2,18},{18,2},{3,19},{19,3},{4,20},{20... | collective-permute-start | bytes 294920 | tf_op jit(solution)/shard_map/ppermute | solution.py:408
  140.2 0.7 copy-start.6
  140.3 0.7 copy-start.7
  140.3 0.8 copy-start.8
  141.1 3.3 %copy-start.3 = (s32[4]{0:T(128)S(1)}, s32[4]{0:T(128)}, u32[]{:S(2)}) copy-start(s32[4]{0:T(128)} %pad_add_fusion.s_ref) | copy-start | bytes 52
  141.1 3.3 %copy-start.4 = (s32[128,2]{0,1:T(2,128)S(1)}, s32[128,2]{0,1:T(2,128)}, u32[]{:S(2)}) copy-start(s32[128,2]{0,1:T(2,128)} %param.9) | copy-start | bytes 3076
  141.1 3.3 %copy-start.5 = (bf16[128,2]{0,1:T(2,128)(2,1)S(1)}, bf16[128,2]{0,1:T(2,128)(2,1)}, u32[]{:S(2)}) copy-start(bf16[128,2]{0,1:T(2,128)(2,1)} %param.10) | copy-start | bytes 1540

commit v4 on v3

--- a/solution.py
+++ b/solution.py
@@ -33,7 +33,7 @@
     )
 
 
-def routing(ids_ref, core):
+def routing(ids_ref):
     experts = 2 * NZ
     row = iota((experts, TOK), 0)
     first = (ids_ref[0:1, :] == row).astype(F32)
@@ -41,11 +41,8 @@
     member = first + second
     earlier = (iota((TOK, TOK), 0) < iota((TOK, TOK), 1)).astype(BF)
     rank = dot(member.astype(BF), earlier, 1, 0)
-    slots = 2 * NZ * CAP
-    slot = iota((slots, experts), 0)
-    half = slot >> 8
-    expert = 2 * ((slot & 255) >> 4) + jnp.where(half == 0, core, 1 - core)
-    expand = (expert == iota((slots, experts), 1)).astype(BF)
+    slots = experts * CAP
+    expand = ((iota((slots, experts), 0) >> 4) == iota((slots, experts), 1)).astype(BF)
     hit = dot(expand, member.astype(BF), 1, 0)
     at = dot(expand, rank.astype(BF), 1, 0)
     place = (iota((slots, TOK), 0) & 15).astype(F32)
@@ -53,46 +50,31 @@
     return first, second, rank, expand, chosen
 
 
-def dispatch_kernel(s_ref, ids_ref, w_ref, tok_ref, cot_ref, own_ref, other_ref):
-    first, second, _, expand, chosen = routing(ids_ref, s_ref[1])
+def dispatch_kernel(s_ref, ids_ref, w_ref, tok_ref, cot_ref, out_ref):
+    first, second, _, expand, chosen = routing(ids_ref)
     w = w_ref[...].astype(F32)
     weighted = first * w[0:1, :] + second * w[1:2, :]
     scale = dot(expand, weighted.astype(BF), 1, 0)
     pick = jnp.where(chosen, 1.0, 0.0).astype(BF)
     pick_scaled = jnp.where(chosen, scale, 0.0).astype(BF)
-    rows = dot(pick, tok_ref[...], 1, 0).astype(BF)
-    cots = dot(pick_scaled, cot_ref[...], 1, 0).astype(BF)
-    half = NZ * CAP
-    own_ref[:, 0] = rows[:half].reshape(NZ, CAP, COL)
-    own_ref[:, 1] = cots[:half].reshape(NZ, CAP, COL)
-    other_ref[:, 0] = rows[half:].reshape(NZ, CAP, COL)
-    other_ref[:, 1] = cots[half:].reshape(NZ, CAP, COL)
+    out_ref[:, :, 0] = dot(pick, tok_ref[...], 1, 0).astype(BF).reshape(NZ, 2, CAP, COL)
+    out_ref[:, :, 1] = dot(pick_scaled, cot_ref[...], 1, 0).astype(BF).reshape(NZ, 2, CAP, COL)
 
 
 def dispatch(where, ids, w, tokens, cotangent):
-    full = lambda *shape: pl.BlockSpec(shape, lambda i, s: (0,) * len(shape))
-    out = jax.ShapeDtypeStruct((NZ, 2, CAP, COL), BF)
-    return pl.pallas_call(
+    mine = pl.BlockSpec((TOK, COL), lambda i, s: (0, s[0]))
+    return call(
         dispatch_kernel,
-        grid_spec=pltpu.PrefetchScalarGridSpec(
-            num_scalar_prefetch=1,
-            grid=(1,),
-            in_specs=[
-                full(2, TOK),
-                full(2, TOK),
-                pl.BlockSpec((TOK, COL), lambda i, s: (0, s[0])),
-                pl.BlockSpec((TOK, COL), lambda i, s: (0, s[0])),
-            ],
-            out_specs=[full(NZ, 2, CAP, COL)] * 2,
-        ),
-        out_shape=[out, out],
-        name="dispatch",
-        cost_estimate=pl.CostEstimate(flops=10**8, bytes_accessed=10**6, transcendentals=0),
-    )(where, ids, w, tokens, cotangent)
+        where,
+        (ids, w, tokens, cotangent),
+        [full(2, TOK), full(2, TOK), mine, mine],
+        full(NZ, 2, 2, CAP, COL),
+        jax.ShapeDtypeStruct((NZ, 2, 2, CAP, COL), BF),
+    )
 
 
 def x_of(s_ref, k):
-    return (s_ref[3] + k) & 3
+    return (s_ref[1] + k) & 3
 
 
 def pack_kernel(s_ref, wg_ref, wu_ref, wd_ref, *out_refs):
@@ -141,7 +123,7 @@
 
 
 def features(x_ref, which, rows):
-    return jnp.concatenate([x_ref[y, :, which].reshape(rows, COL) for y in range(4)], axis=1)
+    return jnp.concatenate([x_ref[:, y, :, which].reshape(rows, COL) for y in range(4)], axis=1)
 
 
 def pre_kernel(s_ref, x_ref, w_ref, out_ref, wgu, wdd):
@@ -166,6 +148,7 @@
 
 PRE = RB + RB // 2
 ACT = PRE + EXT
+HOME = RB // 2 + EXT
 
 
 def pre_activations(where, x, w):
@@ -174,7 +157,7 @@
         where,
         (x, w),
         [
-            pl.BlockSpec((4, NZ // BLK, 2, 2 * CAP, COL), lambda i, s: (0, i, 0, 0, 0)),
+            pl.BlockSpec((2, 4, NZ // BLK, 2, CAP, COL), lambda i, s: (0, 0, i, 0, 0, 0)),
             full(4, 4, 3 * HID, COL),
         ],
         pl.BlockSpec((4, 1, PRE, COL), lambda i, s: (0, i, 0, 0)),
@@ -204,8 +187,8 @@
     grads = jnp.where(low_half, back * up * sigma * (1.0 + gate * (1.0 - sigma)), back * silu).astype(BF)
     weighted = jnp.where(low, hidden[: RB // 2], hidden[RB // 2 :]).astype(BF)
     total = jnp.sum(jnp.where(low_half, hidden * back, 0.0), axis=1, keepdims=True)
-    spread = jnp.where((lane & 31) == (iota((RB, COL), 0) & 31), total, 0.0)
-    group = (iota((EXT, RB), 0) == (iota((EXT, RB), 1) >> 5)).astype(F32)
+    spread = jnp.where((lane & 15) == (iota((RB, COL), 0) & 15), total, 0.0)
+    group = (iota((EXT, RB), 0) == (iota((EXT, RB), 1) >> 4)).astype(F32)
     extra = two_parts(dot(group, spread, 1, 0, lax.Precision.HIGHEST))
     for x in range(4):
         g_ref[x, 0, :RB] = grads
@@ -251,10 +234,13 @@
     parts = g_ref[0, 0, PRE:].astype(F32)
     for x in range(1, 4):
         parts = parts + g_ref[x, 0, PRE:].astype(F32)
-    extra = two_parts(one_sum(parts))
-    for y in range(4):
-        out_ref[y, 0, :RB] = pieces[:, y * COL : (y + 1) * COL]
-        out_ref[y, 0, RB:] = extra
+    sums = one_sum(parts)
+    half = RB // 2
+    for core in range(2):
+        extra = two_parts(sums if core == 0 else pltpu.roll(sums, EXT // 2, 0))
+        for y in range(4):
+            out_ref[core, y, 0, :half] = pieces[core * half : (core + 1) * half, y * COL : (y + 1) * COL]
+            out_ref[core, y, 0, half:] = extra
 
 
 def back(where, g, w):
@@ -263,8 +249,8 @@
         where,
         (g, w),
         [pl.BlockSpec((4, 1, ACT, COL), lambda i, s: (0, i, 0, 0)), full(4, 4, 3 * HID, COL)],
-        pl.BlockSpec((4, 1, RB + EXT, COL), lambda i, s: (0, i, 0, 0)),
-        jax.ShapeDtypeStruct((4, BLK, RB + EXT, COL), BF),
+        pl.BlockSpec((2, 4, 1, HOME, COL), lambda i, s: (0, 0, i, 0, 0)),
+        jax.ShapeDtypeStruct((2, 4, BLK, HOME, COL), BF),
         [pltpu.VMEM((4 * COL, 4 * COL), BF)],
         grid=BLK,
         vmem=SMALL,
@@ -272,7 +258,9 @@
 
 
 def weights_kernel(s_ref, x_ref, g_ref, own_ref, *out_refs):
-    tok, cot = features(x_ref, 0, ROWS), features(x_ref, 1, ROWS)
+    near = NZ // BLK
+    blocks = [x_ref.at[:, :, b * near : (b + 1) * near] for b in range(BLK)]
+    tok, cot = (jnp.concatenate([features(b, which, RB) for b in blocks], axis=0) for which in range(2))
     for k, out_ref in enumerate((own_ref, *out_refs)):
         owner = x_of(s_ref, k)
         grads = jnp.concatenate([g_ref[owner, b, :RB] for b in range(BLK)], axis=0)
@@ -292,7 +280,7 @@
         weights_kernel,
         where,
         (x, g),
-        [full(4, NZ, 2, 2 * CAP, COL), full(4, BLK, ACT, COL)],
+        [full(2, 4, NZ, 2, CAP, COL), full(4, BLK, ACT, COL)],
         [full(*shape)] * 4,
         [jax.ShapeDtypeStruct(shape, F32)] + [jax.ShapeDtypeStruct(shape, BF)] * 3,
         flops=4 * 10**9,
@@ -323,76 +311,60 @@
     )
 
 
-def total_kernel(p_ref, out_ref):
-    rows = p_ref[0, 0].astype(F32)
-    for y in range(1, 4):
-        rows = rows + p_ref[y, 0].astype(F32)
-    out_ref[:, : 2 * CAP] = rows[:RB].astype(BF).reshape(NZ // BLK, 2 * CAP, COL)
-    extra = two_parts(one_sum(rows[RB:])).astype(F32)
+def total_kernel(s_ref, p_ref, out_ref):
+    half, sums = RB // 2, []
+    for core in range(2):
+        rows = p_ref[core, 0, 0].astype(F32)
+        for y in range(1, 4):
+            rows = rows + p_ref[core, y, 0].astype(F32)
+        out_ref[:, core * CAP : (core + 1) * CAP] = rows[:half].astype(BF).reshape(NZ // BLK, CAP, COL)
+        sums.append(one_sum(rows[half:]))
+    extra = two_parts(jnp.where((iota((EXT, COL), 1) & 31) < 16, *sums)).astype(F32)
     for k in range(NZ // BLK):
         out_ref[k, 2 * CAP :] = jnp.broadcast_to(extra[k : k + 1], (EXT, COL)).astype(BF)
 
 
-def total(part):
-    return pl.pallas_call(
+def total(where, part):
+    return call(
         total_kernel,
-        grid=(BLK,),
-        in_specs=[pl.BlockSpec((4, 1, RB + EXT, COL), lambda i: (0, i, 0, 0))],
-        out_specs=pl.BlockSpec((NZ // BLK, 2 * CAP + EXT, COL), lambda i: (i, 0, 0)),
-        out_shape=jax.ShapeDtypeStruct((NZ, 2 * CAP + EXT, COL), BF),
-        compiler_params=pltpu.CompilerParams(vmem_limit_bytes=4 * 2**20),
-        name="total",
-        cost_estimate=pl.CostEstimate(flops=10**7, bytes_accessed=2 * 10**6, transcendentals=0),
-    )(part)
-
-
-def combine_kernel(s_ref, ids_ref, w_ref, own_ref, other_ref, tok_ref, route_ref):
-    core = s_ref[1]
-    first, second, rank, _, chosen = routing(ids_ref, core)
+        where,
+        (part,),
+        [pl.BlockSpec((2, 4, 1, HOME, COL), lambda i, s: (0, 0, i, 0, 0))],
+        pl.BlockSpec((NZ // BLK, 2 * CAP + EXT, COL), lambda i, s: (i, 0, 0)),
+        jax.ShapeDtypeStruct((NZ, 2 * CAP + EXT, COL), BF),
+        grid=BLK,
+        vmem=4 * 2**20,
+    )
+
+
+def combine_kernel(s_ref, ids_ref, w_ref, home_ref, tok_ref, route_ref):
+    first, second, rank, _, chosen = routing(ids_ref)
     pick = jnp.where(chosen, 1.0, 0.0).astype(BF)
-    half = NZ * CAP
-    own = own_ref[:, :CAP].reshape(half, COL)
-    other = other_ref[:, :CAP].reshape(half, COL)
-    tok_ref[...] = (dot(pick[:half], own, 0, 0) + dot(pick[half:], other, 0, 0)).astype(BF)
-    own_sums = own_ref[:, 2 * CAP :].reshape(NZ * EXT, COL)
-    other_sums = other_ref[:, CAP:].reshape(NZ * EXT, COL)
+    rows = home_ref[:, : 2 * CAP].reshape(2 * NZ * CAP, COL)
+    tok_ref[...] = dot(pick, rows, 0, 0).astype(BF)
+    sums = home_ref[:, 2 * CAP :].reshape(NZ * EXT, COL)
     row = iota((NZ * EXT, TOK), 0)
-    leads = (row & 7) == 0
-    chip = row >> 3
     lane = iota((COL, TOK), 0)
     w = w_ref[...].astype(F32)
     for k, member in enumerate((first, second)):
         ids = ids_ref[k : k + 1, :]
-        at = jnp.sum(member * rank, axis=0, keepdims=True).astype(I32)
-        mine = (leads & (ids == 2 * chip + core)).astype(BF)
-        theirs = (leads & (ids == 2 * chip + 1 - core)).astype(BF)
-        near = dot(own_sums, mine, 0, 0)
-        far = dot(other_sums, theirs, 0, 0)
-        near = jnp.where((lane == at) | (lane == at + 32), near, 0.0)
-        far = jnp.where((lane == at + 16) | (lane == at + 48), far, 0.0)
-        route_ref[k : k + 1, :] = jnp.sum(near + far, axis=0, keepdims=True) / w[k : k + 1, :]
-
-
-def combine(where, ids, w, own, other):
-    full = lambda *shape: pl.BlockSpec(shape, lambda i, s: (0,) * len(shape))
-    return pl.pallas_call(
+        at = jnp.sum(member * rank, axis=0, keepdims=True).astype(I32) + 16 * (ids & 1)
+        chip = (((row & 7) == 0) & ((row >> 3) == (ids >> 1))).astype(BF)
+        found = dot(sums, chip, 0, 0)
+        found = jnp.where((lane == at) | (lane == at + 32), found, 0.0)
+        route_ref[k : k + 1, :] = jnp.sum(found, axis=0, keepdims=True) / w[k : k + 1, :]
+
+
+def combine(where, ids, w, home):
+    return call(
         combine_kernel,
-        grid_spec=pltpu.PrefetchScalarGridSpec(
-            num_scalar_prefetch=1,
-            grid=(1,),
-            in_specs=[
-                full(2, TOK),
-                full(2, TOK),
-                full(NZ, 2 * CAP + EXT, COL),
-                full(NZ, CAP + EXT, COL),
-            ],
-            out_specs=[full(TOK, COL), full(2, TOK)],
-        ),
-        out_shape=[jax.ShapeDtypeStruct((TOK, COL), BF), jax.ShapeDtypeStruct((2, TOK), F32)],
-        compiler_params=pltpu.CompilerParams(vmem_limit_bytes=4 * 2**20),
-        name="combine",
-        cost_estimate=pl.CostEstimate(flops=10**8, bytes_accessed=10**6, transcendentals=0),
-    )(where, ids, w, own, other)
+        where,
+        (ids, w, home),
+        [full(2, TOK), full(2, TOK), full(NZ, 2 * CAP + EXT, COL)],
+        [full(TOK, COL), full(2, TOK)],
+        [jax.ShapeDtypeStruct((TOK, COL), BF), jax.ShapeDtypeStruct((2, TOK), F32)],
+        vmem=4 * 2**20,
+    )
 
 
 def exchange(x, axis):
@@ -415,27 +387,24 @@
 
 
 def per_device(tokens, cotangent, expert_ids, route_weight, gate_weight, up_weight, down_weight):
-    y, x, core = lax.axis_index("y"), lax.axis_index("x"), lax.axis_index("c")
-    where = jnp.stack([y * 4 + x, core, y, x]).astype(I32)
+    y, x = lax.axis_index("y"), lax.axis_index("x")
+    where = jnp.stack([y * 4 + x, x]).astype(I32)
     ids, w = expert_ids.T, route_weight.T
-    own, other = dispatch(where, ids, w, tokens, cotangent)
-    got = shifted(other, "c", 1)
-    mine = jnp.stack([own, got], axis=2).reshape(NZ, 2, 2 * CAP, COL)
-    mine = exchange(mine, "z")
+    mine = exchange(dispatch(where, ids, w, tokens, cotangent), "z")
     row_w = row_weights(where, gate_weight, up_weight, down_weight)
-    rows = exchange(copies(mine, 4), "y")
+    both = copies(mine.transpose(1, 0, 2, 3, 4), 4).transpose(1, 0, 2, 3, 4, 5)
+    rows = exchange(both.reshape(8, NZ, 2, CAP, COL), ("c", "y")).reshape(both.shape)
     pre = pre_activations(where, rows, row_w)
     pre = exchange(pre, "x")
     g = activations(where, pre)
     g = exchange(g, "x")
     part = back(where, g, row_w)
-    sums = exchange(part, "y")
+    sums = exchange(part.reshape(8, BLK, HOME, COL), ("c", "y")).reshape(part.shape)
     kept, *sent = weights(where, rows, g)
-    home = exchange(total(sums), "z")
+    home = exchange(total(where, sums), "z")
     moved = [shifted(part, "x", k + 1) for k, part in enumerate(sent)]
     gate_grad, up_grad, down_grad = assemble(where, (kept, *moved))
-    far = shifted(home[:, CAP:], "c", 1)
-    tokens_grad, route_grad = combine(where, ids, w, home, far)
+    tokens_grad, route_grad = combine(where, ids, w, home)
     return tokens_grad, route_grad.T, gate_grad, up_grad, down_grad
 
 

time: 148 us -> 151 us (1.020)
  starting transfers between devices: 56.2 us -> 34.7 us
  blocking collectives: 57.2 us -> 74.4 us
  waiting for transfers between devices: 4.74 us -> 12.8 us
    all_to_all x4, blocking collectives: 57.2 us -> 74.4 us  [exchange(): return lax.all_to_all(x, axis, split_axis=0, concat_axis=0, tiled=True)]
    ppermute x8 -> x6, starting transfers between devices: 36.1 us -> 19.1 us  [shifted(): return lax.ppermute(x, axis, [(i, (i + by) % n) for i in range(n)])]
    ppermute x8 -> x6, waiting for transfers between devices: 4.73 us -> 12.8 us  [shifted(): return lax.ppermute(x, axis, [(i, (i + by) % n) for i in range(n)])]
    pallas_call x6 -> x9, Pallas kernels: 16.5 us -> 23.1 us  [call(): pl.pallas_call(kernel, grid_spec=pltpu.PrefetchScalarGridSpec(num_scalar_...]
    pallas_call x3 -> x0, Pallas kernels: 6.06 us -> none  [the longest x1 2.59 us: dispatch(): pl.pallas_call(dispatch_kernel, grid_spec=pltpu.PrefetchScalarGridSpec(nu...]
    all_to_all x2, starting transfers between devices: 20.1 us -> 15.5 us  [exchange(): return lax.all_to_all(x, axis, split_axis=0, concat_axis=0, tiled=True)]
  transfers between devices with their start and end apart: 10 -> 8, of which waited for: 3 -> 5; matrix products, arithmetic and copies ran while one was open for 1% -> 1% of each run, Pallas kernels for 7% -> 7%
where the time goes in v4:
time: 151 us; the launch traced here: 150 us
  blocking collectives  74.4 us (49%)
  starting transfers between devices  34.7 us (23%)
  Pallas kernels  23.1 us (15%)
  waiting for transfers between devices  12.8 us (8%)
  local copies, waits for them, and re-layouts  2.47 us (2%)
  other arithmetic  1.62 us (1%)
    all_to_all x4, blocking collectives, exchange(): return lax.all_to_all(x, axis, split_axis=0, concat_axis=0, tiled=True)  74.4 us
    pallas_call x9, Pallas kernels, call(): pl.pallas_call(kernel, grid_spec=pltpu.PrefetchScalarGridSpec(num_scalar_...  23.1 us
    ppermute x6, starting transfers between devices, shifted(): return lax.ppermute(x, axis, [(i, (i + by) % n) for i in range(n)])  19.1 us
    all_to_all x2, starting transfers between devices, exchange(): return lax.all_to_all(x, axis, split_axis=0, concat_axis=0, tiled=True)  15.5 us
    ppermute x6, waiting for transfers between devices, shifted(): return lax.ppermute(x, axis, [(i, (i + by) % n) for i in range(n)])  12.8 us
  transfers between devices with their start and end apart: 8, of which 5 were waited for; matrix products, arithmetic and copies ran while one was open for 1% of the time, Pallas kernels for 7%

profile of v4, /device:TPU:1, one launch (start us, length us, event | category | flops | bytes accessed | tf_op | source)
XLA Modules:
  0.0 149.9 jit_solution(12360044215732695668)
XLA Ops:
  0.6 0.6 pad_add_fusion.s_ref
  1.2 2.6 %shard_map.110 = bf16[16,2,2,16,128]{4,3,2,1,0:T(8,128)(2,1)} custom-call(s32[2]{0:T(128)} %pad_add_fusion.s_ref, s32[2,128]{1,0:T(2,128)} %bitcast.18, bf16[2,128]{1,0:T(2,128)(2,1)} %bitcast.20, bf16[128,2048]{1,0:T(8,128)(2,1)} %tok_ref.1, bf16[128,2048]{1,0:T(8,128)(2,1)} %cot_ref.1), custom_call_target="tpu_custom_call" | custom-call | flops 100000000 | bytes 2000000 | tf_op jit(solution)/shard_map/pallas_call | solution.py:94
  3.9 29.5 %all_to_all.30 = bf16[16,2,2,16,128]{4,3,2,1,0:T(8,128)(2,1)S(1)} all-to-all(bf16[16,2,2,16,128]{4,3,2,1,0:T(8,128)(2,1)} %shard_map.110), channel_id=1, replica_groups=mesh['z'=16,'c'=2,'y'=4,'x'=4] {'z'}, dimensions={0} | all-to-all | bytes 524288 | tf_op jit(solution)/shard_map/all_to_all | solution.py:371
  33.4 1.2 transpose.19
  34.6 10.0 %all-to-all-start.1 = ((bf16[8,16,2,16,128]{4,3,2,1,0:T(8,128)(2,1)}), bf16[8,16,2,16,128]{4,3,2,1,0:T(8,128)(2,1)S(1)}, u32[]{:S(2)}, u32[]{:S(2)}) async-start(bf16[8,16,2,16,128]{4,3,2,1,0:T(8,128)(2,1)} %bitcast.5), calls=%async_computation.1 | async-start | bytes 2097152 | tf_op jit(solution)/shard_map/all_to_all | solution.py:371
  44.6 2.8 %shard_map.111 = (bf16[4,192,128]{2,1,0:T(8,128)(2,1)}, bf16[4,192,128]{2,1,0:T(8,128)(2,1)}, bf16[4,192,128]{2,1,0:T(8,128)(2,1)}, bf16[4,192,128]{2,1,0:T(8,128)(2,1)}) custom-call(s32[2]{0:T(128)} %pad_add_fusion.s_ref, bf16[1,64,2048]{2,1,0:T(8,128)(2,1)} %wg_ref.1, bf16[1,64,2048]{2,1,0:T(8,128)(2,1)} %wu_ref.1, bf16[1,64,2048]{2,1,0:T(8,128)(2,1)} %wd_ref.1), custom_call_target="tpu_custom_call" | custom-call | flops 100000000 | bytes 2000000 | tf_op jit(solution)/shard_map/pallas_call | solution.py:94
  47.5 3.1 %collective-permute-start = (bf16[4,192,128]{2,1,0:T(8,128)(2,1)}, bf16[4,192,128]{2,1,0:T(8,128)(2,1)S(1)}, u32[]{:S(2)}, u32[]{:S(2)}) collective-permute-start(bf16[4,192,128]{2,1,0:T(8,128)(2,1)} %get-tuple-element.19), channel_id=1, source_target_pairs={{0,1},{1,2},{2,3},{3,0},{4,5},{5,6},{6,7},{7,4},{8,9},{9,10},{10,1... | collective-permute-start | bytes 589832 | tf_op jit(solution)/shard_map/ppermute | solution.py:380
  50.6 4.4 %collective-permute-start.1 = (bf16[4,192,128]{2,1,0:T(8,128)(2,1)}, bf16[4,192,128]{2,1,0:T(8,128)(2,1)S(1)}, u32[]{:S(2)}, u32[]{:S(2)}) collective-permute-start(bf16[4,192,128]{2,1,0:T(8,128)(2,1)} %get-tuple-element.20), channel_id=1, source_target_pairs={{0,2},{1,3},{2,0},{3,1},{4,6},{5,7},{6,4},{7,5},{8,10},{9,11},{10,... | collective-permute-start | bytes 589832 | tf_op jit(solution)/shard_map/ppermute | solution.py:380
  55.0 3.1 %collective-permute-start.2 = (bf16[4,192,128]{2,1,0:T(8,128)(2,1)}, bf16[4,192,128]{2,1,0:T(8,128)(2,1)S(1)}, u32[]{:S(2)}, u32[]{:S(2)}) collective-permute-start(bf16[4,192,128]{2,1,0:T(8,128)(2,1)} %get-tuple-element.21), channel_id=1, source_target_pairs={{0,3},{1,0},{2,1},{3,2},{4,7},{5,4},{6,5},{7,6},{8,11},{9,8},{10,9... | collective-permute-start | bytes 589832 | tf_op jit(solution)/shard_map/ppermute | solution.py:380
  58.0 0.0 collective-permute-done
  58.0 4.4 %collective-permute-done.1 = bf16[4,192,128]{2,1,0:T(8,128)(2,1)S(1)} collective-permute-done((bf16[4,192,128]{2,1,0:T(8,128)(2,1)}, bf16[4,192,128]{2,1,0:T(8,128)(2,1)S(1)}, u32[]{:S(2)}, u32[]{:S(2)}) %collective-permute-start.1) | collective-permute-done | bytes 196640 | tf_op jit(solution)/shard_map/ppermute | solution.py:380
  62.4 1.4 collective-permute-done.2
  63.8 1.0 pad_maximum_fusion.w_ref
  64.8 0.0 copy-start.2
  64.8 0.0 all-to-all-done.1
  64.8 0.0 copy-start
  64.8 0.6 copy-done.2
  65.4 2.8 %shard_map.112 = bf16[4,4,192,128]{3,2,1,0:T(8,128)(2,1)S(1)} custom-call(s32[2]{0:T(128)S(1)} %copy-done.2, bf16[2,4,16,2,16,128]{5,4,3,2,1,0:T(8,128)(2,1)S(1)} %bitcast.14, bf16[4,4,192,128]{3,2,1,0:T(8,128)(2,1)S(1)} %pad_maximum_fusion.w_ref), custom_call_target="tpu_custom_call" | custom-call | flops 100000000 | bytes 2000000 | tf_op jit(solution)/shard_map/pallas_call | solution.py:94
  68.3 0.0 copy-done
  68.3 14.4 %all_to_all.31.p_ref = bf16[4,4,192,128]{3,2,1,0:T(8,128)(2,1)S(1)} all-to-all(bf16[4,4,192,128]{3,2,1,0:T(8,128)(2,1)S(1)} %shard_map.112), channel_id=1, replica_groups=mesh['z'=16,'c'=2,'y'=4,'x'=4] {'x'}, dimensions={0} | all-to-all | bytes 1572864 | tf_op jit(solution)/shard_map/all_to_all | solution.py:371
  82.7 2.1 %shard_map.113 = bf16[4,4,200,128]{3,2,1,0:T(8,128)(2,1)S(1)} custom-call(s32[2]{0:T(128)S(1)} %copy-done.2, bf16[4,4,192,128]{3,2,1,0:T(8,128)(2,1)S(1)} %all_to_all.31.p_ref), custom_call_target="tpu_custom_call" | custom-call | flops 100000000 | bytes 2000000 | tf_op jit(solution)/shard_map/pallas_call | solution.py:94
  84.8 12.5 %all_to_all.32.g_ref = bf16[4,4,200,128]{3,2,1,0:T(8,128)(2,1)S(1)} all-to-all(bf16[4,4,200,128]{3,2,1,0:T(8,128)(2,1)S(1)} %shard_map.113), channel_id=1, replica_groups=mesh['z'=16,'c'=2,'y'=4,'x'=4] {'x'}, dimensions={0} | all-to-all | bytes 1638400 | tf_op jit(solution)/shard_map/all_to_all | solution.py:371
  97.3 0.0 copy-start.1
  97.3 1.8 %shard_map.114 = bf16[2,4,4,72,128]{4,3,2,1,0:T(8,128)(2,1)S(1)} custom-call(s32[2]{0:T(128)S(1)} %copy-done.2, bf16[4,4,200,128]{3,2,1,0:T(8,128)(2,1)S(1)} %all_to_all.32.g_ref, bf16[4,4,192,128]{3,2,1,0:T(8,128)(2,1)S(1)} %pad_maximum_fusion.w_ref), custom_call_target="tpu_custom_call" | custom-call | flops 100000000 | bytes 2000000 | tf_op jit(solution)/shard_map/pallas_call | solution.py:94
  99.1 0.0 copy-done.1
  99.1 18.0 %all_to_all.33 = bf16[8,4,72,128]{3,2,1,0:T(8,128)(2,1)S(1)} all-to-all(bf16[8,4,72,128]{3,2,1,0:T(8,128)(2,1)S(1)} %bitcast.16), channel_id=1, replica_groups=mesh['z'=16,'c'=2,'y'=4,'x'=4] {'c','y'}, dimensions={0} | all-to-all | bytes 1179648 | tf_op jit(solution)/shard_map/all_to_all | solution.py:371
  117.1 2.3 %shard_map.115 = bf16[16,40,128]{2,1,0:T(8,128)(2,1)} custom-call(s32[2]{0:T(128)S(1)} %copy-done.2, bf16[2,4,4,72,128]{4,3,2,1,0:T(8,128)(2,1)S(1)} %bitcast.17), custom_call_target="tpu_custom_call" | custom-call | flops 100000000 | bytes 2000000 | tf_op jit(solution)/shard_map/pallas_call | solution.py:94
  119.4 5.5 %all-to-all-start.5 = ((bf16[16,40,128]{2,1,0:T(8,128)(2,1)}), bf16[16,40,128]{2,1,0:T(8,128)(2,1)S(1)}, u32[]{:S(2)}, u32[]{:S(2)}) async-start(bf16[16,40,128]{2,1,0:T(8,128)(2,1)} %shard_map.115), calls=%async_computation.5 | async-start | bytes 327680 | tf_op jit(solution)/shard_map/all_to_all | solution.py:371
  125.0 3.6 %shard_map.117 = (f32[192,512]{1,0:T(8,128)}, bf16[192,512]{1,0:T(8,128)(2,1)}, bf16[192,512]{1,0:T(8,128)(2,1)}, bf16[192,512]{1,0:T(8,128)(2,1)}) custom-call(s32[2]{0:T(128)} %pad_add_fusion.s_ref, bf16[2,4,16,2,16,128]{5,4,3,2,1,0:T(8,128)(2,1)} %bitcast.15, bf16[4,4,200,128]{3,2,1,0:T(8,128)(2,1)} %copy-done.1), custom_call_target="tpu_custom_call" | custom-call | flops 4000000000 | bytes 2000000 | tf_op jit(solution)/shard_map/pallas_call | solution.py:94
  128.6 2.2 %collective-permute-start.3 = (bf16[192,512]{1,0:T(8,128)(2,1)}, bf16[192,512]{1,0:T(8,128)(2,1)S(1)}, u32[]{:S(2)}, u32[]{:S(2)}) collective-permute-start(bf16[192,512]{1,0:T(8,128)(2,1)} %get-tuple-element.25), channel_id=1, source_target_pairs={{0,1},{1,2},{2,3},{3,0},{4,5},{5,6},{6,7},{7,4},{8,9},{9,10},{10,1... | collective-permute-start | bytes 589832 | tf_op jit(solution)/shard_map/ppermute | solution.py:380
  130.8 3.7 %collective-permute-start.4 = (bf16[192,512]{1,0:T(8,128)(2,1)}, bf16[192,512]{1,0:T(8,128)(2,1)S(1)}, u32[]{:S(2)}, u32[]{:S(2)}) collective-permute-start(bf16[192,512]{1,0:T(8,128)(2,1)} %get-tuple-element.26), channel_id=1, source_target_pairs={{0,2},{1,3},{2,0},{3,1},{4,6},{5,7},{6,4},{7,5},{8,10},{9,11},{10,... | collective-permute-start | bytes 589832 | tf_op jit(solution)/shard_map/ppermute | solution.py:380
  134.5 2.7 %collective-permute-start.5 = (bf16[192,512]{1,0:T(8,128)(2,1)}, bf16[192,512]{1,0:T(8,128)(2,1)S(1)}, u32[]{:S(2)}, u32[]{:S(2)}) collective-permute-start(bf16[192,512]{1,0:T(8,128)(2,1)} %get-tuple-element.27), channel_id=1, source_target_pairs={{0,3},{1,0},{2,1},{3,2},{4,7},{5,4},{6,5},{7,6},{8,11},{9,8},{10,9... | collective-permute-start | bytes 589832 | tf_op jit(solution)/shard_map/ppermute | solution.py:380
  137.2 1.1 collective-permute-done.3.refs_1_
  138.2 0.0 copy-start.6
  138.3 3.1 %collective-permute-done.4.refs_2_ = bf16[192,512]{1,0:T(8,128)(2,1)S(1)} collective-permute-done((bf16[192,512]{1,0:T(8,128)(2,1)}, bf16[192,512]{1,0:T(8,128)(2,1)S(1)}, u32[]{:S(2)}, u32[]{:S(2)}) %collective-permute-start.4) | collective-permute-done | bytes 196640 | tf_op jit(solution)/shard_map/ppermute | solution.py:380
  141.3 2.9 %collective-permute-done.5.refs_3_ = bf16[192,512]{1,0:T(8,128)(2,1)S(1)} collective-permute-done((bf16[192,512]{1,0:T(8,128)(2,1)}, bf16[192,512]{1,0:T(8,128)(2,1)S(1)}, u32[]{:S(2)}, u32[]{:S(2)}) %collective-permute-start.5) | collective-permute-done | bytes 196640 | tf_op jit(solution)/shard_map/ppermute | solution.py:380
  144.2 0.0 copy-start.8
  144.2 0.0 copy-done.6
  144.2 0.0 copy-done.7
  144.2 0.7 copy-done.8
  144.9 0.0 copy-start.3
  144.9 0.0 copy-start.4
  144.9 3.3 %shard_map.118 = (f32[1,64,2048]{2,1,0:T(8,128)}, f32[1,64,2048]{2,1,0:T(8,128)}, f32[1,64,2048]{2,1,0:T(8,128)}) custom-call(s32[2]{0:T(128)} %pad_add_fusion.s_ref, f32[192,512]{1,0:T(8,128)} %get-tuple-element.24.refs_0_, bf16[192,512]{1,0:T(8,128)(2,1)} %copy-done.6, bf16[192,512]{1,0:T(8,128)(2,1)} %copy-done.7, bf16[192,512]{1,0:T(8,128)(2,1)} %copy-done.8), custom_call_target="tpu_custom_call" | custom-call | flops 1000000000 | bytes 2000000 | tf_op jit(solution)/shard_map/pallas_call | solution.py:94
  148.2 0.0 all-to-all-done.5.home_ref
  148.2 0.0 copy-done.3
  148.2 0.0 copy-done.4
  148.2 0.0 copy-done.5
  148.3 1.7 %shard_map.116 = (bf16[128,128]{1,0:T(8,128)(2,1)}, f32[2,128]{1,0:T(2,128)}) custom-call(s32[2]{0:T(128)S(1)} %copy-done.3, s32[2,128]{1,0:T(2,128)S(1)} %bitcast.19, bf16[2,128]{1,0:T(2,128)(2,1)S(1)} %bitcast.21, bf16[16,40,128]{2,1,0:T(8,128)(2,1)S(1)} %all-to-all-done.5.home_ref), custom_call_target="tpu_custom_call" | custom-call | flops 100000000 | bytes 2000000 | tf_op jit(solution)/shard_map/pallas_call | solution.py:94
  (3 shorter events, 0.0 us)
Async XLA Ops:
  34.6 30.2 %all-to-all-start.1 = ((bf16[8,16,2,16,128]{4,3,2,1,0:T(8,128)(2,1)}), bf16[8,16,2,16,128]{4,3,2,1,0:T(8,128)(2,1)S(1)}, u32[]{:S(2)}, u32[]{:S(2)}) async-start(bf16[8,16,2,16,128]{4,3,2,1,0:T(8,128)(2,1)} %bitcast.5), calls=%async_computation.1 | async-start | bytes 2097152 | tf_op jit(solution)/shard_map/all_to_all | solution.py:371
  47.5 10.6 %collective-permute-start = (bf16[4,192,128]{2,1,0:T(8,128)(2,1)}, bf16[4,192,128]{2,1,0:T(8,128)(2,1)S(1)}, u32[]{:S(2)}, u32[]{:S(2)}) collective-permute-start(bf16[4,192,128]{2,1,0:T(8,128)(2,1)} %get-tuple-element.19), channel_id=1, source_target_pairs={{0,1},{1,2},{2,3},{3,0},{4,5},{5,6},{6,7},{7,4},{8,9},{9,10},{10,1... | collective-permute-start | bytes 589832 | tf_op jit(solution)/shard_map/ppermute | solution.py:380
  50.6 11.9 %collective-permute-start.1 = (bf16[4,192,128]{2,1,0:T(8,128)(2,1)}, bf16[4,192,128]{2,1,0:T(8,128)(2,1)S(1)}, u32[]{:S(2)}, u32[]{:S(2)}) collective-permute-start(bf16[4,192,128]{2,1,0:T(8,128)(2,1)} %get-tuple-element.20), channel_id=1, source_target_pairs={{0,2},{1,3},{2,0},{3,1},{4,6},{5,7},{6,4},{7,5},{8,10},{9,11},{10,... | collective-permute-start | bytes 589832 | tf_op jit(solution)/shard_map/ppermute | solution.py:380
  55.0 8.8 %collective-permute-start.2 = (bf16[4,192,128]{2,1,0:T(8,128)(2,1)}, bf16[4,192,128]{2,1,0:T(8,128)(2,1)S(1)}, u32[]{:S(2)}, u32[]{:S(2)}) collective-permute-start(bf16[4,192,128]{2,1,0:T(8,128)(2,1)} %get-tuple-element.21), channel_id=1, source_target_pairs={{0,3},{1,0},{2,1},{3,2},{4,7},{5,4},{6,5},{7,6},{8,11},{9,8},{10,9... | collective-permute-start | bytes 589832 | tf_op jit(solution)/shard_map/ppermute | solution.py:380
  64.8 0.6 copy-start.2
  64.8 3.4 %copy-start = (bf16[8,16,2,16,128]{4,3,2,1,0:T(8,128)(2,1)}, bf16[8,16,2,16,128]{4,3,2,1,0:T(8,128)(2,1)S(1)}, u32[]{:S(2)}) copy-start(bf16[8,16,2,16,128]{4,3,2,1,0:T(8,128)(2,1)S(1)} %all-to-all-done.1) | copy-start | bytes 3145732
  97.3 1.8 %copy-start.1 = (bf16[4,4,200,128]{3,2,1,0:T(8,128)(2,1)}, bf16[4,4,200,128]{3,2,1,0:T(8,128)(2,1)S(1)}, u32[]{:S(2)}) copy-start(bf16[4,4,200,128]{3,2,1,0:T(8,128)(2,1)S(1)} %all_to_all.32.g_ref) | copy-start | bytes 2457604
  119.4 28.8 %all-to-all-start.5 = ((bf16[16,40,128]{2,1,0:T(8,128)(2,1)}), bf16[16,40,128]{2,1,0:T(8,128)(2,1)S(1)}, u32[]{:S(2)}, u32[]{:S(2)}) async-start(bf16[16,40,128]{2,1,0:T(8,128)(2,1)} %shard_map.115), calls=%async_computation.5 | async-start | bytes 327680 | tf_op jit(solution)/shard_map/all_to_all | solution.py:371
  128.6 9.7 %collective-permute-start.3 = (bf16[192,512]{1,0:T(8,128)(2,1)}, bf16[192,512]{1,0:T(8,128)(2,1)S(1)}, u32[]{:S(2)}, u32[]{:S(2)}) collective-permute-start(bf16[192,512]{1,0:T(8,128)(2,1)} %get-tuple-element.25), channel_id=1, source_target_pairs={{0,1},{1,2},{2,3},{3,0},{4,5},{5,6},{6,7},{7,4},{8,9},{9,10},{10,1... | collective-permute-start | bytes 589832 | tf_op jit(solution)/shard_map/ppermute | solution.py:380
  130.8 10.6 %collective-permute-start.4 = (bf16[192,512]{1,0:T(8,128)(2,1)}, bf16[192,512]{1,0:T(8,128)(2,1)S(1)}, u32[]{:S(2)}, u32[]{:S(2)}) collective-permute-start(bf16[192,512]{1,0:T(8,128)(2,1)} %get-tuple-element.26), channel_id=1, source_target_pairs={{0,2},{1,3},{2,0},{3,1},{4,6},{5,7},{6,4},{7,5},{8,10},{9,11},{10,... | collective-permute-start | bytes 589832 | tf_op jit(solution)/shard_map/ppermute | solution.py:380
  134.5 9.8 %collective-permute-start.5 = (bf16[192,512]{1,0:T(8,128)(2,1)}, bf16[192,512]{1,0:T(8,128)(2,1)S(1)}, u32[]{:S(2)}, u32[]{:S(2)}) collective-permute-start(bf16[192,512]{1,0:T(8,128)(2,1)} %get-tuple-element.27), channel_id=1, source_target_pairs={{0,3},{1,0},{2,1},{3,2},{4,7},{5,4},{6,5},{7,6},{8,11},{9,8},{10,9... | collective-permute-start | bytes 589832 | tf_op jit(solution)/shard_map/ppermute | solution.py:380
  138.2 6.0 %copy-start.6 = (bf16[192,512]{1,0:T(8,128)(2,1)}, bf16[192,512]{1,0:T(8,128)(2,1)S(1)}, u32[]{:S(2)}) copy-start(bf16[192,512]{1,0:T(8,128)(2,1)S(1)} %collective-permute-done.3.refs_1_) | copy-start | bytes 589828
  141.3 2.9 %copy-start.7 = (bf16[192,512]{1,0:T(8,128)(2,1)}, bf16[192,512]{1,0:T(8,128)(2,1)S(1)}, u32[]{:S(2)}) copy-start(bf16[192,512]{1,0:T(8,128)(2,1)S(1)} %collective-permute-done.4.refs_2_) | copy-start | bytes 589828
  144.2 0.7 copy-start.8
  144.9 3.3 %copy-start.3 = (s32[2]{0:T(128)S(1)}, s32[2]{0:T(128)}, u32[]{:S(2)}) copy-start(s32[2]{0:T(128)} %pad_add_fusion.s_ref) | copy-start | bytes 28
  144.9 3.3 %copy-start.4 = (s32[128,2]{0,1:T(2,128)S(1)}, s32[128,2]{0,1:T(2,128)}, u32[]{:S(2)}) copy-start(s32[128,2]{0,1:T(2,128)} %param.9) | copy-start | bytes 3076
  144.9 3.3 %copy-start.5 = (bf16[128,2]{0,1:T(2,128)(2,1)S(1)}, bf16[128,2]{0,1:T(2,128)(2,1)}, u32[]{:S(2)}) copy-start(bf16[128,2]{0,1:T(2,128)(2,1)} %param.10) | copy-start | bytes 1540

commit v5 on v4

--- a/solution.py
+++ b/solution.py
@@ -17,10 +17,11 @@
 COL = 128
 HID = 64
 ROWS = 512
-BLK = 4
+BLK = 2
 RB = ROWS // BLK
 SMALL = 12 * 2**20
-EXT = 8
+EXT = 2 * NZ // BLK
+DUP = 8
 
 
 def iota(shape, dim):
@@ -126,18 +127,31 @@
     return jnp.concatenate([x_ref[:, y, :, which].reshape(rows, COL) for y in range(4)], axis=1)
 
 
-def pre_kernel(s_ref, x_ref, w_ref, out_ref, wgu, wdd):
-    @pl.when(pl.program_id(0) == 0)
-    def _():
-        for k in range(4):
-            for y in range(4):
-                cols = slice(y * COL, (y + 1) * COL)
-                wgu[k * COL : (k + 1) * COL, cols] = w_ref[k, y, : 2 * HID]
-                wdd[k * COL : k * COL + HID, cols] = w_ref[k, y, 2 * HID :]
-                wdd[k * COL + HID : (k + 1) * COL, cols] = w_ref[k, y, 2 * HID :]
-
-    pre = dot(features(x_ref, 0, RB), wgu[...], 1, 1).astype(BF)
-    back = dot(features(x_ref, 1, RB), wdd[...], 1, 1)
+def layout_kernel(s_ref, w0_ref, w1_ref, w2_ref, w3_ref, wgu_ref, wdd_ref):
+    for k, w_ref in enumerate((w0_ref, w1_ref, w2_ref, w3_ref)):
+        for y in range(4):
+            cols = slice(y * COL, (y + 1) * COL)
+            wgu_ref[k * COL : (k + 1) * COL, cols] = w_ref[y, : 2 * HID]
+            wdd_ref[k * COL : k * COL + HID, cols] = w_ref[y, 2 * HID :]
+            wdd_ref[k * COL + HID : (k + 1) * COL, cols] = w_ref[y, 2 * HID :]
+
+
+def layout(where, ws):
+    shape = (4 * COL, 4 * COL)
+    return call(
+        layout_kernel,
+        where,
+        ws,
+        [full(4, 3 * HID, COL)] * 4,
+        [full(*shape)] * 2,
+        [jax.ShapeDtypeStruct(shape, BF)] * 2,
+        vmem=SMALL,
+    )
+
+
+def pre_kernel(s_ref, x_ref, wgu_ref, wdd_ref, out_ref):
+    pre = dot(features(x_ref, 0, RB), wgu_ref[...], 1, 1).astype(BF)
+    back = dot(features(x_ref, 1, RB), wdd_ref[...], 1, 1)
     for k in range(4):
         cols = slice(k * COL, (k + 1) * COL)
         to = x_of(s_ref, -k)
@@ -151,18 +165,18 @@
 HOME = RB // 2 + EXT
 
 
-def pre_activations(where, x, w):
+def pre_activations(where, x, wgu, wdd):
     return call(
         pre_kernel,
         where,
-        (x, w),
+        (x, wgu, wdd),
         [
             pl.BlockSpec((2, 4, NZ // BLK, 2, CAP, COL), lambda i, s: (0, 0, i, 0, 0, 0)),
-            full(4, 4, 3 * HID, COL),
+            full(4 * COL, 4 * COL),
+            full(4 * COL, 4 * COL),
         ],
         pl.BlockSpec((4, 1, PRE, COL), lambda i, s: (0, i, 0, 0)),
         jax.ShapeDtypeStruct((4, BLK, PRE, COL), BF),
-        [pltpu.VMEM((4 * COL, 4 * COL), BF), pltpu.VMEM((4 * COL, 4 * COL), BF)],
         grid=BLK,
         vmem=SMALL,
     )
@@ -221,16 +235,9 @@
     return both + pltpu.roll(both, 32, 1)
 
 
-def back_kernel(s_ref, g_ref, w_ref, out_ref, w):
-    @pl.when(pl.program_id(0) == 0)
-    def _():
-        for k in range(4):
-            rows = pl.ds(pl.multiple_of(x_of(s_ref, -k) * COL, COL), COL)
-            for y in range(4):
-                w[rows, y * COL : (y + 1) * COL] = w_ref[k, y, : 2 * HID]
-
-    grads = jnp.concatenate([g_ref[x, 0, :RB] for x in range(4)], axis=1)
-    pieces = dot(grads, w[...], 1, 0).astype(BF)
+def back_kernel(s_ref, g_ref, w_ref, out_ref):
+    grads = jnp.concatenate([g_ref[x_of(s_ref, -k), 0, :RB] for k in range(4)], axis=1)
+    pieces = dot(grads, w_ref[...], 1, 0).astype(BF)
     parts = g_ref[0, 0, PRE:].astype(F32)
     for x in range(1, 4):
         parts = parts + g_ref[x, 0, PRE:].astype(F32)
@@ -248,10 +255,9 @@
         back_kernel,
         where,
         (g, w),
-        [pl.BlockSpec((4, 1, ACT, COL), lambda i, s: (0, i, 0, 0)), full(4, 4, 3 * HID, COL)],
+        [pl.BlockSpec((4, 1, ACT, COL), lambda i, s: (0, i, 0, 0)), full(4 * COL, 4 * COL)],
         pl.BlockSpec((2, 4, 1, HOME, COL), lambda i, s: (0, 0, i, 0, 0)),
         jax.ShapeDtypeStruct((2, 4, BLK, HOME, COL), BF),
-        [pltpu.VMEM((4 * COL, 4 * COL), BF)],
         grid=BLK,
         vmem=SMALL,
     )
@@ -321,7 +327,7 @@
         sums.append(one_sum(rows[half:]))
     extra = two_parts(jnp.where((iota((EXT, COL), 1) & 31) < 16, *sums)).astype(F32)
     for k in range(NZ // BLK):
-        out_ref[k, 2 * CAP :] = jnp.broadcast_to(extra[k : k + 1], (EXT, COL)).astype(BF)
+        out_ref[k, 2 * CAP :] = jnp.broadcast_to(extra[k : k + 1], (DUP, COL)).astype(BF)
 
 
 def total(where, part):
@@ -330,8 +336,8 @@
         where,
         (part,),
         [pl.BlockSpec((2, 4, 1, HOME, COL), lambda i, s: (0, 0, i, 0, 0))],
-        pl.BlockSpec((NZ // BLK, 2 * CAP + EXT, COL), lambda i, s: (i, 0, 0)),
-        jax.ShapeDtypeStruct((NZ, 2 * CAP + EXT, COL), BF),
+        pl.BlockSpec((NZ // BLK, 2 * CAP + DUP, COL), lambda i, s: (i, 0, 0)),
+        jax.ShapeDtypeStruct((NZ, 2 * CAP + DUP, COL), BF),
         grid=BLK,
         vmem=4 * 2**20,
     )
@@ -342,8 +348,8 @@
     pick = jnp.where(chosen, 1.0, 0.0).astype(BF)
     rows = home_ref[:, : 2 * CAP].reshape(2 * NZ * CAP, COL)
     tok_ref[...] = dot(pick, rows, 0, 0).astype(BF)
-    sums = home_ref[:, 2 * CAP :].reshape(NZ * EXT, COL)
-    row = iota((NZ * EXT, TOK), 0)
+    sums = home_ref[:, 2 * CAP :].reshape(NZ * DUP, COL)
+    row = iota((NZ * DUP, TOK), 0)
     lane = iota((COL, TOK), 0)
     w = w_ref[...].astype(F32)
     for k, member in enumerate((first, second)):
@@ -360,7 +366,7 @@
         combine_kernel,
         where,
         (ids, w, home),
-        [full(2, TOK), full(2, TOK), full(NZ, 2 * CAP + EXT, COL)],
+        [full(2, TOK), full(2, TOK), full(NZ, 2 * CAP + DUP, COL)],
         [full(TOK, COL), full(2, TOK)],
         [jax.ShapeDtypeStruct((TOK, COL), BF), jax.ShapeDtypeStruct((2, TOK), F32)],
         vmem=4 * 2**20,
@@ -383,7 +389,7 @@
 def row_weights(where, wg, wu, wd):
     own, *others = pack(where, wg, wu, wd)
     moved = [shifted(other, "x", k + 1) for k, other in enumerate(others)]
-    return jnp.stack([own, *moved])
+    return layout(where, (own, *moved))
 
 
 def per_device(tokens, cotangent, expert_ids, route_weight, gate_weight, up_weight, down_weight):
@@ -391,14 +397,14 @@
     where = jnp.stack([y * 4 + x, x]).astype(I32)
     ids, w = expert_ids.T, route_weight.T
     mine = exchange(dispatch(where, ids, w, tokens, cotangent), "z")
-    row_w = row_weights(where, gate_weight, up_weight, down_weight)
+    wgu, wdd = row_weights(where, gate_weight, up_weight, down_weight)
     both = copies(mine.transpose(1, 0, 2, 3, 4), 4).transpose(1, 0, 2, 3, 4, 5)
     rows = exchange(both.reshape(8, NZ, 2, CAP, COL), ("c", "y")).reshape(both.shape)
-    pre = pre_activations(where, rows, row_w)
+    pre = pre_activations(where, rows, wgu, wdd)
     pre = exchange(pre, "x")
     g = activations(where, pre)
     g = exchange(g, "x")
-    part = back(where, g, row_w)
+    part = back(where, g, wgu)
     sums = exchange(part.reshape(8, BLK, HOME, COL), ("c", "y")).reshape(part.shape)
     kept, *sent = weights(where, rows, g)
     home = exchange(total(where, sums), "z")

time: 151 us -> 148 us (0.980)
  Pallas kernels: 23.1 us -> 20.8 us
    pallas_call x9 -> x10, Pallas kernels: 23.1 us -> 20.8 us  [call(): pl.pallas_call(kernel, grid_spec=pltpu.PrefetchScalarGridSpec(num_scalar_...]
  transfers between devices with their start and end apart: 8 -> 8, of which waited for: 5 -> 5; matrix products, arithmetic and copies ran while one was open for 1% -> 0% of each run, Pallas kernels for 7% -> 7%
where the time goes in v5:
time: 148 us; the launch traced here: 147 us
  blocking collectives  74.5 us (50%)
  starting transfers between devices  34.6 us (23%)
  Pallas kernels  20.8 us (14%)
  waiting for transfers between devices  12.8 us (9%)
  local copies, waits for them, and re-layouts  2.81 us (2%)
    all_to_all x4, blocking collectives, exchange(): return lax.all_to_all(x, axis, split_axis=0, concat_axis=0, tiled=True)  74.5 us
    pallas_call x10, Pallas kernels, call(): pl.pallas_call(kernel, grid_spec=pltpu.PrefetchScalarGridSpec(num_scalar_...  20.8 us
    ppermute x6, starting transfers between devices, shifted(): return lax.ppermute(x, axis, [(i, (i + by) % n) for i in range(n)])  19.1 us
    all_to_all x2, starting transfers between devices, exchange(): return lax.all_to_all(x, axis, split_axis=0, concat_axis=0, tiled=True)  15.5 us
    ppermute x6, waiting for transfers between devices, shifted(): return lax.ppermute(x, axis, [(i, (i + by) % n) for i in range(n)])  12.8 us
  transfers between devices with their start and end apart: 8, of which 5 were waited for; matrix products, arithmetic and copies ran while one was open for 0% of the time, Pallas kernels for 7%

profile of v5, /device:TPU:1, one launch (start us, length us, event | category | flops | bytes accessed | tf_op | source)
XLA Modules:
  0.0 146.9 jit_solution(387291577534392198)
XLA Ops:
  0.6 0.6 pad_add_fusion.s_ref
  1.2 2.6 %shard_map.110 = bf16[16,2,2,16,128]{4,3,2,1,0:T(8,128)(2,1)} custom-call(s32[2]{0:T(128)} %pad_add_fusion.s_ref, s32[2,128]{1,0:T(2,128)} %bitcast.14, bf16[2,128]{1,0:T(2,128)(2,1)} %bitcast.16, bf16[128,2048]{1,0:T(8,128)(2,1)} %tok_ref.1, bf16[128,2048]{1,0:T(8,128)(2,1)} %cot_ref.1), custom_call_target="tpu_custom_call" | custom-call | flops 100000000 | bytes 2000000 | tf_op jit(solution)/shard_map/pallas_call | solution.py:95
  3.9 29.5 %all_to_all.30 = bf16[16,2,2,16,128]{4,3,2,1,0:T(8,128)(2,1)S(1)} all-to-all(bf16[16,2,2,16,128]{4,3,2,1,0:T(8,128)(2,1)} %shard_map.110), channel_id=1, replica_groups=mesh['z'=16,'c'=2,'y'=4,'x'=4] {'z'}, dimensions={0} | all-to-all | bytes 524288 | tf_op jit(solution)/shard_map/all_to_all | solution.py:377
  33.4 1.2 transpose.19
  34.6 10.0 %all-to-all-start.1 = ((bf16[8,16,2,16,128]{4,3,2,1,0:T(8,128)(2,1)}), bf16[8,16,2,16,128]{4,3,2,1,0:T(8,128)(2,1)S(1)}, u32[]{:S(2)}, u32[]{:S(2)}) async-start(bf16[8,16,2,16,128]{4,3,2,1,0:T(8,128)(2,1)} %bitcast.5), calls=%async_computation.1 | async-start | bytes 2097152 | tf_op jit(solution)/shard_map/all_to_all | solution.py:377
  44.6 2.9 %shard_map.111 = (bf16[4,192,128]{2,1,0:T(8,128)(2,1)}, bf16[4,192,128]{2,1,0:T(8,128)(2,1)}, bf16[4,192,128]{2,1,0:T(8,128)(2,1)}, bf16[4,192,128]{2,1,0:T(8,128)(2,1)}) custom-call(s32[2]{0:T(128)} %pad_add_fusion.s_ref, bf16[1,64,2048]{2,1,0:T(8,128)(2,1)} %wg_ref.1, bf16[1,64,2048]{2,1,0:T(8,128)(2,1)} %wu_ref.1, bf16[1,64,2048]{2,1,0:T(8,128)(2,1)} %wd_ref.1), custom_call_target="tpu_custom_call" | custom-call | flops 100000000 | bytes 2000000 | tf_op jit(solution)/shard_map/pallas_call | solution.py:95
  47.4 3.1 %collective-permute-start = (bf16[4,192,128]{2,1,0:T(8,128)(2,1)}, bf16[4,192,128]{2,1,0:T(8,128)(2,1)S(1)}, u32[]{:S(2)}, u32[]{:S(2)}) collective-permute-start(bf16[4,192,128]{2,1,0:T(8,128)(2,1)} %get-tuple-element.21), channel_id=1, source_target_pairs={{0,1},{1,2},{2,3},{3,0},{4,5},{5,6},{6,7},{7,4},{8,9},{9,10},{10,1... | collective-permute-start | bytes 589832 | tf_op jit(solution)/shard_map/ppermute | solution.py:386
  50.6 4.4 %collective-permute-start.1 = (bf16[4,192,128]{2,1,0:T(8,128)(2,1)}, bf16[4,192,128]{2,1,0:T(8,128)(2,1)S(1)}, u32[]{:S(2)}, u32[]{:S(2)}) collective-permute-start(bf16[4,192,128]{2,1,0:T(8,128)(2,1)} %get-tuple-element.22), channel_id=1, source_target_pairs={{0,2},{1,3},{2,0},{3,1},{4,6},{5,7},{6,4},{7,5},{8,10},{9,11},{10,... | collective-permute-start | bytes 589832 | tf_op jit(solution)/shard_map/ppermute | solution.py:386
  54.9 0.0 copy-start.3
  54.9 3.1 %collective-permute-start.2 = (bf16[4,192,128]{2,1,0:T(8,128)(2,1)}, bf16[4,192,128]{2,1,0:T(8,128)(2,1)S(1)}, u32[]{:S(2)}, u32[]{:S(2)}) collective-permute-start(bf16[4,192,128]{2,1,0:T(8,128)(2,1)} %get-tuple-element.23), channel_id=1, source_target_pairs={{0,3},{1,0},{2,1},{3,2},{4,7},{5,4},{6,5},{7,6},{8,11},{9,8},{10,9... | collective-permute-start | bytes 589832 | tf_op jit(solution)/shard_map/ppermute | solution.py:386
  58.0 0.0 collective-permute-done.w1_ref
  58.0 4.4 %collective-permute-done.1.w2_ref = bf16[4,192,128]{2,1,0:T(8,128)(2,1)S(1)} collective-permute-done((bf16[4,192,128]{2,1,0:T(8,128)(2,1)}, bf16[4,192,128]{2,1,0:T(8,128)(2,1)S(1)}, u32[]{:S(2)}, u32[]{:S(2)}) %collective-permute-start.1) | collective-permute-done | bytes 196640 | tf_op jit(solution)/shard_map/ppermute | solution.py:386
  62.4 1.4 collective-permute-done.2.w3_ref
  63.8 0.0 copy-done.3
  63.8 0.0 copy-start.2
  63.8 0.9 copy-done.2
  64.7 0.7 shard_map.112
  65.4 0.0 all-to-all-done.1
  65.4 0.0 copy-start
  65.4 1.7 %shard_map.113 = bf16[4,2,384,128]{3,2,1,0:T(8,128)(2,1)S(1)} custom-call(s32[2]{0:T(128)S(1)} %copy-done.3, bf16[2,4,16,2,16,128]{5,4,3,2,1,0:T(8,128)(2,1)S(1)} %bitcast.10, bf16[512,512]{1,0:T(8,128)(2,1)S(1)} %get-tuple-element.24.wgu_ref.w_ref, bf16[512,512]{1,0:T(8,128)(2,1)S(1)} %get-tuple-element.25.wdd_ref), custom_call_target="tpu_custom_call" | custom-call | flops 100000000 | bytes 2000000 | tf_op jit(solution)/shard_map/pallas_call | solution.py:95
  67.1 0.0 copy-done
  67.1 14.4 %all_to_all.31.p_ref = bf16[4,2,384,128]{3,2,1,0:T(8,128)(2,1)S(1)} all-to-all(bf16[4,2,384,128]{3,2,1,0:T(8,128)(2,1)S(1)} %shard_map.113), channel_id=1, replica_groups=mesh['z'=16,'c'=2,'y'=4,'x'=4] {'x'}, dimensions={0} | all-to-all | bytes 1572864 | tf_op jit(solution)/shard_map/all_to_all | solution.py:377
  81.5 1.5 %shard_map.114 = bf16[4,2,400,128]{3,2,1,0:T(8,128)(2,1)S(1)} custom-call(s32[2]{0:T(128)S(1)} %copy-done.3, bf16[4,2,384,128]{3,2,1,0:T(8,128)(2,1)S(1)} %all_to_all.31.p_ref), custom_call_target="tpu_custom_call" | custom-call | flops 100000000 | bytes 2000000 | tf_op jit(solution)/shard_map/pallas_call | solution.py:95
  83.0 12.6 %all_to_all.32.g_ref = bf16[4,2,400,128]{3,2,1,0:T(8,128)(2,1)S(1)} all-to-all(bf16[4,2,400,128]{3,2,1,0:T(8,128)(2,1)S(1)} %shard_map.114), channel_id=1, replica_groups=mesh['z'=16,'c'=2,'y'=4,'x'=4] {'x'}, dimensions={0} | all-to-all | bytes 1638400 | tf_op jit(solution)/shard_map/all_to_all | solution.py:377
  95.6 0.0 copy-start.1
  95.6 1.3 shard_map.115
  96.9 0.0 copy-done.1
  96.9 18.0 %all_to_all.33 = bf16[8,2,144,128]{3,2,1,0:T(8,128)(2,1)S(1)} all-to-all(bf16[8,2,144,128]{3,2,1,0:T(8,128)(2,1)S(1)} %bitcast.13), channel_id=1, replica_groups=mesh['z'=16,'c'=2,'y'=4,'x'=4] {'c','y'}, dimensions={0} | all-to-all | bytes 1179648 | tf_op jit(solution)/shard_map/all_to_all | solution.py:377
  114.9 1.6 %shard_map.116 = bf16[16,40,128]{2,1,0:T(8,128)(2,1)} custom-call(s32[2]{0:T(128)S(1)} %copy-done.3, bf16[2,4,2,144,128]{4,3,2,1,0:T(8,128)(2,1)S(1)} %bitcast.12), custom_call_target="tpu_custom_call" | custom-call | flops 100000000 | bytes 2000000 | tf_op jit(solution)/shard_map/pallas_call | solution.py:95
  116.4 5.5 %all-to-all-start.5 = ((bf16[16,40,128]{2,1,0:T(8,128)(2,1)}), bf16[16,40,128]{2,1,0:T(8,128)(2,1)S(1)}, u32[]{:S(2)}, u32[]{:S(2)}) async-start(bf16[16,40,128]{2,1,0:T(8,128)(2,1)} %shard_map.116), calls=%async_computation.5 | async-start | bytes 327680 | tf_op jit(solution)/shard_map/all_to_all | solution.py:377
  121.9 3.6 %shard_map.118 = (f32[192,512]{1,0:T(8,128)}, bf16[192,512]{1,0:T(8,128)(2,1)}, bf16[192,512]{1,0:T(8,128)(2,1)}, bf16[192,512]{1,0:T(8,128)(2,1)}) custom-call(s32[2]{0:T(128)} %pad_add_fusion.s_ref, bf16[2,4,16,2,16,128]{5,4,3,2,1,0:T(8,128)(2,1)} %bitcast.11, bf16[4,2,400,128]{3,2,1,0:T(8,128)(2,1)} %copy-done.1), custom_call_target="tpu_custom_call" | custom-call | flops 4000000000 | bytes 2000000 | tf_op jit(solution)/shard_map/pallas_call | solution.py:95
  125.6 2.2 %collective-permute-start.3 = (bf16[192,512]{1,0:T(8,128)(2,1)}, bf16[192,512]{1,0:T(8,128)(2,1)S(1)}, u32[]{:S(2)}, u32[]{:S(2)}) collective-permute-start(bf16[192,512]{1,0:T(8,128)(2,1)} %get-tuple-element.29), channel_id=1, source_target_pairs={{0,1},{1,2},{2,3},{3,0},{4,5},{5,6},{6,7},{7,4},{8,9},{9,10},{10,1... | collective-permute-start | bytes 589832 | tf_op jit(solution)/shard_map/ppermute | solution.py:386
  127.7 3.7 %collective-permute-start.4 = (bf16[192,512]{1,0:T(8,128)(2,1)}, bf16[192,512]{1,0:T(8,128)(2,1)S(1)}, u32[]{:S(2)}, u32[]{:S(2)}) collective-permute-start(bf16[192,512]{1,0:T(8,128)(2,1)} %get-tuple-element.30), channel_id=1, source_target_pairs={{0,2},{1,3},{2,0},{3,1},{4,6},{5,7},{6,4},{7,5},{8,10},{9,11},{10,... | collective-permute-start | bytes 589832 | tf_op jit(solution)/shard_map/ppermute | solution.py:386
  131.4 2.7 %collective-permute-start.5 = (bf16[192,512]{1,0:T(8,128)(2,1)}, bf16[192,512]{1,0:T(8,128)(2,1)S(1)}, u32[]{:S(2)}, u32[]{:S(2)}) collective-permute-start(bf16[192,512]{1,0:T(8,128)(2,1)} %get-tuple-element.31), channel_id=1, source_target_pairs={{0,3},{1,0},{2,1},{3,2},{4,7},{5,4},{6,5},{7,6},{8,11},{9,8},{10,9... | collective-permute-start | bytes 589832 | tf_op jit(solution)/shard_map/ppermute | solution.py:386
  134.2 1.1 collective-permute-done.3.refs_1_
  135.2 0.0 copy-start.7
  135.2 3.1 %collective-permute-done.4.refs_2_ = bf16[192,512]{1,0:T(8,128)(2,1)S(1)} collective-permute-done((bf16[192,512]{1,0:T(8,128)(2,1)}, bf16[192,512]{1,0:T(8,128)(2,1)S(1)}, u32[]{:S(2)}, u32[]{:S(2)}) %collective-permute-start.4) | collective-permute-done | bytes 196640 | tf_op jit(solution)/shard_map/ppermute | solution.py:386
  138.3 0.0 copy-start.8
  138.3 2.9 %collective-permute-done.5.refs_3_ = bf16[192,512]{1,0:T(8,128)(2,1)S(1)} collective-permute-done((bf16[192,512]{1,0:T(8,128)(2,1)}, bf16[192,512]{1,0:T(8,128)(2,1)S(1)}, u32[]{:S(2)}, u32[]{:S(2)}) %collective-permute-start.5) | collective-permute-done | bytes 196640 | tf_op jit(solution)/shard_map/ppermute | solution.py:386
  141.2 0.0 copy-done.7
  141.2 0.0 copy-done.8
  141.2 0.7 copy-done.9
  141.9 3.3 %shard_map.119 = (f32[1,64,2048]{2,1,0:T(8,128)}, f32[1,64,2048]{2,1,0:T(8,128)}, f32[1,64,2048]{2,1,0:T(8,128)}) custom-call(s32[2]{0:T(128)} %pad_add_fusion.s_ref, f32[192,512]{1,0:T(8,128)} %get-tuple-element.28.refs_0_, bf16[192,512]{1,0:T(8,128)(2,1)} %copy-done.7, bf16[192,512]{1,0:T(8,128)(2,1)} %copy-done.8, bf16[192,512]{1,0:T(8,128)(2,1)} %copy-done.9), custom_call_target="tpu_custom_call" | custom-call | flops 1000000000 | bytes 2000000 | tf_op jit(solution)/shard_map/pallas_call | solution.py:95
  145.2 0.0 all-to-all-done.5.home_ref
  145.2 0.0 copy-done.4
  145.2 0.0 copy-done.5
  145.2 0.0 copy-done.6
  145.2 1.7 %shard_map.117 = (bf16[128,128]{1,0:T(8,128)(2,1)}, f32[2,128]{1,0:T(2,128)}) custom-call(s32[2]{0:T(128)S(1)} %copy-done.4, s32[2,128]{1,0:T(2,128)S(1)} %bitcast.15, bf16[2,128]{1,0:T(2,128)(2,1)S(1)} %bitcast.17, bf16[16,40,128]{2,1,0:T(8,128)(2,1)S(1)} %all-to-all-done.5.home_ref), custom_call_target="tpu_custom_call" | custom-call | flops 100000000 | bytes 2000000 | tf_op jit(solution)/shard_map/pallas_call | solution.py:95
  (5 shorter events, 0.0 us)
Async XLA Ops:
  34.6 30.8 %all-to-all-start.1 = ((bf16[8,16,2,16,128]{4,3,2,1,0:T(8,128)(2,1)}), bf16[8,16,2,16,128]{4,3,2,1,0:T(8,128)(2,1)S(1)}, u32[]{:S(2)}, u32[]{:S(2)}) async-start(bf16[8,16,2,16,128]{4,3,2,1,0:T(8,128)(2,1)} %bitcast.5), calls=%async_computation.1 | async-start | bytes 2097152 | tf_op jit(solution)/shard_map/all_to_all | solution.py:377
  47.4 10.6 %collective-permute-start = (bf16[4,192,128]{2,1,0:T(8,128)(2,1)}, bf16[4,192,128]{2,1,0:T(8,128)(2,1)S(1)}, u32[]{:S(2)}, u32[]{:S(2)}) collective-permute-start(bf16[4,192,128]{2,1,0:T(8,128)(2,1)} %get-tuple-element.21), channel_id=1, source_target_pairs={{0,1},{1,2},{2,3},{3,0},{4,5},{5,6},{6,7},{7,4},{8,9},{9,10},{10,1... | collective-permute-start | bytes 589832 | tf_op jit(solution)/shard_map/ppermute | solution.py:386
  50.6 11.8 %collective-permute-start.1 = (bf16[4,192,128]{2,1,0:T(8,128)(2,1)}, bf16[4,192,128]{2,1,0:T(8,128)(2,1)S(1)}, u32[]{:S(2)}, u32[]{:S(2)}) collective-permute-start(bf16[4,192,128]{2,1,0:T(8,128)(2,1)} %get-tuple-element.22), channel_id=1, source_target_pairs={{0,2},{1,3},{2,0},{3,1},{4,6},{5,7},{6,4},{7,5},{8,10},{9,11},{10,... | collective-permute-start | bytes 589832 | tf_op jit(solution)/shard_map/ppermute | solution.py:386
  54.9 8.8 %copy-start.3 = (s32[2]{0:T(128)S(1)}, s32[2]{0:T(128)}, u32[]{:S(2)}) copy-start(s32[2]{0:T(128)} %pad_add_fusion.s_ref) | copy-start | bytes 28
  54.9 8.8 %collective-permute-start.2 = (bf16[4,192,128]{2,1,0:T(8,128)(2,1)}, bf16[4,192,128]{2,1,0:T(8,128)(2,1)S(1)}, u32[]{:S(2)}, u32[]{:S(2)}) collective-permute-start(bf16[4,192,128]{2,1,0:T(8,128)(2,1)} %get-tuple-element.23), channel_id=1, source_target_pairs={{0,3},{1,0},{2,1},{3,2},{4,7},{5,4},{6,5},{7,6},{8,11},{9,8},{10,9... | collective-permute-start | bytes 589832 | tf_op jit(solution)/shard_map/ppermute | solution.py:386
  63.8 0.9 copy-start.2
  65.4 1.7 %copy-start = (bf16[8,16,2,16,128]{4,3,2,1,0:T(8,128)(2,1)}, bf16[8,16,2,16,128]{4,3,2,1,0:T(8,128)(2,1)S(1)}, u32[]{:S(2)}) copy-start(bf16[8,16,2,16,128]{4,3,2,1,0:T(8,128)(2,1)S(1)} %all-to-all-done.1) | copy-start | bytes 3145732
  95.6 1.3 copy-start.1
  116.4 28.8 %all-to-all-start.5 = ((bf16[16,40,128]{2,1,0:T(8,128)(2,1)}), bf16[16,40,128]{2,1,0:T(8,128)(2,1)S(1)}, u32[]{:S(2)}, u32[]{:S(2)}) async-start(bf16[16,40,128]{2,1,0:T(8,128)(2,1)} %shard_map.116), calls=%async_computation.5 | async-start | bytes 327680 | tf_op jit(solution)/shard_map/all_to_all | solution.py:377
  125.6 9.7 %collective-permute-start.3 = (bf16[192,512]{1,0:T(8,128)(2,1)}, bf16[192,512]{1,0:T(8,128)(2,1)S(1)}, u32[]{:S(2)}, u32[]{:S(2)}) collective-permute-start(bf16[192,512]{1,0:T(8,128)(2,1)} %get-tuple-element.29), channel_id=1, source_target_pairs={{0,1},{1,2},{2,3},{3,0},{4,5},{5,6},{6,7},{7,4},{8,9},{9,10},{10,1... | collective-permute-start | bytes 589832 | tf_op jit(solution)/shard_map/ppermute | solution.py:386
  127.7 10.6 %collective-permute-start.4 = (bf16[192,512]{1,0:T(8,128)(2,1)}, bf16[192,512]{1,0:T(8,128)(2,1)S(1)}, u32[]{:S(2)}, u32[]{:S(2)}) collective-permute-start(bf16[192,512]{1,0:T(8,128)(2,1)} %get-tuple-element.30), channel_id=1, source_target_pairs={{0,2},{1,3},{2,0},{3,1},{4,6},{5,7},{6,4},{7,5},{8,10},{9,11},{10,... | collective-permute-start | bytes 589832 | tf_op jit(solution)/shard_map/ppermute | solution.py:386
  131.4 9.8 %collective-permute-start.5 = (bf16[192,512]{1,0:T(8,128)(2,1)}, bf16[192,512]{1,0:T(8,128)(2,1)S(1)}, u32[]{:S(2)}, u32[]{:S(2)}) collective-permute-start(bf16[192,512]{1,0:T(8,128)(2,1)} %get-tuple-element.31), channel_id=1, source_target_pairs={{0,3},{1,0},{2,1},{3,2},{4,7},{5,4},{6,5},{7,6},{8,11},{9,8},{10,9... | collective-permute-start | bytes 589832 | tf_op jit(solution)/shard_map/ppermute | solution.py:386
  135.2 6.0 %copy-start.7 = (bf16[192,512]{1,0:T(8,128)(2,1)}, bf16[192,512]{1,0:T(8,128)(2,1)S(1)}, u32[]{:S(2)}) copy-start(bf16[192,512]{1,0:T(8,128)(2,1)S(1)} %collective-permute-done.3.refs_1_) | copy-start | bytes 589828
  138.3 2.9 %copy-start.8 = (bf16[192,512]{1,0:T(8,128)(2,1)}, bf16[192,512]{1,0:T(8,128)(2,1)S(1)}, u32[]{:S(2)}) copy-start(bf16[192,512]{1,0:T(8,128)(2,1)S(1)} %collective-permute-done.4.refs_2_) | copy-start | bytes 589828
  141.2 0.7 copy-start.9
  141.9 3.3 %copy-start.4 = (s32[2]{0:T(128)S(1)}, s32[2]{0:T(128)}, u32[]{:S(2)}) copy-start(s32[2]{0:T(128)} %pad_add_fusion.s_ref) | copy-start | bytes 28
  141.9 3.3 %copy-start.5 = (s32[128,2]{0,1:T(2,128)S(1)}, s32[128,2]{0,1:T(2,128)}, u32[]{:S(2)}) copy-start(s32[128,2]{0,1:T(2,128)} %param.9) | copy-start | bytes 3076
  141.9 3.3 %copy-start.6 = (bf16[128,2]{0,1:T(2,128)(2,1)S(1)}, bf16[128,2]{0,1:T(2,128)(2,1)}, u32[]{:S(2)}) copy-start(bf16[128,2]{0,1:T(2,128)(2,1)} %param.10) | copy-start | bytes 1540

commit v6 on v5

v6 whole, which is shorter than its diff:
```python
import jax
import jax.numpy as jnp
from jax import lax
from jax.experimental import pallas as pl
from jax.experimental.pallas import tpu as pltpu
from jax.sharding import Mesh
from jax.sharding import PartitionSpec as P


GROUP = ("c", "y", "u")

BF = jnp.bfloat16
F32 = jnp.float32
I32 = jnp.int32
NZ = 16
TP = 16
TOK = 128
CAP = 16
COL = 128
HALF = 8
HID = 64
ROWS = 512
BLK = 2
RB = ROWS // BLK
SMALL = 12 * 2**20
EXT = 2 * NZ // BLK
DUP = 8


def iota(shape, dim):
    return lax.broadcasted_iota(I32, shape, dim)


def dot(a, b, ca, cb, precision=None):
    return lax.dot_general(
        a, b, (((ca,), (cb,)), ((), ())), precision=precision, preferred_element_type=F32
    )


def routing(ids_ref):
    experts = 2 * NZ
    row = iota((experts, TOK), 0)
    first = (ids_ref[0:1, :] == row).astype(F32)
    second = (ids_ref[1:2, :] == row).astype(F32)
    member = first + second
    earlier = (iota((TOK, TOK), 0) < iota((TOK, TOK), 1)).astype(BF)
    rank = dot(member.astype(BF), earlier, 1, 0)
    slots = experts * CAP
    expand = ((iota((slots, experts), 0) >> 4) == iota((slots, experts), 1)).astype(BF)
    hit = dot(expand, member.astype(BF), 1, 0)
    at = dot(expand, rank.astype(BF), 1, 0)
    place = (iota((slots, TOK), 0) & 15).astype(F32)
    chosen = (hit > 0.5) & (at == place)
    return first, second, rank, expand, chosen


def dispatch_kernel(s_ref, ids_ref, w_ref, tok_ref, cot_ref, out_ref):
    first, second, _, expand, chosen = routing(ids_ref)
    w = w_ref[...].astype(F32)
    weighted = first * w[0:1, :] + second * w[1:2, :]
    scale = dot(expand, weighted.astype(BF), 1, 0)
    pick = jnp.where(chosen, 1.0, 0.0).astype(BF)
    pick_scaled = jnp.where(chosen, scale, 0.0).astype(BF)
    out_ref[:, :, 0] = dot(pick, tok_ref[...], 1, 0).astype(BF).reshape(NZ, 2, CAP, COL)
    out_ref[:, :, 1] = dot(pick_scaled, cot_ref[...], 1, 0).astype(BF).reshape(NZ, 2, CAP, COL)


def dispatch(where, ids, w, tokens, cotangent):
    mine = pl.BlockSpec((TOK, COL), lambda i, s: (0, s[0]))
    return call(
        dispatch_kernel,
        where,
        (ids, w, tokens, cotangent),
        [full(2, TOK), full(2, TOK), mine, mine],
        full(NZ, 2, 2, CAP, COL),
        jax.ShapeDtypeStruct((NZ, 2, 2, CAP, COL), BF),
    )


def cols(q):
    return slice(q * COL, (q + 1) * COL)


def block(q, v):
    j = (q >> 1) * 4 + (q & 1) * 2 + v
    return pl.ds(pl.multiple_of(j * COL, COL), COL)


def full(*shape):
    return pl.BlockSpec(shape, lambda i, s: (0,) * len(shape))


def call(kernel, where, args, in_specs, out_specs, out_shape, scratch=(), grid=1, flops=10**8, vmem=None):
    return pl.pallas_call(
        kernel,
        grid_spec=pltpu.PrefetchScalarGridSpec(
            num_scalar_prefetch=1,
            grid=(grid,),
            in_specs=in_specs,
            out_specs=out_specs,
            scratch_shapes=list(scratch),
        ),
        out_shape=out_shape,
        compiler_params=pltpu.CompilerParams(vmem_limit_bytes=vmem),
        cost_estimate=pl.CostEstimate(flops=flops, bytes_accessed=2 * 10**6, transcendentals=0),
    )(where, *args)


def pack_kernel(s_ref, wg_ref, wu_ref, wd_ref, out_ref):
    for i, w_ref in enumerate((wg_ref, wu_ref, wd_ref)):
        for q in range(HALF):
            out_ref[i, :, cols(q)] = w_ref[0, :, block(q, 1 - s_ref[1])]


def pack(where, ws):
    shape = (3, HID, HALF * COL)
    return call(
        pack_kernel,
        where,
        ws,
        [full(1, HID, TP * COL)] * 3,
        full(*shape),
        jax.ShapeDtypeStruct(shape, BF),
    )


def layout_kernel(s_ref, wg_ref, wu_ref, wd_ref, got_ref, up_ref, down_ref):
    v = s_ref[1]
    for i, w_ref in enumerate((wg_ref, wu_ref, wd_ref)):
        to_ref, at = (up_ref, i * 2 * HID) if i < 2 else (down_ref, 0)
        mine = pl.ds(pl.multiple_of(at + v * HID, HID), HID)
        theirs = pl.ds(pl.multiple_of(at + (1 - v) * HID, HID), HID)
        to_ref[theirs, :] = got_ref[i]
        for q in range(HALF):
            to_ref[mine, cols(q)] = w_ref[0, :, block(q, v)]


def layout(where, ws, got):
    d = HALF * COL
    return call(
        layout_kernel,
        where,
        (*ws, got),
        [full(1, HID, TP * COL)] * 3 + [full(3, HID, d)],
        [full(4 * HID, d), full(2 * HID, d)],
        [jax.ShapeDtypeStruct((4 * HID, d), BF), jax.ShapeDtypeStruct((2 * HID, d), BF)],
        vmem=SMALL,
    )


def features(x_ref, which, rows):
    pieces = [x_ref[:, q >> 1, q & 1, :, which].reshape(rows, COL) for q in range(HALF)]
    return jnp.concatenate(pieces, axis=1)


def pre_kernel(s_ref, x_ref, up_ref, down_ref, kept_ref, sent_ref):
    pre = dot(features(x_ref, 0, RB), up_ref[...], 1, 1)
    back = dot(features(x_ref, 1, RB), down_ref[...], 1, 1)
    for i, part in enumerate((pre[:, :COL], pre[:, COL:], back)):
        kept_ref[0, i] = part
        sent_ref[0, i] = part.astype(BF)


THREE = (BLK, 3, RB, COL)
HOME = RB // 2 + EXT


def three():
    return pl.BlockSpec((1, 3, RB, COL), lambda i, s: (i, 0, 0, 0))


def pre_activations(where, x, up, down):
    d = HALF * COL
    return call(
        pre_kernel,
        where,
        (x, up, down),
        [
            pl.BlockSpec((2, 4, 2, NZ // BLK, 2, CAP, COL), lambda i, s: (0, 0, 0, i, 0, 0, 0)),
            full(4 * HID, d),
            full(2 * HID, d),
        ],
        [three(), three()],
        [jax.ShapeDtypeStruct(THREE, F32), jax.ShapeDtypeStruct(THREE, BF)],
        grid=BLK,
        vmem=SMALL,
    )


def two_parts(sums):
    high = sums.astype(BF).astype(F32)
    return jnp.where(iota((EXT, COL), 1) < 32, high, sums - high).astype(BF)


def one_sum(parts):
    both = parts + pltpu.roll(parts, COL - 32, 1)
    low = iota((EXT, COL), 1) < 32
    both = jnp.where(low, both, 0.0)
    return both + pltpu.roll(both, 32, 1)


def act_kernel(s_ref, kept_ref, got_ref, up_ref, out_ref, act_ref):
    gate, up, back = (kept_ref[0, i] + got_ref[0, i].astype(F32) for i in range(3))
    sigma = 1.0 / (1.0 + jnp.exp(-gate))
    silu = gate * sigma
    hidden = silu * up
    grad_gate = (back * up * sigma * (1.0 + gate * (1.0 - sigma))).astype(BF)
    grad_up = (back * silu).astype(BF)
    act_ref[0, 0] = grad_gate
    act_ref[0, 1] = grad_up
    act_ref[0, 2] = hidden.astype(BF)
    total = jnp.sum(hidden * back, axis=1, keepdims=True)
    spread = jnp.where((iota((RB, COL), 1) & 15) == (iota((RB, COL), 0) & 15), total, 0.0)
    group = (iota((EXT, RB), 0) == (iota((EXT, RB), 1) >> 4)).astype(F32)
    sums = dot(group, spread, 1, 0, lax.Precision.HIGHEST)
    pieces = dot(jnp.concatenate([grad_gate, grad_up], axis=1), up_ref[...], 1, 0).astype(BF)
    half = RB // 2
    for core in range(2):
        extra = two_parts(sums if core == 0 else pltpu.roll(sums, EXT // 2, 0))
        for q in range(HALF):
            out_ref[core, q, 0, :half] = pieces[core * half : (core + 1) * half, cols(q)]
            out_ref[core, q, 0, half:] = extra


def activations(where, kept, got, up):
    shape = (2, HALF, BLK, HOME, COL)
    return call(
        act_kernel,
        where,
        (kept, got, up),
        [three(), three(), full(4 * HID, HALF * COL)],
        [pl.BlockSpec((2, HALF, 1, HOME, COL), lambda i, s: (0, 0, i, 0, 0)), three()],
        [jax.ShapeDtypeStruct(shape, BF), jax.ShapeDtypeStruct(THREE, BF)],
        grid=BLK,
        vmem=SMALL,
    )


def weights_kernel(s_ref, x_ref, act_ref, kept_ref, sent_ref):
    near = NZ // BLK
    blocks = [x_ref.at[:, :, :, b * near : (b + 1) * near] for b in range(BLK)]
    tok, cot = (jnp.concatenate([features(b, which, RB) for b in blocks], axis=0) for which in range(2))
    first = s_ref[1] == 0
    for i, rows in enumerate((tok, tok, cot)):
        act = jnp.concatenate([act_ref[b, i] for b in range(BLK)], axis=0)
        both = dot(act, rows, 0, 0)
        here = slice(i * HID, (i + 1) * HID)
        kept_ref[here] = jnp.where(first, both[:HID], both[HID:])
        sent_ref[here] = jnp.where(first, both[HID:], both[:HID]).astype(BF)


def weights(where, x, act):
    shape = (3 * HID, HALF * COL)
    return call(
        weights_kernel,
        where,
        (x, act),
        [full(2, 4, 2, NZ, 2, CAP, COL), full(*THREE)],
        [full(*shape)] * 2,
        [jax.ShapeDtypeStruct(shape, F32), jax.ShapeDtypeStruct(shape, BF)],
        flops=4 * 10**9,
    )


def assemble_kernel(s_ref, kept_ref, got_ref, *out_refs):
    v = s_ref[1]
    for i, out_ref in enumerate(out_refs):
        here = slice(i * HID, (i + 1) * HID)
        for q in range(HALF):
            out_ref[0, :, block(q, v)] = kept_ref[here, cols(q)]
            out_ref[0, :, block(q, 1 - v)] = got_ref[here, cols(q)].astype(F32)


def assemble(where, kept, got):
    shape = (1, HID, TP * COL)
    return call(
        assemble_kernel,
        where,
        (kept, got),
        [full(3 * HID, HALF * COL)] * 2,
        [full(*shape)] * 3,
        [jax.ShapeDtypeStruct(shape, F32)] * 3,
        flops=10**9,
    )


def total_kernel(s_ref, p_ref, out_ref):
    half, sums = RB // 2, []
    for core in range(2):
        rows = p_ref[core, 0, 0].astype(F32)
        for q in range(1, HALF):
            rows = rows + p_ref[core, q, 0].astype(F32)
        out_ref[:, core * CAP : (core + 1) * CAP] = rows[:half].astype(BF).reshape(NZ // BLK, CAP, COL)
        sums.append(one_sum(rows[half:]))
    extra = two_parts(jnp.where((iota((EXT, COL), 1) & 31) < 16, *sums)).astype(F32)
    for k in range(NZ // BLK):
        out_ref[k, 2 * CAP :] = jnp.broadcast_to(extra[k : k + 1], (DUP, COL)).astype(BF)


def total(where, part):
    return call(
        total_kernel,
        where,
        (part,),
        [pl.BlockSpec((2, HALF, 1, HOME, COL), lambda i, s: (0, 0, i, 0, 0))],
        pl.BlockSpec((NZ // BLK, 2 * CAP + DUP, COL), lambda i, s: (i, 0, 0)),
        jax.ShapeDtypeStruct((NZ, 2 * CAP + DUP, COL), BF),
        grid=BLK,
        vmem=8 * 2**20,
    )


def combine_kernel(s_ref, ids_ref, w_ref, home_ref, tok_ref, route_ref):
    first, second, rank, _, chosen = routing(ids_ref)
    pick = jnp.where(chosen, 1.0, 0.0).astype(BF)
    rows = home_ref[:, : 2 * CAP].reshape(2 * NZ * CAP, COL)
    tok_ref[...] = dot(pick, rows, 0, 0).astype(BF)
    sums = home_ref[:, 2 * CAP :].reshape(NZ * DUP, COL)
    row = iota((NZ * DUP, TOK), 0)
    lane = iota((COL, TOK), 0)
    w = w_ref[...].astype(F32)
    for k, member in enumerate((first, second)):
        ids = ids_ref[k : k + 1, :]
        at = jnp.sum(member * rank, axis=0, keepdims=True).astype(I32) + 16 * (ids & 1)
        chip = (((row & 7) == 0) & ((row >> 3) == (ids >> 1))).astype(BF)
        found = dot(sums, chip, 0, 0)
        found = jnp.where((lane == at) | (lane == at + 32), found, 0.0)
        route_ref[k : k + 1, :] = jnp.sum(found, axis=0, keepdims=True) / w[k : k + 1, :]


def combine(where, ids, w, home):
    return call(
        combine_kernel,
        where,
        (ids, w, home),
        [full(2, TOK), full(2, TOK), full(NZ, 2 * CAP + DUP, COL)],
        [full(TOK, COL), full(2, TOK)],
        [jax.ShapeDtypeStruct((TOK, COL), BF), jax.ShapeDtypeStruct((2, TOK), F32)],
        vmem=4 * 2**20,
    )


def exchange(x, axis):
    return lax.all_to_all(x, axis, split_axis=0, concat_axis=0, tiled=True)


def copies(x, n):
    return jnp.broadcast_to(x[None], (n, *x.shape))


def swapped(x):
    return lax.ppermute(x, "v", [(0, 1), (1, 0)])


def row_weights(where, ws):
    sent = pack(where, ws)
    got = swapped(sent)
    return layout(where, ws, got)


def per_device(tokens, cotangent, expert_ids, route_weight, *ws):
    y, u, v = (lax.axis_index(axis) for axis in GROUP[1:] + ("v",))
    where = jnp.stack([y * 4 + u * 2 + v, v]).astype(I32)
    ids, w = expert_ids.T, route_weight.T
    mine = exchange(dispatch(where, ids, w, tokens, cotangent), "z")
    up, down = row_weights(where, ws)
    both = copies(mine.transpose(1, 0, 2, 3, 4), HALF).transpose(1, 0, 2, 3, 4, 5)
    rows = exchange(both.reshape(2 * HALF, NZ, 2, CAP, COL), GROUP)
    rows = rows.reshape(2, 4, 2, NZ, 2, CAP, COL)
    kept, sent = pre_activations(where, rows, up, down)
    got = swapped(sent)
    part, act = activations(where, kept, got, up)
    sums = exchange(part.reshape(2 * HALF, BLK, HOME, COL), GROUP).reshape(part.shape)
    kept, sent = weights(where, rows, act)
    home = exchange(total(where, sums), "z")
    got = swapped(sent)
    gate_grad, up_grad, down_grad = assemble(where, kept, got)
    tokens_grad, route_grad = combine(where, ids, w, home)
    return tokens_grad, route_grad.T, gate_grad, up_grad, down_grad


def solution(mesh):
    grid = Mesh(mesh.devices.reshape(NZ, 2, 4, 2, 2), ("z", "c", "y", "u", "v"))
    ep, tp = ("z", "c"), ("y", "u", "v")
    weight = P(ep, tp, None)
    return jax.shard_map(
        per_device,
        mesh=grid,
        in_specs=(P(ep, None), P(ep, None), P(ep, None), P(ep, None), weight, weight, weight),
        out_specs=(P(ep, tp), P(ep, None), weight, weight, weight),
        check_vma=False,
    )
```

time: 148 us -> 156 us (1.054)
  waiting for transfers between devices: 12.8 us -> 46.5 us
  blocking collectives: 74.5 us -> 56.3 us
  starting transfers between devices: 34.6 us -> 26.3 us
    ppermute x6 -> x3, waiting for transfers between devices: 12.8 us -> 46.5 us  [swapped(): return lax.ppermute(x, 'v', [(0, 1), (1, 0)])]
    all_to_all x4 -> x2, blocking collectives: 74.5 us -> 56.3 us  [exchange(): return lax.all_to_all(x, axis, split_axis=0, concat_axis=0, tiled=True)]
    ppermute x6 -> x3, starting transfers between devices: 19.1 us -> 8.18 us  [swapped(): return lax.ppermute(x, 'v', [(0, 1), (1, 0)])]
    all_to_all x2, starting transfers between devices: 15.5 us -> 18.2 us  [exchange(): return lax.all_to_all(x, axis, split_axis=0, concat_axis=0, tiled=True)]
    pallas_call x10 -> x9, Pallas kernels: 20.8 us -> 19.7 us  [call(): pl.pallas_call(kernel, grid_spec=pltpu.PrefetchScalarGridSpec(num_scalar_...]
  transfers between devices with their start and end apart: 8 -> 5, of which waited for: 5 -> 3; matrix products, arithmetic and copies ran while one was open for 0% -> 0% of each run, Pallas kernels for 7% -> 7%
where the time goes in v6:
time: 156 us; the launch traced here: 155 us
  blocking collectives  56.3 us (36%)
  waiting for transfers between devices  46.5 us (30%)
  starting transfers between devices  26.3 us (17%)
  Pallas kernels  19.7 us (13%)
  local copies, waits for them, and re-layouts  4.36 us (3%)
    all_to_all x2, blocking collectives, exchange(): return lax.all_to_all(x, axis, split_axis=0, concat_axis=0, tiled=True)  56.3 us
    ppermute x3, waiting for transfers between devices, swapped(): return lax.ppermute(x, 'v', [(0, 1), (1, 0)])  46.5 us
    pallas_call x9, Pallas kernels, call(): pl.pallas_call(kernel, grid_spec=pltpu.PrefetchScalarGridSpec(num_scalar_...  19.7 us
    all_to_all x2, starting transfers between devices, exchange(): return lax.all_to_all(x, axis, split_axis=0, concat_axis=0, tiled=True)  18.2 us
    ppermute x3, starting transfers between devices, swapped(): return lax.ppermute(x, 'v', [(0, 1), (1, 0)])  8.18 us
  transfers between devices with their start and end apart: 5, of which 3 were waited for; matrix products, arithmetic and copies ran while one was open for 0% of the time, Pallas kernels for 7%

profile of v6, /device:TPU:1, one launch (start us, length us, event | category | flops | bytes accessed | tf_op | source)
XLA Modules:
  0.0 154.6 jit_solution(1979137618474533720)
XLA Ops:
  0.6 0.7 pad_add_fusion.s_ref
  1.3 2.6 %shard_map.110 = bf16[16,2,2,16,128]{4,3,2,1,0:T(8,128)(2,1)} custom-call(s32[2]{0:T(128)} %pad_add_fusion.s_ref, s32[2,128]{1,0:T(2,128)} %bitcast.14, bf16[2,128]{1,0:T(2,128)(2,1)} %bitcast.16, bf16[128,2048]{1,0:T(8,128)(2,1)} %tok_ref.1, bf16[128,2048]{1,0:T(8,128)(2,1)} %cot_ref.1), custom_call_target="tpu_custom_call" | custom-call | flops 100000000 | bytes 2000000 | tf_op jit(solution)/shard_map/pallas_call | solution.py:94
  3.9 29.5 %all_to_all.20 = bf16[16,2,2,16,128]{4,3,2,1,0:T(8,128)(2,1)S(1)} all-to-all(bf16[16,2,2,16,128]{4,3,2,1,0:T(8,128)(2,1)} %shard_map.110), channel_id=1, replica_groups=mesh['z'=16,'c'=2,'y'=4,'u'=2,'v'=2] {'z'}, dimensions={0} | all-to-all | bytes 524288 | tf_op jit(solution)/shard_map/all_to_all | solution.py:344
  33.5 1.7 %transpose.19 = bf16[2,8,16,2,16,128]{5,4,3,2,1,0:T(8,128)(2,1)} broadcast(bf16[2,16,2,16,128]{4,3,2,1,0:T(8,128)(2,1)S(1)} %copy.12), dimensions={0,2,3,4,5} | broadcast | bytes 2359296 | tf_op jit(solution)/shard_map/transpose | solution.py:367
  35.2 0.0 copy-start.1
  35.2 0.0 copy-start.2
  35.2 0.0 copy-start.3
  35.2 0.0 copy-start.6
  35.2 12.7 %all-to-all-start.1 = ((bf16[16,16,2,16,128]{4,3,2,1,0:T(8,128)(2,1)}), bf16[16,16,2,16,128]{4,3,2,1,0:T(8,128)(2,1)S(1)}, u32[]{:S(2)}, u32[]{:S(2)}) async-start(bf16[16,16,2,16,128]{4,3,2,1,0:T(8,128)(2,1)} %bitcast.18), calls=%async_computation.1 | async-start | bytes 4194304 | tf_op jit(solution)/shard_map/all_to_all | solution.py:344
  47.9 2.6 %shard_map.111 = bf16[3,64,1024]{2,1,0:T(8,128)(2,1)} custom-call(s32[2]{0:T(128)} %pad_add_fusion.s_ref, bf16[1,64,2048]{2,1,0:T(8,128)(2,1)} %wg_ref.3, bf16[1,64,2048]{2,1,0:T(8,128)(2,1)} %wu_ref.3, bf16[1,64,2048]{2,1,0:T(8,128)(2,1)} %wd_ref.3), custom_call_target="tpu_custom_call" | custom-call | flops 100000000 | bytes 2000000 | tf_op jit(solution)/shard_map/pallas_call | solution.py:94
  50.5 2.2 %collective-permute-start = (bf16[3,64,1024]{2,1,0:T(8,128)(2,1)}, bf16[3,64,1024]{2,1,0:T(8,128)(2,1)S(1)}, u32[]{:S(2)}, u32[]{:S(2)}) collective-permute-start(bf16[3,64,1024]{2,1,0:T(8,128)(2,1)} %shard_map.111), channel_id=1, source_target_pairs={{0,1},{1,0},{2,3},{3,2},{4,5},{5,4},{6,7},{7,6},{8,9},{9,8},{10,11... | collective-permute-start | bytes 1179656 | tf_op jit(solution)/shard_map/ppermute | solution.py:352
  52.7 28.0 %collective-permute-done.got_ref = bf16[3,64,1024]{2,1,0:T(8,128)(2,1)S(1)} collective-permute-done((bf16[3,64,1024]{2,1,0:T(8,128)(2,1)}, bf16[3,64,1024]{2,1,0:T(8,128)(2,1)S(1)}, u32[]{:S(2)}, u32[]{:S(2)}) %collective-permute-start) | collective-permute-done | bytes 393248 | tf_op jit(solution)/shard_map/ppermute | solution.py:352
  80.7 0.0 copy-done.1
  80.8 0.0 copy-done.2
  80.8 0.0 copy-done.3
  80.8 0.0 copy-done.6
  80.8 0.7 shard_map.112
  81.4 0.0 copy-start.4
  81.5 0.7 copy-done.4
  82.2 0.0 all-to-all-done.1
  82.2 0.0 copy-start
  82.2 0.0 copy-start.5
  82.2 1.1 copy-done.5
  83.3 1.7 %shard_map.113 = (f32[2,3,256,128]{3,2,1,0:T(8,128)S(1)}, bf16[2,3,256,128]{3,2,1,0:T(8,128)(2,1)S(1)}) custom-call(s32[2]{0:T(128)S(1)} %copy-done.6, bf16[2,4,2,16,2,16,128]{6,5,4,3,2,1,0:T(8,128)(2,1)S(1)} %bitcast.10, bf16[256,1024]{1,0:T(8,128)(2,1)S(1)} %get-tuple-element.18.up_ref, bf16[128,1024]{1,0:T(8,128)(2,1)S(1)} %copy-done.5), custom_call_target="tpu_custom_call" | custom-call | flops 100000000 | bytes 2000000 | tf_op jit(solution)/shard_map/pallas_call | solution.py:94
  84.9 3.9 %collective-permute-start.1 = (bf16[2,3,256,128]{3,2,1,0:T(8,128)(2,1)S(1)}, bf16[2,3,256,128]{3,2,1,0:T(8,128)(2,1)S(1)}, u32[]{:S(2)}, u32[]{:S(2)}) collective-permute-start(bf16[2,3,256,128]{3,2,1,0:T(8,128)(2,1)S(1)} %get-tuple-element.21), channel_id=1, source_target_pairs={{0,1},{1,0},{2,3},{3,2},{4,5},{5,4},{6,7},{7,6},{8,9},{9,8},{10,11... | collective-permute-start | bytes 1179656 | tf_op jit(solution)/shard_map/ppermute | solution.py:352
  88.9 8.9 %collective-permute-done.1.got_ref = bf16[2,3,256,128]{3,2,1,0:T(8,128)(2,1)S(1)} collective-permute-done((bf16[2,3,256,128]{3,2,1,0:T(8,128)(2,1)S(1)}, bf16[2,3,256,128]{3,2,1,0:T(8,128)(2,1)S(1)}, u32[]{:S(2)}, u32[]{:S(2)}) %collective-permute-start.1) | collective-permute-done | bytes 393248 | tf_op jit(solution)/shard_map/ppermute | solution.py:352
  97.8 1.7 %shard_map.114 = (bf16[2,8,2,144,128]{4,3,2,1,0:T(8,128)(2,1)S(1)}, bf16[2,3,256,128]{3,2,1,0:T(8,128)(2,1)S(1)}) custom-call(s32[2]{0:T(128)S(1)} %copy-done.6, f32[2,3,256,128]{3,2,1,0:T(8,128)S(1)} %get-tuple-element.20.kept_ref, bf16[2,3,256,128]{3,2,1,0:T(8,128)(2,1)S(1)} %collective-permute-done.1.got_ref, bf16[256,1024]{1,0:T(8,128)(2,1)S(1)} %get-tuple-element.18.up_ref), custom_call_target="tpu_custom_call" | custom-call | flops 100000000 | bytes 2000000 | tf_op jit(solution)/shard_map/pallas_call | solution.py:94
  99.5 0.0 copy-done
  99.5 0.0 copy-start.10
  99.5 26.8 %all_to_all.21 = bf16[16,2,144,128]{3,2,1,0:T(8,128)(2,1)S(1)} all-to-all(bf16[16,2,144,128]{3,2,1,0:T(8,128)(2,1)S(1)} %bitcast.13), channel_id=1, replica_groups=mesh['z'=16,'c'=2,'y'=4,'u'=2,'v'=2] {'c','y','u'}, dimensions={0} | all-to-all | bytes 2359296 | tf_op jit(solution)/shard_map/all_to_all | solution.py:344
  126.3 0.0 copy-done.10
  126.3 1.6 %shard_map.115 = bf16[16,40,128]{2,1,0:T(8,128)(2,1)} custom-call(s32[2]{0:T(128)S(1)} %copy-done.6, bf16[2,8,2,144,128]{4,3,2,1,0:T(8,128)(2,1)S(1)} %bitcast.12), custom_call_target="tpu_custom_call" | custom-call | flops 100000000 | bytes 2000000 | tf_op jit(solution)/shard_map/pallas_call | solution.py:94
  127.9 5.5 %all-to-all-start.3 = ((bf16[16,40,128]{2,1,0:T(8,128)(2,1)}), bf16[16,40,128]{2,1,0:T(8,128)(2,1)S(1)}, u32[]{:S(2)}, u32[]{:S(2)}) async-start(bf16[16,40,128]{2,1,0:T(8,128)(2,1)} %shard_map.115), calls=%async_computation.3 | async-start | bytes 327680 | tf_op jit(solution)/shard_map/all_to_all | solution.py:344
  133.4 3.9 %shard_map.117 = (f32[192,1024]{1,0:T(8,128)}, bf16[192,1024]{1,0:T(8,128)(2,1)}) custom-call(s32[2]{0:T(128)} %pad_add_fusion.s_ref, bf16[2,4,2,16,2,16,128]{6,5,4,3,2,1,0:T(8,128)(2,1)} %bitcast.11, bf16[2,3,256,128]{3,2,1,0:T(8,128)(2,1)} %copy-done.10), custom_call_target="tpu_custom_call" | custom-call | flops 4000000000 | bytes 2000000 | tf_op jit(solution)/shard_map/pallas_call | solution.py:94
  137.3 0.0 copy-start.7
  137.3 0.0 copy-start.8
  137.3 0.0 copy-start.9
  137.3 2.0 %collective-permute-start.2 = (bf16[192,1024]{1,0:T(8,128)(2,1)}, bf16[192,1024]{1,0:T(8,128)(2,1)S(1)}, u32[]{:S(2)}, u32[]{:S(2)}) collective-permute-start(bf16[192,1024]{1,0:T(8,128)(2,1)} %get-tuple-element.27), channel_id=1, source_target_pairs={{0,1},{1,0},{2,3},{3,2},{4,5},{5,4},{6,7},{7,6},{8,9},{9,8},{10,11... | collective-permute-start | bytes 1179656 | tf_op jit(solution)/shard_map/ppermute | solution.py:352
  139.4 9.6 %collective-permute-done.2.got_ref = bf16[192,1024]{1,0:T(8,128)(2,1)S(1)} collective-permute-done((bf16[192,1024]{1,0:T(8,128)(2,1)}, bf16[192,1024]{1,0:T(8,128)(2,1)S(1)}, u32[]{:S(2)}, u32[]{:S(2)}) %collective-permute-start.2) | collective-permute-done | bytes 393248 | tf_op jit(solution)/shard_map/ppermute | solution.py:352
  148.9 0.0 copy-start.11
  148.9 0.7 copy-done.11
  149.7 3.2 %shard_map.118 = (f32[1,64,2048]{2,1,0:T(8,128)}, f32[1,64,2048]{2,1,0:T(8,128)}, f32[1,64,2048]{2,1,0:T(8,128)}) custom-call(s32[2]{0:T(128)} %pad_add_fusion.s_ref, f32[192,1024]{1,0:T(8,128)} %get-tuple-element.26.kept_ref, bf16[192,1024]{1,0:T(8,128)(2,1)} %copy-done.11), custom_call_target="tpu_custom_call" | custom-call | flops 1000000000 | bytes 2000000 | tf_op jit(solution)/shard_map/pallas_call | solution.py:94
  152.9 0.0 all-to-all-done.3.home_ref
  152.9 0.0 copy-done.7
  152.9 0.0 copy-done.8
  152.9 0.0 copy-done.9
  152.9 1.7 %shard_map.116 = (bf16[128,128]{1,0:T(8,128)(2,1)}, f32[2,128]{1,0:T(2,128)}) custom-call(s32[2]{0:T(128)S(1)} %copy-done.7, s32[2,128]{1,0:T(2,128)S(1)} %bitcast.15, bf16[2,128]{1,0:T(2,128)(2,1)S(1)} %bitcast.17, bf16[16,40,128]{2,1,0:T(8,128)(2,1)S(1)} %all-to-all-done.3.home_ref), custom_call_target="tpu_custom_call" | custom-call | flops 100000000 | bytes 2000000 | tf_op jit(solution)/shard_map/pallas_call | solution.py:94
  (1 shorter events, 0.0 us)
Async XLA Ops:
  35.2 45.5 %copy-start.1 = (bf16[1,64,2048]{2,1,0:T(8,128)(2,1)S(1)}, bf16[1,64,2048]{2,1,0:T(8,128)(2,1)}, u32[]{:S(2)}) copy-start(bf16[1,64,2048]{2,1,0:T(8,128)(2,1)} %wg_ref.3) | copy-start | bytes 786436
  35.2 45.5 %copy-start.2 = (bf16[1,64,2048]{2,1,0:T(8,128)(2,1)S(1)}, bf16[1,64,2048]{2,1,0:T(8,128)(2,1)}, u32[]{:S(2)}) copy-start(bf16[1,64,2048]{2,1,0:T(8,128)(2,1)} %wu_ref.3) | copy-start | bytes 786436
  35.2 45.5 %copy-start.3 = (bf16[1,64,2048]{2,1,0:T(8,128)(2,1)S(1)}, bf16[1,64,2048]{2,1,0:T(8,128)(2,1)}, u32[]{:S(2)}) copy-start(bf16[1,64,2048]{2,1,0:T(8,128)(2,1)} %wd_ref.3) | copy-start | bytes 786436
  35.2 45.5 %copy-start.6 = (s32[2]{0:T(128)S(1)}, s32[2]{0:T(128)}, u32[]{:S(2)}) copy-start(s32[2]{0:T(128)} %pad_add_fusion.s_ref) | copy-start | bytes 28
  35.2 46.9 %all-to-all-start.1 = ((bf16[16,16,2,16,128]{4,3,2,1,0:T(8,128)(2,1)}), bf16[16,16,2,16,128]{4,3,2,1,0:T(8,128)(2,1)S(1)}, u32[]{:S(2)}, u32[]{:S(2)}) async-start(bf16[16,16,2,16,128]{4,3,2,1,0:T(8,128)(2,1)} %bitcast.18), calls=%async_computation.1 | async-start | bytes 4194304 | tf_op jit(solution)/shard_map/all_to_all | solution.py:344
  50.5 30.2 %collective-permute-start = (bf16[3,64,1024]{2,1,0:T(8,128)(2,1)}, bf16[3,64,1024]{2,1,0:T(8,128)(2,1)S(1)}, u32[]{:S(2)}, u32[]{:S(2)}) collective-permute-start(bf16[3,64,1024]{2,1,0:T(8,128)(2,1)} %shard_map.111), channel_id=1, source_target_pairs={{0,1},{1,0},{2,3},{3,2},{4,5},{5,4},{6,7},{7,6},{8,9},{9,8},{10,11... | collective-permute-start | bytes 1179656 | tf_op jit(solution)/shard_map/ppermute | solution.py:352
  81.4 0.7 copy-start.4
  82.2 17.3 %copy-start = (bf16[16,16,2,16,128]{4,3,2,1,0:T(8,128)(2,1)}, bf16[16,16,2,16,128]{4,3,2,1,0:T(8,128)(2,1)S(1)}, u32[]{:S(2)}) copy-start(bf16[16,16,2,16,128]{4,3,2,1,0:T(8,128)(2,1)S(1)} %all-to-all-done.1) | copy-start | bytes 6291460
  82.2 1.1 copy-start.5
  84.9 12.8 %collective-permute-start.1 = (bf16[2,3,256,128]{3,2,1,0:T(8,128)(2,1)S(1)}, bf16[2,3,256,128]{3,2,1,0:T(8,128)(2,1)S(1)}, u32[]{:S(2)}, u32[]{:S(2)}) collective-permute-start(bf16[2,3,256,128]{3,2,1,0:T(8,128)(2,1)S(1)} %get-tuple-element.21), channel_id=1, source_target_pairs={{0,1},{1,0},{2,3},{3,2},{4,5},{5,4},{6,7},{7,6},{8,9},{9,8},{10,11... | collective-permute-start | bytes 1179656 | tf_op jit(solution)/shard_map/ppermute | solution.py:352
  99.5 26.8 %copy-start.10 = (bf16[2,3,256,128]{3,2,1,0:T(8,128)(2,1)}, bf16[2,3,256,128]{3,2,1,0:T(8,128)(2,1)S(1)}, u32[]{:S(2)}) copy-start(bf16[2,3,256,128]{3,2,1,0:T(8,128)(2,1)S(1)} %get-tuple-element.25.act_ref) | copy-start | bytes 1179652
  127.9 25.0 %all-to-all-start.3 = ((bf16[16,40,128]{2,1,0:T(8,128)(2,1)}), bf16[16,40,128]{2,1,0:T(8,128)(2,1)S(1)}, u32[]{:S(2)}, u32[]{:S(2)}) async-start(bf16[16,40,128]{2,1,0:T(8,128)(2,1)} %shard_map.115), calls=%async_computation.3 | async-start | bytes 327680 | tf_op jit(solution)/shard_map/all_to_all | solution.py:344
  137.3 15.6 %copy-start.7 = (s32[2]{0:T(128)S(1)}, s32[2]{0:T(128)}, u32[]{:S(2)}) copy-start(s32[2]{0:T(128)} %pad_add_fusion.s_ref) | copy-start | bytes 28
  137.3 15.6 %copy-start.8 = (s32[128,2]{0,1:T(2,128)S(1)}, s32[128,2]{0,1:T(2,128)}, u32[]{:S(2)}) copy-start(s32[128,2]{0,1:T(2,128)} %param.9) | copy-start | bytes 3076
  137.3 15.6 %copy-start.9 = (bf16[128,2]{0,1:T(2,128)(2,1)S(1)}, bf16[128,2]{0,1:T(2,128)(2,1)}, u32[]{:S(2)}) copy-start(bf16[128,2]{0,1:T(2,128)(2,1)} %param.10) | copy-start | bytes 1540
  137.3 11.6 %collective-permute-start.2 = (bf16[192,1024]{1,0:T(8,128)(2,1)}, bf16[192,1024]{1,0:T(8,128)(2,1)S(1)}, u32[]{:S(2)}, u32[]{:S(2)}) collective-permute-start(bf16[192,1024]{1,0:T(8,128)(2,1)} %get-tuple-element.27), channel_id=1, source_target_pairs={{0,1},{1,0},{2,3},{3,2},{4,5},{5,4},{6,7},{7,6},{8,9},{9,8},{10,11... | collective-permute-start | bytes 1179656 | tf_op jit(solution)/shard_map/ppermute | solution.py:352
  148.9 0.8 copy-start.11

commit v7 on v5

--- a/solution.py
+++ b/solution.py
@@ -51,15 +51,18 @@
     return first, second, rank, expand, chosen
 
 
-def dispatch_kernel(s_ref, ids_ref, w_ref, tok_ref, cot_ref, out_ref):
+def dispatch_kernel(s_ref, ids_ref, w_ref, tok_ref, cot_ref, own_ref, other_ref):
     first, second, _, expand, chosen = routing(ids_ref)
     w = w_ref[...].astype(F32)
     weighted = first * w[0:1, :] + second * w[1:2, :]
     scale = dot(expand, weighted.astype(BF), 1, 0)
     pick = jnp.where(chosen, 1.0, 0.0).astype(BF)
     pick_scaled = jnp.where(chosen, scale, 0.0).astype(BF)
-    out_ref[:, :, 0] = dot(pick, tok_ref[...], 1, 0).astype(BF).reshape(NZ, 2, CAP, COL)
-    out_ref[:, :, 1] = dot(pick_scaled, cot_ref[...], 1, 0).astype(BF).reshape(NZ, 2, CAP, COL)
+    first_core = s_ref[1] == 0
+    for i, rows in enumerate((dot(pick, tok_ref[...], 1, 0), dot(pick_scaled, cot_ref[...], 1, 0))):
+        rows = rows.reshape(NZ, 2, CAP, COL)
+        own_ref[:, i] = jnp.where(first_core, rows[:, 0], rows[:, 1]).astype(BF)
+        other_ref[:, i] = jnp.where(first_core, rows[:, 1], rows[:, 0]).astype(BF)
 
 
 def dispatch(where, ids, w, tokens, cotangent):
@@ -69,19 +72,24 @@
         where,
         (ids, w, tokens, cotangent),
         [full(2, TOK), full(2, TOK), mine, mine],
-        full(NZ, 2, 2, CAP, COL),
-        jax.ShapeDtypeStruct((NZ, 2, 2, CAP, COL), BF),
-    )
-
-
-def x_of(s_ref, k):
-    return (s_ref[1] + k) & 3
+        [full(NZ, 2, CAP, COL)] * 2,
+        [jax.ShapeDtypeStruct((NZ, 2, CAP, COL), BF)] * 2,
+    )
+
+
+def b_of(s_ref, k):
+    return (s_ref[2] + k) & 3
+
+
+def block(s_ref, a, b):
+    j = jnp.where(s_ref[1] == 0, a * 4 + b, b * 4 + a)
+    return pl.ds(pl.multiple_of(j * COL, COL), COL)
 
 
 def pack_kernel(s_ref, wg_ref, wu_ref, wd_ref, *out_refs):
     for k, out_ref in enumerate(out_refs):
         for y in range(4):
-            cols = pl.ds(pl.multiple_of((y * 4 + x_of(s_ref, k)) * COL, COL), COL)
+            cols = block(s_ref, y, b_of(s_ref, k))
             out_ref[y, :HID] = wg_ref[0, :, cols]
             out_ref[y, HID : 2 * HID] = wu_ref[0, :, cols]
             out_ref[y, 2 * HID :] = wd_ref[0, :, cols]
@@ -124,7 +132,7 @@
 
 
 def features(x_ref, which, rows):
-    return jnp.concatenate([x_ref[:, y, :, which].reshape(rows, COL) for y in range(4)], axis=1)
+    return jnp.concatenate([x_ref[y, :, :, which].reshape(rows, COL) for y in range(4)], axis=1)
 
 
 def layout_kernel(s_ref, w0_ref, w1_ref, w2_ref, w3_ref, wgu_ref, wdd_ref):
@@ -154,7 +162,7 @@
     back = dot(features(x_ref, 1, RB), wdd_ref[...], 1, 1)
     for k in range(4):
         cols = slice(k * COL, (k + 1) * COL)
-        to = x_of(s_ref, -k)
+        to = b_of(s_ref, -k)
         half = back[:, cols]
         out_ref[to, 0, :RB] = pre[:, cols]
         out_ref[to, 0, RB:] = jnp.where(low_lanes(RB // 2), half[: RB // 2], half[RB // 2 :]).astype(BF)
@@ -162,7 +170,6 @@
 
 PRE = RB + RB // 2
 ACT = PRE + EXT
-HOME = RB // 2 + EXT
 
 
 def pre_activations(where, x, wgu, wdd):
@@ -171,7 +178,7 @@
         where,
         (x, wgu, wdd),
         [
-            pl.BlockSpec((2, 4, NZ // BLK, 2, CAP, COL), lambda i, s: (0, 0, i, 0, 0, 0)),
+            pl.BlockSpec((4, NZ // BLK, 2, 2, CAP, COL), lambda i, s: (0, i, 0, 0, 0, 0)),
             full(4 * COL, 4 * COL),
             full(4 * COL, 4 * COL),
         ],
@@ -236,18 +243,15 @@
 
 
 def back_kernel(s_ref, g_ref, w_ref, out_ref):
-    grads = jnp.concatenate([g_ref[x_of(s_ref, -k), 0, :RB] for k in range(4)], axis=1)
+    grads = jnp.concatenate([g_ref[b_of(s_ref, -k), 0, :RB] for k in range(4)], axis=1)
     pieces = dot(grads, w_ref[...], 1, 0).astype(BF)
     parts = g_ref[0, 0, PRE:].astype(F32)
     for x in range(1, 4):
         parts = parts + g_ref[x, 0, PRE:].astype(F32)
-    sums = one_sum(parts)
-    half = RB // 2
-    for core in range(2):
-        extra = two_parts(sums if core == 0 else pltpu.roll(sums, EXT // 2, 0))
-        for y in range(4):
-            out_ref[core, y, 0, :half] = pieces[core * half : (core + 1) * half, y * COL : (y + 1) * COL]
-            out_ref[core, y, 0, half:] = extra
+    extra = two_parts(one_sum(parts))
+    for y in range(4):
+        out_ref[y, 0, :RB] = pieces[:, y * COL : (y + 1) * COL]
+        out_ref[y, 0, RB:] = extra
 
 
 def back(where, g, w):
@@ -256,8 +260,8 @@
         where,
         (g, w),
         [pl.BlockSpec((4, 1, ACT, COL), lambda i, s: (0, i, 0, 0)), full(4 * COL, 4 * COL)],
-        pl.BlockSpec((2, 4, 1, HOME, COL), lambda i, s: (0, 0, i, 0, 0)),
-        jax.ShapeDtypeStruct((2, 4, BLK, HOME, COL), BF),
+        pl.BlockSpec((4, 1, RB + EXT, COL), lambda i, s: (0, i, 0, 0)),
+        jax.ShapeDtypeStruct((4, BLK, RB + EXT, COL), BF),
         grid=BLK,
         vmem=SMALL,
     )
@@ -265,10 +269,10 @@
 
 def weights_kernel(s_ref, x_ref, g_ref, own_ref, *out_refs):
     near = NZ // BLK
-    blocks = [x_ref.at[:, :, b * near : (b + 1) * near] for b in range(BLK)]
+    blocks = [x_ref.at[:, b * near : (b + 1) * near] for b in range(BLK)]
     tok, cot = (jnp.concatenate([features(b, which, RB) for b in blocks], axis=0) for which in range(2))
     for k, out_ref in enumerate((own_ref, *out_refs)):
-        owner = x_of(s_ref, k)
+        owner = b_of(s_ref, k)
         grads = jnp.concatenate([g_ref[owner, b, :RB] for b in range(BLK)], axis=0)
         halves = []
         for b in range(BLK):
@@ -286,7 +290,7 @@
         weights_kernel,
         where,
         (x, g),
-        [full(2, 4, NZ, 2, CAP, COL), full(4, BLK, ACT, COL)],
+        [full(4, NZ, 2, 2, CAP, COL), full(4, BLK, ACT, COL)],
         [full(*shape)] * 4,
         [jax.ShapeDtypeStruct(shape, F32)] + [jax.ShapeDtypeStruct(shape, BF)] * 3,
         flops=4 * 10**9,
@@ -297,7 +301,7 @@
     *parts, dg_ref, du_ref, dd_ref = refs
     for k, p_ref in enumerate(parts):
         for y in range(4):
-            cols = pl.ds(pl.multiple_of((y * 4 + x_of(s_ref, -k)) * COL, COL), COL)
+            cols = block(s_ref, y, b_of(s_ref, -k))
             here = slice(y * COL, (y + 1) * COL)
             dg_ref[0, :, cols] = p_ref[:HID, here].astype(F32)
             du_ref[0, :, cols] = p_ref[HID : 2 * HID, here].astype(F32)
@@ -318,16 +322,16 @@
 
 
 def total_kernel(s_ref, p_ref, out_ref):
-    half, sums = RB // 2, []
-    for core in range(2):
-        rows = p_ref[core, 0, 0].astype(F32)
-        for y in range(1, 4):
-            rows = rows + p_ref[core, y, 0].astype(F32)
-        out_ref[:, core * CAP : (core + 1) * CAP] = rows[:half].astype(BF).reshape(NZ // BLK, CAP, COL)
-        sums.append(one_sum(rows[half:]))
-    extra = two_parts(jnp.where((iota((EXT, COL), 1) & 31) < 16, *sums)).astype(F32)
-    for k in range(NZ // BLK):
-        out_ref[k, 2 * CAP :] = jnp.broadcast_to(extra[k : k + 1], (DUP, COL)).astype(BF)
+    rows = p_ref[0, 0].astype(F32)
+    for y in range(1, 4):
+        rows = rows + p_ref[y, 0].astype(F32)
+    near = NZ // BLK
+    out_ref[:, : 2 * CAP] = rows[:RB].astype(BF).reshape(near, 2 * CAP, COL)
+    sums = two_parts(one_sum(rows[RB:])).astype(F32)
+    left = (iota((DUP, COL), 1) & 31) < 16
+    for k in range(near):
+        pair = [jnp.broadcast_to(sums[i : i + 1], (DUP, COL)) for i in (2 * k, 2 * k + 1)]
+        out_ref[k, 2 * CAP :] = jnp.where(left, *pair).astype(BF)
 
 
 def total(where, part):
@@ -335,7 +339,7 @@
         total_kernel,
         where,
         (part,),
-        [pl.BlockSpec((2, 4, 1, HOME, COL), lambda i, s: (0, 0, i, 0, 0))],
+        [pl.BlockSpec((4, 1, RB + EXT, COL), lambda i, s: (0, i, 0, 0))],
         pl.BlockSpec((NZ // BLK, 2 * CAP + DUP, COL), lambda i, s: (i, 0, 0)),
         jax.ShapeDtypeStruct((NZ, 2 * CAP + DUP, COL), BF),
         grid=BLK,
@@ -343,74 +347,117 @@
     )
 
 
-def combine_kernel(s_ref, ids_ref, w_ref, home_ref, tok_ref, route_ref):
+def combine_kernel(s_ref, ids_ref, w_ref, home_ref, far_ref, tok_ref, route_ref):
+    core = s_ref[1]
     first, second, rank, _, chosen = routing(ids_ref)
     pick = jnp.where(chosen, 1.0, 0.0).astype(BF)
-    rows = home_ref[:, : 2 * CAP].reshape(2 * NZ * CAP, COL)
+    home, far = home_ref[:, :CAP], far_ref[:, :CAP]
+    low = jnp.where(core == 0, home, far)
+    high = jnp.where(core == 0, far, home)
+    rows = jnp.concatenate([low, high], axis=1).reshape(2 * NZ * CAP, COL)
     tok_ref[...] = dot(pick, rows, 0, 0).astype(BF)
-    sums = home_ref[:, 2 * CAP :].reshape(NZ * DUP, COL)
+    home_sums = home_ref[:, 2 * CAP :].reshape(NZ * DUP, COL)
+    far_sums = far_ref[:, CAP:].reshape(NZ * DUP, COL)
     row = iota((NZ * DUP, TOK), 0)
+    leads, chip = (row & 7) == 0, row >> 3
     lane = iota((COL, TOK), 0)
     w = w_ref[...].astype(F32)
     for k, member in enumerate((first, second)):
         ids = ids_ref[k : k + 1, :]
-        at = jnp.sum(member * rank, axis=0, keepdims=True).astype(I32) + 16 * (ids & 1)
-        chip = (((row & 7) == 0) & ((row >> 3) == (ids >> 1))).astype(BF)
-        found = dot(sums, chip, 0, 0)
-        found = jnp.where((lane == at) | (lane == at + 32), found, 0.0)
-        route_ref[k : k + 1, :] = jnp.sum(found, axis=0, keepdims=True) / w[k : k + 1, :]
-
-
-def combine(where, ids, w, home):
+        at = jnp.sum(member * rank, axis=0, keepdims=True).astype(I32)
+        near = dot(home_sums, (leads & (ids == 2 * chip + core)).astype(BF), 0, 0)
+        away = dot(far_sums, (leads & (ids == 2 * chip + 1 - core)).astype(BF), 0, 0)
+        near = jnp.where((lane == at) | (lane == at + 32), near, 0.0)
+        away = jnp.where((lane == at + 16) | (lane == at + 48), away, 0.0)
+        route_ref[k : k + 1, :] = jnp.sum(near + away, axis=0, keepdims=True) / w[k : k + 1, :]
+
+
+def combine(where, ids, w, home, far):
     return call(
         combine_kernel,
         where,
-        (ids, w, home),
-        [full(2, TOK), full(2, TOK), full(NZ, 2 * CAP + DUP, COL)],
+        (ids, w, home, far),
+        [
+            full(2, TOK),
+            full(2, TOK),
+            full(NZ, 2 * CAP + DUP, COL),
+            full(NZ, CAP + DUP, COL),
+        ],
         [full(TOK, COL), full(2, TOK)],
         [jax.ShapeDtypeStruct((TOK, COL), BF), jax.ShapeDtypeStruct((2, TOK), F32)],
         vmem=4 * 2**20,
     )
 
 
+PLANE = ("c", "y", "x")
+
+
+def device(core, a, b):
+    return core * 16 + (a * 4 + b if core == 0 else b * 4 + a)
+
+
+def lines(first):
+    places = [[(a, b) if first else (b, a) for a in range(4)] for b in range(4)]
+    return [[device(core, a, b) for a, b in line] for core in range(2) for line in places]
+
+
 def exchange(x, axis):
     return lax.all_to_all(x, axis, split_axis=0, concat_axis=0, tiled=True)
 
 
+def line_exchange(x, first):
+    return lax.all_to_all(
+        x, PLANE, split_axis=0, concat_axis=0, tiled=True, axis_index_groups=lines(first)
+    )
+
+
+def shifted(x, by):
+    pairs = [
+        (device(core, a, b), device(core, a, (b + by) % 4))
+        for core in range(2)
+        for a in range(4)
+        for b in range(4)
+    ]
+    return lax.ppermute(x, PLANE, pairs)
+
+
+def swapped(x):
+    return lax.ppermute(x, "c", [(0, 1), (1, 0)])
+
+
 def copies(x, n):
     return jnp.broadcast_to(x[None], (n, *x.shape))
 
 
-def shifted(x, axis, by):
-    n = lax.axis_size(axis)
-    return lax.ppermute(x, axis, [(i, (i + by) % n) for i in range(n)])
-
-
 def row_weights(where, wg, wu, wd):
     own, *others = pack(where, wg, wu, wd)
-    moved = [shifted(other, "x", k + 1) for k, other in enumerate(others)]
+    moved = [shifted(other, k + 1) for k, other in enumerate(others)]
     return layout(where, (own, *moved))
 
 
 def per_device(tokens, cotangent, expert_ids, route_weight, gate_weight, up_weight, down_weight):
-    y, x = lax.axis_index("y"), lax.axis_index("x")
-    where = jnp.stack([y * 4 + x, x]).astype(I32)
+    y, x, core = lax.axis_index("y"), lax.axis_index("x"), lax.axis_index("c")
+    where = jnp.stack([y * 4 + x, core, jnp.where(core == 0, x, y)]).astype(I32)
     ids, w = expert_ids.T, route_weight.T
-    mine = exchange(dispatch(where, ids, w, tokens, cotangent), "z")
+    own, other = dispatch(where, ids, w, tokens, cotangent)
+    mine = jnp.stack([own, swapped(other)], axis=1)
+    mine = exchange(mine, "z")
     wgu, wdd = row_weights(where, gate_weight, up_weight, down_weight)
-    both = copies(mine.transpose(1, 0, 2, 3, 4), 4).transpose(1, 0, 2, 3, 4, 5)
-    rows = exchange(both.reshape(8, NZ, 2, CAP, COL), ("c", "y")).reshape(both.shape)
+    rows = line_exchange(copies(mine, 4), True)
     pre = pre_activations(where, rows, wgu, wdd)
-    pre = exchange(pre, "x")
+    pre = line_exchange(pre, False)
     g = activations(where, pre)
-    g = exchange(g, "x")
+    g = line_exchange(g, False)
     part = back(where, g, wgu)
-    sums = exchange(part.reshape(8, BLK, HOME, COL), ("c", "y")).reshape(part.shape)
+    sums = line_exchange(part, True)
     kept, *sent = weights(where, rows, g)
     home = exchange(total(where, sums), "z")
-    moved = [shifted(part, "x", k + 1) for k, part in enumerate(sent)]
+    moved = []
+    for k, part in enumerate(sent):
+        moved.append(shifted(part, k + 1))
     gate_grad, up_grad, down_grad = assemble(where, (kept, *moved))
-    tokens_grad, route_grad = combine(where, ids, w, home)
+    far = swapped(home[:, CAP:])
+    tokens_grad, route_grad = combine(where, ids, w, home, far)
     return tokens_grad, route_grad.T, gate_grad, up_grad, down_grad
 
 

time: 148 us -> 142 us (0.959)
  blocking collectives: 74.5 us -> 56.8 us
  starting transfers between devices: 34.6 us -> 51.3 us
  waiting for transfers between devices: 12.8 us -> 6.4 us
    all_to_all x4 -> x1, blocking collectives: 74.5 us -> 23.4 us  [exchange(): return lax.all_to_all(x, axis, split_axis=0, concat_axis=0, tiled=True)]
    all_to_all x0 -> x3, blocking collectives: none -> 33.4 us  [line_exchange(): lax.all_to_all(x, PLANE, split_axis=0, concat_axis=0, tiled=True, axis_in...]
    ppermute x6 -> x8, starting transfers between devices: 19.1 us -> 38 us  [the longest x6 19.3 us: shifted(): return lax.ppermute(x, PLANE, pairs)]
    ppermute x6 -> x8, waiting for transfers between devices: 12.8 us -> 6.4 us  [the longest x6 5.22 us: shifted(): return lax.ppermute(x, PLANE, pairs)]
    all_to_all x2 -> x1, starting transfers between devices: 15.5 us -> 9.24 us  [exchange(): return lax.all_to_all(x, axis, split_axis=0, concat_axis=0, tiled=True)]
    all_to_all x0 -> x1, starting transfers between devices: none -> 4.01 us  [line_exchange(): lax.all_to_all(x, PLANE, split_axis=0, concat_axis=0, tiled=True, axis_in...]
  transfers between devices with their start and end apart: 8 -> 10, of which waited for: 5 -> 3; matrix products, arithmetic and copies ran while one was open for 0% -> 0% of each run, Pallas kernels for 7% -> 7%
where the time goes in v7:
time: 142 us; the launch traced here: 141 us
  blocking collectives  56.8 us (40%)
  starting transfers between devices  51.3 us (36%)
  Pallas kernels  20.8 us (15%)
  waiting for transfers between devices  6.4 us (5%)
  local copies, waits for them, and re-layouts  3.05 us (2%)
  other arithmetic  1.58 us (1%)
    all_to_all x3, blocking collectives, line_exchange(): lax.all_to_all(x, PLANE, split_axis=0, concat_axis=0, tiled=True, axis_in...  33.4 us
    all_to_all x1, blocking collectives, exchange(): return lax.all_to_all(x, axis, split_axis=0, concat_axis=0, tiled=True)  23.4 us
    pallas_call x10, Pallas kernels, call(): pl.pallas_call(kernel, grid_spec=pltpu.PrefetchScalarGridSpec(num_scalar_...  20.8 us
    ppermute x6, starting transfers between devices, shifted(): return lax.ppermute(x, PLANE, pairs)  19.3 us
    ppermute x2, starting transfers between devices, swapped(): return lax.ppermute(x, 'c', [(0, 1), (1, 0)])  18.7 us
    all_to_all x1, starting transfers between devices, exchange(): return lax.all_to_all(x, axis, split_axis=0, concat_axis=0, tiled=True)  9.24 us
    ppermute x6, waiting for transfers between devices, shifted(): return lax.ppermute(x, PLANE, pairs)  5.22 us
    all_to_all x1, starting transfers between devices, line_exchange(): lax.all_to_all(x, PLANE, split_axis=0, concat_axis=0, tiled=True, axis_in...  4.01 us
  transfers between devices with their start and end apart: 10, of which 3 were waited for; matrix products, arithmetic and copies ran while one was open for 0% of the time, Pallas kernels for 7%

profile of v7, /device:TPU:1, one launch (start us, length us, event | category | flops | bytes accessed | tf_op | source)
XLA Modules:
  0.0 140.8 jit_solution(15509191216010140690)
XLA Ops:
  0.6 0.7 pad_add_fusion.s_ref
  1.3 2.6 %shard_map.110 = (bf16[16,2,16,128]{3,2,1,0:T(8,128)(2,1)}, bf16[16,2,16,128]{3,2,1,0:T(8,128)(2,1)}) custom-call(s32[3]{0:T(128)} %pad_add_fusion.s_ref, s32[2,128]{1,0:T(2,128)} %bitcast.8, bf16[2,128]{1,0:T(2,128)(2,1)} %bitcast.10, bf16[128,2048]{1,0:T(8,128)(2,1)} %tok_ref.1, bf16[128,2048]{1,0:T(8,128)(2,1)} %cot_ref.1), custom_call_target="tpu_custom_call" | custom-call | flops 100000000 | bytes 2000000 | tf_op jit(solution)/shard_map/pallas_call | solution.py:103
  3.9 8.7 %collective-permute-start = (bf16[16,2,16,128]{3,2,1,0:T(8,128)(2,1)}, bf16[16,2,16,128]{3,2,1,0:T(8,128)(2,1)S(1)}, u32[]{:S(2)}, u32[]{:S(2)}) collective-permute-start(bf16[16,2,16,128]{3,2,1,0:T(8,128)(2,1)} %get-tuple-element.23), channel_id=1, source_target_pairs={{0,16},{16,0},{1,17},{17,1},{2,18},{18,2},{3,19},{19,3},{4,20},{20... | collective-permute-start | bytes 393224 | tf_op jit(solution)/shard_map/ppermute | solution.py:425
  12.7 1.2 collective-permute-done
  13.9 0.9 pad_maximum_fusion
  14.8 23.4 %all_to_all.30 = bf16[16,2,2,16,128]{4,3,2,1,0:T(8,128)(2,1)S(1)} all-to-all(bf16[16,2,2,16,128]{4,3,2,1,0:T(8,128)(2,1)S(1)} %copy.13), channel_id=1, replica_groups=mesh['z'=16,'c'=2,'y'=4,'x'=4] {'z'}, dimensions={0} | all-to-all | bytes 524288 | tf_op jit(solution)/shard_map/all_to_all | solution.py:405
  38.2 1.3 broadcast_in_dim.2
  39.5 4.0 %all-to-all-start.1 = ((bf16[4,16,2,2,16,128]{5,4,3,2,1,0:T(8,128)(2,1)}), bf16[4,16,2,2,16,128]{5,4,3,2,1,0:T(8,128)(2,1)S(1)}, u32[]{:S(2)}, u32[]{:S(2)}) async-start(bf16[4,16,2,2,16,128]{5,4,3,2,1,0:T(8,128)(2,1)} %broadcast_in_dim.2), calls=%async_computation.1 | async-start | bytes 2097152 | tf_op jit(solution)/shard_map/all_to_all | solution.py:409
  43.5 2.8 %shard_map.111 = (bf16[4,192,128]{2,1,0:T(8,128)(2,1)}, bf16[4,192,128]{2,1,0:T(8,128)(2,1)}, bf16[4,192,128]{2,1,0:T(8,128)(2,1)}, bf16[4,192,128]{2,1,0:T(8,128)(2,1)}) custom-call(s32[3]{0:T(128)} %pad_add_fusion.s_ref, bf16[1,64,2048]{2,1,0:T(8,128)(2,1)} %wg_ref.1, bf16[1,64,2048]{2,1,0:T(8,128)(2,1)} %wu_ref.1, bf16[1,64,2048]{2,1,0:T(8,128)(2,1)} %wd_ref.1), custom_call_target="tpu_custom_call" | custom-call | flops 100000000 | bytes 2000000 | tf_op jit(solution)/shard_map/pallas_call | solution.py:103
  46.3 3.2 %collective-permute-start.1 = (bf16[4,192,128]{2,1,0:T(8,128)(2,1)}, bf16[4,192,128]{2,1,0:T(8,128)(2,1)S(1)}, u32[]{:S(2)}, u32[]{:S(2)}) collective-permute-start(bf16[4,192,128]{2,1,0:T(8,128)(2,1)} %get-tuple-element.25), channel_id=1, source_target_pairs={{0,1},{1,2},{2,3},{3,0},{4,5},{5,6},{6,7},{7,4},{8,9},{9,10},{10,1... | collective-permute-start | bytes 589832 | tf_op jit(solution)/shard_map/ppermute | solution.py:421
  49.5 4.5 %collective-permute-start.2 = (bf16[4,192,128]{2,1,0:T(8,128)(2,1)}, bf16[4,192,128]{2,1,0:T(8,128)(2,1)S(1)}, u32[]{:S(2)}, u32[]{:S(2)}) collective-permute-start(bf16[4,192,128]{2,1,0:T(8,128)(2,1)} %get-tuple-element.26), channel_id=1, source_target_pairs={{0,2},{1,3},{2,0},{3,1},{4,6},{5,7},{6,4},{7,5},{8,10},{9,11},{10,... | collective-permute-start | bytes 589832 | tf_op jit(solution)/shard_map/ppermute | solution.py:421
  54.1 0.0 copy-start.3
  54.1 3.0 %collective-permute-start.3 = (bf16[4,192,128]{2,1,0:T(8,128)(2,1)}, bf16[4,192,128]{2,1,0:T(8,128)(2,1)S(1)}, u32[]{:S(2)}, u32[]{:S(2)}) collective-permute-start(bf16[4,192,128]{2,1,0:T(8,128)(2,1)} %get-tuple-element.27), channel_id=1, source_target_pairs={{0,3},{1,0},{2,1},{3,2},{4,7},{5,4},{6,5},{7,6},{8,11},{9,8},{10,9... | collective-permute-start | bytes 589832 | tf_op jit(solution)/shard_map/ppermute | solution.py:421
  57.0 0.0 collective-permute-done.1.w1_ref
  57.1 4.6 %collective-permute-done.2.w2_ref = bf16[4,192,128]{2,1,0:T(8,128)(2,1)S(1)} collective-permute-done((bf16[4,192,128]{2,1,0:T(8,128)(2,1)}, bf16[4,192,128]{2,1,0:T(8,128)(2,1)S(1)}, u32[]{:S(2)}, u32[]{:S(2)}) %collective-permute-start.2) | collective-permute-done | bytes 196640 | tf_op jit(solution)/shard_map/ppermute | solution.py:421
  61.6 0.7 collective-permute-done.3.w3_ref
  62.3 0.0 copy-done.3
  62.3 0.9 copy-done.2
  63.2 0.7 shard_map.112
  63.9 0.0 all-to-all-done.1.x_ref
  63.9 0.0 copy-start
  63.9 1.7 %shard_map.113 = bf16[4,2,384,128]{3,2,1,0:T(8,128)(2,1)S(1)} custom-call(s32[3]{0:T(128)S(1)} %copy-done.3, bf16[4,16,2,2,16,128]{5,4,3,2,1,0:T(8,128)(2,1)S(1)} %all-to-all-done.1.x_ref, bf16[512,512]{1,0:T(8,128)(2,1)S(1)} %get-tuple-element.28.wgu_ref.w_ref, bf16[512,512]{1,0:T(8,128)(2,1)S(1)} %get-tuple-element.29.wdd_ref), custom_call_target="tpu_custom_call" | custom-call | flops 100000000 | bytes 2000000 | tf_op jit(solution)/shard_map/pallas_call | solution.py:103
  65.6 0.0 copy-done
  65.6 11.6 %all_to_all.31.p_ref = bf16[4,2,384,128]{3,2,1,0:T(8,128)(2,1)S(1)} all-to-all(bf16[4,2,384,128]{3,2,1,0:T(8,128)(2,1)S(1)} %shard_map.113), channel_id=1, replica_groups={{0,1,2,3},{4,5,6,7},{8,9,10,11},{12,13,14,15},{16,20,24,28},{17,21,25,2..., dimensions={0} | all-to-all | bytes 1572864 | tf_op jit(solution)/shard_map/all_to_all | solution.py:409
  77.2 1.5 %shard_map.114 = bf16[4,2,400,128]{3,2,1,0:T(8,128)(2,1)S(1)} custom-call(s32[3]{0:T(128)S(1)} %copy-done.3, bf16[4,2,384,128]{3,2,1,0:T(8,128)(2,1)S(1)} %all_to_all.31.p_ref), custom_call_target="tpu_custom_call" | custom-call | flops 100000000 | bytes 2000000 | tf_op jit(solution)/shard_map/pallas_call | solution.py:103
  78.7 10.9 %all_to_all.32.g_ref = bf16[4,2,400,128]{3,2,1,0:T(8,128)(2,1)S(1)} all-to-all(bf16[4,2,400,128]{3,2,1,0:T(8,128)(2,1)S(1)} %shard_map.114), channel_id=1, replica_groups={{0,1,2,3},{4,5,6,7},{8,9,10,11},{12,13,14,15},{16,20,24,28},{17,21,25,2..., dimensions={0} | all-to-all | bytes 1638400 | tf_op jit(solution)/shard_map/all_to_all | solution.py:409
  89.6 1.3 shard_map.115
  90.9 0.0 copy-done.1
  90.9 11.0 %all_to_all.33.p_ref = bf16[4,2,272,128]{3,2,1,0:T(8,128)(2,1)S(1)} all-to-all(bf16[4,2,272,128]{3,2,1,0:T(8,128)(2,1)S(1)} %shard_map.115), channel_id=1, replica_groups={{0,4,8,12},{1,5,9,13},{2,6,10,14},{3,7,11,15},{16,17,18,19},{20,21,22,2..., dimensions={0} | all-to-all | bytes 1114112 | tf_op jit(solution)/shard_map/all_to_all | solution.py:409
  101.8 1.6 %shard_map.116 = bf16[16,40,128]{2,1,0:T(8,128)(2,1)} custom-call(s32[3]{0:T(128)S(1)} %copy-done.3, bf16[4,2,272,128]{3,2,1,0:T(8,128)(2,1)S(1)} %all_to_all.33.p_ref), custom_call_target="tpu_custom_call" | custom-call | flops 100000000 | bytes 2000000 | tf_op jit(solution)/shard_map/pallas_call | solution.py:103
  103.4 9.2 %all-to-all-start.5 = ((bf16[16,40,128]{2,1,0:T(8,128)(2,1)}), bf16[16,40,128]{2,1,0:T(8,128)(2,1)S(1)}, u32[]{:S(2)}, u32[]{:S(2)}) async-start(bf16[16,40,128]{2,1,0:T(8,128)(2,1)} %shard_map.116), calls=%async_computation.5 | async-start | bytes 327680 | tf_op jit(solution)/shard_map/all_to_all | solution.py:405
  112.7 3.6 %shard_map.118 = (f32[192,512]{1,0:T(8,128)}, bf16[192,512]{1,0:T(8,128)(2,1)}, bf16[192,512]{1,0:T(8,128)(2,1)}, bf16[192,512]{1,0:T(8,128)(2,1)}) custom-call(s32[3]{0:T(128)} %pad_add_fusion.s_ref, bf16[4,16,2,2,16,128]{5,4,3,2,1,0:T(8,128)(2,1)} %copy-done, bf16[4,2,400,128]{3,2,1,0:T(8,128)(2,1)} %copy-done.1), custom_call_target="tpu_custom_call" | custom-call | flops 4000000000 | bytes 2000000 | tf_op jit(solution)/shard_map/pallas_call | solution.py:103
  116.3 2.2 %collective-permute-start.5 = (bf16[192,512]{1,0:T(8,128)(2,1)}, bf16[192,512]{1,0:T(8,128)(2,1)S(1)}, u32[]{:S(2)}, u32[]{:S(2)}) collective-permute-start(bf16[192,512]{1,0:T(8,128)(2,1)} %get-tuple-element.33), channel_id=1, source_target_pairs={{0,1},{1,2},{2,3},{3,0},{4,5},{5,6},{6,7},{7,4},{8,9},{9,10},{10,1... | collective-permute-start | bytes 589832 | tf_op jit(solution)/shard_map/ppermute | solution.py:421
  118.5 3.4 %collective-permute-start.6 = (bf16[192,512]{1,0:T(8,128)(2,1)}, bf16[192,512]{1,0:T(8,128)(2,1)S(1)}, u32[]{:S(2)}, u32[]{:S(2)}) collective-permute-start(bf16[192,512]{1,0:T(8,128)(2,1)} %get-tuple-element.34), channel_id=1, source_target_pairs={{0,2},{1,3},{2,0},{3,1},{4,6},{5,7},{6,4},{7,5},{8,10},{9,11},{10,... | collective-permute-start | bytes 589832 | tf_op jit(solution)/shard_map/ppermute | solution.py:421
  121.9 3.0 %collective-permute-start.7 = (bf16[192,512]{1,0:T(8,128)(2,1)}, bf16[192,512]{1,0:T(8,128)(2,1)S(1)}, u32[]{:S(2)}, u32[]{:S(2)}) collective-permute-start(bf16[192,512]{1,0:T(8,128)(2,1)} %get-tuple-element.35), channel_id=1, source_target_pairs={{0,3},{1,0},{2,1},{3,2},{4,7},{5,4},{6,5},{7,6},{8,11},{9,8},{10,9... | collective-permute-start | bytes 589832 | tf_op jit(solution)/shard_map/ppermute | solution.py:421
  124.9 0.0 all-to-all-done.5.home_ref
  124.9 10.0 %collective-permute-start.4 = (bf16[16,24,128]{2,1,0:T(8,128)(2,1)S(1)}, bf16[16,24,128]{2,1,0:T(8,128)(2,1)S(1)}, u32[]{:S(2)}, u32[]{:S(2)}) collective-permute-start(bf16[16,24,128]{2,1,0:T(8,128)(2,1)S(1)} %slice.4), channel_id=1, source_target_pairs={{0,16},{16,0},{1,17},{17,1},{2,18},{18,2},{3,19},{19,3},{4,20},{20... | collective-permute-start | bytes 294920 | tf_op jit(solution)/shard_map/ppermute | solution.py:425
  134.9 0.0 collective-permute-done.5.refs_1_
  134.9 0.0 copy-start.7
  135.0 0.0 collective-permute-done.6.refs_2_
  135.0 0.0 collective-permute-done.7.refs_3_
  135.0 0.6 copy-done.7
  135.6 0.1 copy-done.8
  135.7 0.1 copy-done.9
  135.8 3.3 %shard_map.119 = (f32[1,64,2048]{2,1,0:T(8,128)}, f32[1,64,2048]{2,1,0:T(8,128)}, f32[1,64,2048]{2,1,0:T(8,128)}) custom-call(s32[3]{0:T(128)} %pad_add_fusion.s_ref, f32[192,512]{1,0:T(8,128)} %get-tuple-element.32.refs_0_, bf16[192,512]{1,0:T(8,128)(2,1)} %copy-done.7, bf16[192,512]{1,0:T(8,128)(2,1)} %copy-done.8, bf16[192,512]{1,0:T(8,128)(2,1)} %copy-done.9), custom_call_target="tpu_custom_call" | custom-call | flops 1000000000 | bytes 2000000 | tf_op jit(solution)/shard_map/pallas_call | solution.py:103
  139.1 0.0 collective-permute-done.4.far_ref
  139.1 0.0 copy-done.6
  139.1 1.7 %shard_map.117 = (bf16[128,128]{1,0:T(8,128)(2,1)}, f32[2,128]{1,0:T(2,128)}) custom-call(s32[3]{0:T(128)S(1)} %copy-done.4, s32[2,128]{1,0:T(2,128)S(1)} %bitcast.9, bf16[2,128]{1,0:T(2,128)(2,1)S(1)} %bitcast.11, bf16[16,40,128]{2,1,0:T(8,128)(2,1)S(1)} %all-to-all-done.5.home_ref, bf16[16,24,128]{2,1,0:T(8,128)(2,1)S(1)} %collective-permute-done.4.far_ref), custom_call_target="tpu_custom_call" | custom-call | flops 100000000 | bytes 2000000 | tf_op jit(solution)/shard_map/pallas_call | solution.py:103
  (11 shorter events, 0.0 us)
Async XLA Ops:
  3.9 9.9 %collective-permute-start = (bf16[16,2,16,128]{3,2,1,0:T(8,128)(2,1)}, bf16[16,2,16,128]{3,2,1,0:T(8,128)(2,1)S(1)}, u32[]{:S(2)}, u32[]{:S(2)}) collective-permute-start(bf16[16,2,16,128]{3,2,1,0:T(8,128)(2,1)} %get-tuple-element.23), channel_id=1, source_target_pairs={{0,16},{16,0},{1,17},{17,1},{2,18},{18,2},{3,19},{19,3},{4,20},{20... | collective-permute-start | bytes 393224 | tf_op jit(solution)/shard_map/ppermute | solution.py:425
  39.5 24.4 %all-to-all-start.1 = ((bf16[4,16,2,2,16,128]{5,4,3,2,1,0:T(8,128)(2,1)}), bf16[4,16,2,2,16,128]{5,4,3,2,1,0:T(8,128)(2,1)S(1)}, u32[]{:S(2)}, u32[]{:S(2)}) async-start(bf16[4,16,2,2,16,128]{5,4,3,2,1,0:T(8,128)(2,1)} %broadcast_in_dim.2), calls=%async_computation.1 | async-start | bytes 2097152 | tf_op jit(solution)/shard_map/all_to_all | solution.py:409
  46.3 10.7 %collective-permute-start.1 = (bf16[4,192,128]{2,1,0:T(8,128)(2,1)}, bf16[4,192,128]{2,1,0:T(8,128)(2,1)S(1)}, u32[]{:S(2)}, u32[]{:S(2)}) collective-permute-start(bf16[4,192,128]{2,1,0:T(8,128)(2,1)} %get-tuple-element.25), channel_id=1, source_target_pairs={{0,1},{1,2},{2,3},{3,0},{4,5},{5,6},{6,7},{7,4},{8,9},{9,10},{10,1... | collective-permute-start | bytes 589832 | tf_op jit(solution)/shard_map/ppermute | solution.py:421
  49.5 12.1 %collective-permute-start.2 = (bf16[4,192,128]{2,1,0:T(8,128)(2,1)}, bf16[4,192,128]{2,1,0:T(8,128)(2,1)S(1)}, u32[]{:S(2)}, u32[]{:S(2)}) collective-permute-start(bf16[4,192,128]{2,1,0:T(8,128)(2,1)} %get-tuple-element.26), channel_id=1, source_target_pairs={{0,2},{1,3},{2,0},{3,1},{4,6},{5,7},{6,4},{7,5},{8,10},{9,11},{10,... | collective-permute-start | bytes 589832 | tf_op jit(solution)/shard_map/ppermute | solution.py:421
  54.1 8.2 %copy-start.3 = (s32[3]{0:T(128)S(1)}, s32[3]{0:T(128)}, u32[]{:S(2)}) copy-start(s32[3]{0:T(128)} %pad_add_fusion.s_ref) | copy-start | bytes 40
  54.1 8.2 %collective-permute-start.3 = (bf16[4,192,128]{2,1,0:T(8,128)(2,1)}, bf16[4,192,128]{2,1,0:T(8,128)(2,1)S(1)}, u32[]{:S(2)}, u32[]{:S(2)}) collective-permute-start(bf16[4,192,128]{2,1,0:T(8,128)(2,1)} %get-tuple-element.27), channel_id=1, source_target_pairs={{0,3},{1,0},{2,1},{3,2},{4,7},{5,4},{6,5},{7,6},{8,11},{9,8},{10,9... | collective-permute-start | bytes 589832 | tf_op jit(solution)/shard_map/ppermute | solution.py:421
  62.3 0.9 copy-start.2
  63.9 1.7 %copy-start = (bf16[4,16,2,2,16,128]{5,4,3,2,1,0:T(8,128)(2,1)}, bf16[4,16,2,2,16,128]{5,4,3,2,1,0:T(8,128)(2,1)S(1)}, u32[]{:S(2)}) copy-start(bf16[4,16,2,2,16,128]{5,4,3,2,1,0:T(8,128)(2,1)S(1)} %all-to-all-done.1.x_ref) | copy-start | bytes 3145732
  89.6 1.3 copy-start.1
  103.4 21.5 %all-to-all-start.5 = ((bf16[16,40,128]{2,1,0:T(8,128)(2,1)}), bf16[16,40,128]{2,1,0:T(8,128)(2,1)S(1)}, u32[]{:S(2)}, u32[]{:S(2)}) async-start(bf16[16,40,128]{2,1,0:T(8,128)(2,1)} %shard_map.116), calls=%async_computation.5 | async-start | bytes 327680 | tf_op jit(solution)/shard_map/all_to_all | solution.py:405
  116.3 18.6 %collective-permute-start.5 = (bf16[192,512]{1,0:T(8,128)(2,1)}, bf16[192,512]{1,0:T(8,128)(2,1)S(1)}, u32[]{:S(2)}, u32[]{:S(2)}) collective-permute-start(bf16[192,512]{1,0:T(8,128)(2,1)} %get-tuple-element.33), channel_id=1, source_target_pairs={{0,1},{1,2},{2,3},{3,0},{4,5},{5,6},{6,7},{7,4},{8,9},{9,10},{10,1... | collective-permute-start | bytes 589832 | tf_op jit(solution)/shard_map/ppermute | solution.py:421
  118.5 16.5 %collective-permute-start.6 = (bf16[192,512]{1,0:T(8,128)(2,1)}, bf16[192,512]{1,0:T(8,128)(2,1)S(1)}, u32[]{:S(2)}, u32[]{:S(2)}) collective-permute-start(bf16[192,512]{1,0:T(8,128)(2,1)} %get-tuple-element.34), channel_id=1, source_target_pairs={{0,2},{1,3},{2,0},{3,1},{4,6},{5,7},{6,4},{7,5},{8,10},{9,11},{10,... | collective-permute-start | bytes 589832 | tf_op jit(solution)/shard_map/ppermute | solution.py:421
  121.9 13.1 %collective-permute-start.7 = (bf16[192,512]{1,0:T(8,128)(2,1)}, bf16[192,512]{1,0:T(8,128)(2,1)S(1)}, u32[]{:S(2)}, u32[]{:S(2)}) collective-permute-start(bf16[192,512]{1,0:T(8,128)(2,1)} %get-tuple-element.35), channel_id=1, source_target_pairs={{0,3},{1,0},{2,1},{3,2},{4,7},{5,4},{6,5},{7,6},{8,11},{9,8},{10,9... | collective-permute-start | bytes 589832 | tf_op jit(solution)/shard_map/ppermute | solution.py:421
  124.9 14.2 %collective-permute-start.4 = (bf16[16,24,128]{2,1,0:T(8,128)(2,1)S(1)}, bf16[16,24,128]{2,1,0:T(8,128)(2,1)S(1)}, u32[]{:S(2)}, u32[]{:S(2)}) collective-permute-start(bf16[16,24,128]{2,1,0:T(8,128)(2,1)S(1)} %slice.4), channel_id=1, source_target_pairs={{0,16},{16,0},{1,17},{17,1},{2,18},{18,2},{3,19},{19,3},{4,20},{20... | collective-permute-start | bytes 294920 | tf_op jit(solution)/shard_map/ppermute | solution.py:425
  134.9 0.7 copy-start.7
  135.0 0.7 copy-start.8
  135.0 0.8 copy-start.9
  135.8 3.3 %copy-start.4 = (s32[3]{0:T(128)S(1)}, s32[3]{0:T(128)}, u32[]{:S(2)}) copy-start(s32[3]{0:T(128)} %pad_add_fusion.s_ref) | copy-start | bytes 40
  135.8 3.3 %copy-start.5 = (s32[128,2]{0,1:T(2,128)S(1)}, s32[128,2]{0,1:T(2,128)}, u32[]{:S(2)}) copy-start(s32[128,2]{0,1:T(2,128)} %param.9) | copy-start | bytes 3076
  135.8 3.3 %copy-start.6 = (bf16[128,2]{0,1:T(2,128)(2,1)S(1)}, bf16[128,2]{0,1:T(2,128)(2,1)}, u32[]{:S(2)}) copy-start(bf16[128,2]{0,1:T(2,128)(2,1)} %param.10) | copy-start | bytes 1540
